TPU v7x, 512 devices: a 8x2x16 block of a 8x8x16 slice. The times are simulated.
512 devices in a mesh: grp: 2 (over y), sp: 16 (over z), tp: 16 (over x, core).
Axes of the slice: x: 8, y: 2, z: 16, core: 2. Of those that a mesh axis runs over, the one named last changes fastest.
The devices are a block of a 8x8x16 slice.
Arguments:
- target: bfloat16 [8192, 2048], P(('grp', 'sp', 'tp')), parts along dimension 0, may hold values from -20 to 20
- source: bfloat16 [16384, 2048], P(('grp', 'sp')), parts along dimension 0, may hold values from -20 to 20
- source_gain: float32 [2048], replicated, may hold values from 0.1 to 1.9
- query_gain: float32 [2, 2048], replicated, may hold values from 0.1 to 1.9
- out_gain: float32 [2, 2048], replicated, may hold values from 0.1 to 1.9
- query_weight: bfloat16 [2, 2048, 2048], P(None, None, 'tp'), may hold values from -1 to 1
- key_weight: bfloat16 [2, 2048, 512], P(None, None, 'tp'), may hold values from -1 to 1
- value_weight: bfloat16 [2, 2048, 512], P(None, None, 'tp'), may hold values from -0.125 to 0.125
- out_weight: bfloat16 [2, 2048, 2048], P(None, 'tp'), may hold values from -0.125 to 0.125
Outputs:
- result: bfloat16 [8192, 2048], P(('grp', 'sp', 'tp')), parts along dimension 0
There are 2 independent parts, one for each index of `grp`. A program takes and returns all parts, laid end to end along the dimension named above; an argument that names none is the same for every part. Nothing has to cross between parts.
All inputs are finite; a program needn't handle non-finite values.
Results may differ from a plain program's by a relative error of at most 0.024.
Values may be sent and summed in bfloat16 or wider, within the bound.
No kernel may reach another device: no remote copies, remote signals or barrier semaphores. Data moves between devices by JAX's collectives and lax.ppermute only.
A program may use at most 64 MiB of HBM per device.

v0:
```python
import jax
import jax.numpy as jnp
from jax import lax
from jax.sharding import PartitionSpec as P

HD = 256
QH = 8
KVH = 2
LAYERS = 2


EPSILON = 1e-06


def swapped(value, axis, distance):
    mask = 2**distance
    pairs = [(source, source ^ mask) for source in range(lax.axis_size(axis))]
    return lax.ppermute(value, axis, pairs)


def joined_along(blocks, dim):
    blocks = jnp.moveaxis(blocks, 0, dim)
    dims = blocks.shape
    return blocks.reshape(*dims[:dim], dims[dim] * dims[dim + 1], *dims[dim + 2 :])


def sent_to_all(value, axis):
    copies = jnp.broadcast_to(value, (lax.axis_size(axis), *value.shape))
    return lax.all_to_all(copies, axis, split_axis=0, concat_axis=0, tiled=True)


def gather_directly(value, axis, dim):
    return joined_along(sent_to_all(value, axis), dim)


def side_by_side(arrays, axis, dim, along):
    columns = [a.reshape(*a.shape[:along], -1) for a in arrays]
    both = jnp.concatenate(columns, axis=along)
    result, at, done = (lax.all_gather(both, axis, axis=dim, tiled=True), 0, [])
    for a, column in zip(arrays, columns):
        slab = result[..., at : at + column.shape[along]]
        done.append(slab.reshape(*slab.shape[:along], *a.shape[along:]))
        at += column.shape[along]
    return tuple(done)


def in_blocks(value, dim, peers):
    before, after = (value.shape[:dim], value.shape[dim + 1 :])
    return jnp.moveaxis(value.reshape(*before, peers, -1, *after), dim, 0)


def sum_at_owner(value, axis, dim):
    blocks = in_blocks(value, dim, lax.axis_size(axis))
    arrived = lax.all_to_all(blocks, axis, split_axis=0, concat_axis=0, tiled=True)
    return arrived.astype(jnp.float32).sum(axis=0)


def rms_scaled(matrix_rows, gain_row):
    values = matrix_rows.astype(jnp.float32)
    inverse = lax.rsqrt(jnp.mean(values * values, axis=-1, keepdims=True) + EPSILON)
    return values * inverse * gain_row


def group_rounds(holding, bit_count, position):
    for bit_number in range(bit_count):
        my_bit = position >> bit_number & 1
        if holding.shape[0] > 1:
            halves = holding.reshape((holding.shape[0] // 2, 2) + holding.shape[1:])
            kept_part = lax.dynamic_index_in_dim(halves, my_bit, 1, False)
            outgoing = lax.dynamic_index_in_dim(halves, 1 - my_bit, 1, False)
        else:
            kept_part = holding
            outgoing = holding
        arrived = swapped(outgoing, "tp", bit_number)
        holding = jnp.where(
            my_bit == 0,
            jnp.concatenate([kept_part, arrived], 1),
            jnp.concatenate([arrived, kept_part], 1),
        )
    return holding


def spread_heads(factor, piece_index, piece_width):
    columns = jnp.repeat(factor, HD, axis=1)
    pieces = columns.reshape(factor.shape[0], columns.shape[1] // piece_width, piece_width)
    return jnp.take(pieces, piece_index, axis=1)


def merge_partials(weighted, row_peak, row_total, bit_count, position):
    piece_width = weighted.shape[2]
    piece_index = jnp.arange(weighted.shape[1], dtype=jnp.int32)
    for bit_number in range(bit_count):
        my_bit = position >> bit_number & 1
        halves = weighted.reshape(weighted.shape[0], weighted.shape[1] // 2, 2, piece_width)
        kept_part = lax.dynamic_index_in_dim(halves, my_bit, 2, False)
        outgoing = lax.dynamic_index_in_dim(halves, 1 - my_bit, 2, False)
        piece_index = lax.dynamic_index_in_dim(piece_index.reshape(-1, 2), my_bit, 1, False)
        far_weighted, far_peak, far_total = (
            swapped(outgoing.astype(jnp.bfloat16), "tp", bit_number).astype(outgoing.dtype),
            swapped(row_peak.astype(jnp.bfloat16), "tp", bit_number).astype(row_peak.dtype),
            swapped(row_total.astype(jnp.bfloat16), "tp", bit_number).astype(row_total.dtype),
        )
        new_peak = jnp.maximum(row_peak, far_peak)
        near_factor = jnp.exp(row_peak - new_peak)
        far_factor = jnp.exp(far_peak - new_peak)
        row_total = row_total * near_factor + far_total * far_factor
        weighted = kept_part * spread_heads(
            near_factor, piece_index, piece_width
        ) + far_weighted * spread_heads(far_factor, piece_index, piece_width)
        row_peak = new_peak
    return (weighted, row_total, piece_index)


def attend(carried, key_rows, value_rows, grouped, score_scale):
    row_peak, row_total, weighted = carried
    scores = (
        jnp.einsum("rhd,nd->rhn", grouped, key_rows, preferred_element_type=jnp.float32)
        * score_scale
    )
    new_peak = jnp.maximum(row_peak, jnp.max(scores, axis=2))
    weights = jnp.exp(scores - new_peak[:, :, None])
    row_total = jnp.sum(weights, axis=2)
    weighted = jnp.einsum(
        "rhn,nd->rhd", weights.astype(jnp.bfloat16), value_rows, preferred_element_type=jnp.float32
    )
    return (new_peak, row_total, weighted)


def body(
    target,
    source,
    source_gain,
    query_gain,
    out_gain,
    query_weight,
    key_weight,
    value_weight,
    out_weight,
):
    tp_devices = lax.axis_size("tp")
    group_size = tp_devices // KVH
    bit_count = group_size.bit_length() - 1
    position = lax.axis_index("tp") % group_size
    score_scale = HD ** (-0.5)
    heads_here = QH // KVH
    matrices = 2 * LAYERS
    slices = key_weight.shape[2]
    block_rows = source.shape[0] // group_size
    normed_source = rms_scaled(source, source_gain).astype(jnp.bfloat16)
    joined = jnp.concatenate(
        [
            matrix[layer_index]
            for layer_index in range(LAYERS)
            for matrix in (key_weight, value_weight)
        ],
        axis=1,
    )
    key_slices = jnp.dot(normed_source, joined, preferred_element_type=jnp.float32).astype(
        jnp.bfloat16
    )
    holding = group_rounds(
        key_slices.reshape(group_size, 1, block_rows, matrices, slices), bit_count, position
    )
    local_keys = jnp.transpose(holding[0], (2, 1, 0, 3)).reshape(matrices, block_rows, HD)
    residual = target
    stored = None
    for layer_index in range(LAYERS):
        normed = rms_scaled(residual, query_gain[layer_index]).astype(jnp.bfloat16)
        layer_weight = query_weight[layer_index]
        queries = jnp.dot(
            gather_directly(normed, "tp", 0), layer_weight, preferred_element_type=jnp.float32
        ).astype(jnp.bfloat16)
        rows_all = queries.shape[0]
        gathered = group_rounds(queries[None, None], bit_count, position)[0]
        grouped = jnp.transpose(gathered, (1, 0, 2)).reshape(rows_all, heads_here, HD)
        start_state = (
            jnp.full((rows_all, heads_here), -1e30, jnp.float32),
            jnp.zeros((rows_all, heads_here), jnp.float32),
            jnp.zeros((rows_all, heads_here, HD), jnp.float32),
        )
        if layer_index == 0:
            empty_rows = jnp.zeros(
                (lax.axis_size("sp") * block_rows, matrices - 2, HD), jnp.bfloat16
            )
            later_keys = jnp.transpose(local_keys[2:], (1, 0, 2))
            portions = side_by_side((local_keys[0], local_keys[1], later_keys), "sp", 0, 1)
            updated = attend(
                (start_state + (empty_rows,))[:3], portions[0], portions[1], grouped, score_scale
            )
            kept_rows = portions[2]
            row_peak, row_total, weighted, stored = updated + (kept_rows,)
        else:
            row_peak, row_total, weighted = attend(
                start_state,
                stored[:, 2 * layer_index - 2],
                stored[:, 2 * layer_index - 1],
                grouped,
                score_scale,
            )
        piece_width = heads_here * HD // group_size
        merged, row_total, piece_index = merge_partials(
            weighted.reshape(rows_all, group_size, piece_width),
            row_peak,
            row_total,
            bit_count,
            position,
        )
        attended = (merged[:, 0] / spread_heads(row_total, piece_index, piece_width)[:, 0]).astype(
            jnp.bfloat16
        )
        out_layer = out_weight[layer_index]
        summed_rows = sum_at_owner(
            jnp.dot(attended, out_layer, preferred_element_type=jnp.float32).astype(jnp.bfloat16),
            "tp",
            0,
        )
        residual = (
            residual.astype(jnp.float32) + rms_scaled(summed_rows, out_gain[layer_index])
        ).astype(jnp.bfloat16)
    return residual


def solution(mesh):
    in_specs = (
        P(("grp", "sp", "tp"), None),
        P(("grp", "sp"), None),
        P(),
        P(),
        P(),
        P(None, None, "tp"),
        P(None, None, "tp"),
        P(None, None, "tp"),
        P(None, "tp", None),
    )
    out_specs = P(("grp", "sp", "tp"), None)
    return jax.shard_map(body, mesh=mesh, in_specs=in_specs, out_specs=out_specs, check_vma=False)
```

profile of v0, /device:TPU:65, one launch (start us, length us, event | category | flops | bytes accessed | tf_op | source)
XLA Modules:
  0.0 382.2 jit_solution(11852382880942072104)
XLA Ops:
  13.1 43.5 %collective-permute-start.3 = (bf16[4,1,64,4,32]{2,4,3,1,0:T(8,128)(2,1)S(1)}, bf16[4,1,64,4,32]{2,4,3,1,0:T(8,128)(2,1)S(1)}, u32[]{:S(2)}, u32[]{:S(2)}) collective-permute-start(bf16[4,1,64,4,32]{2,4,3,1,0:T(8,128)(2,1)S(1)} %bitcast.245), channel_id=1, source_target_pairs={{0,1},{1,0},{2,3},{3,2},{4,5},{5,4},{6,7},{7,6},{8,9},{9,8},{10,11... | collective-permute-start | bytes 196616 | tf_op jit(solution)/shard_map/ppermute | solution.py:18
  59.7 4.6 %collective-permute-done.4 = bf16[2,2,64,4,32]{2,4,3,1,0:T(8,128)(2,1)S(1)} collective-permute-done((bf16[2,2,64,4,32]{2,4,3,1,0:T(8,128)(2,1)S(1)}, bf16[2,2,64,4,32]{2,4,3,1,0:T(8,128)(2,1)S(1)}, u32[]{:S(2)}, u32[]{:S(2)}) %collective-permute-start.4) | collective-permute-done | bytes 65568 | tf_op jit(solution)/shard_map/ppermute | solution.py:18
  66.5 8.9 %collective-permute-done.5 = bf16[1,4,64,4,32]{2,4,3,1,0:T(8,128)(2,1)S(1)} collective-permute-done((bf16[1,4,64,4,32]{2,4,3,1,0:T(8,128)(2,1)S(1)}, bf16[1,4,64,4,32]{2,4,3,1,0:T(8,128)(2,1)S(1)}, u32[]{:S(2)}, u32[]{:S(2)}) %collective-permute-start.5) | collective-permute-done | bytes 65568 | tf_op jit(solution)/shard_map/ppermute | solution.py:18
  77.9 4.0 %all-to-all-start = ((bf16[16,16,2048]{2,1,0:T(8,128)(2,1)}), bf16[16,16,2048]{2,1,0:T(8,128)(2,1)S(1)}, u32[]{:S(2)}, u32[]{:S(2)}) async-start(bf16[16,16,2048]{2,1,0:T(8,128)(2,1)} %broadcast_in_dim.145), calls=%async_computation | async-start | bytes 2097152 | tf_op jit(solution)/shard_map/all_to_all | solution.py:29
  82.2 27.8 %all-to-all-done = bf16[16,16,2048]{2,1,0:T(8,128)(2,1)S(1)} async-done(((bf16[16,16,2048]{2,1,0:T(8,128)(2,1)}), bf16[16,16,2048]{2,1,0:T(8,128)(2,1)S(1)}, u32[]{:S(2)}, u32[]{:S(2)}) %all-to-all-start) | async-done | bytes 1048608 | tf_op jit(solution)/shard_map/all_to_all | solution.py:29
  115.6 4.9 %collective-permute-done.1 = bf16[1,2,256,128]{2,3,1,0:T(8,128)(2,1)S(1)} collective-permute-done((bf16[1,2,256,128]{2,3,1,0:T(8,128)(2,1)S(1)}, bf16[1,2,256,128]{2,3,1,0:T(8,128)(2,1)S(1)}, u32[]{:S(2)}, u32[]{:S(2)}) %collective-permute-start.1) | collective-permute-done | bytes 131104 | tf_op jit(solution)/shard_map/ppermute | solution.py:18
  125.3 12.0 %collective-permute-done.2 = bf16[1,4,256,128]{2,3,1,0:T(8,128)(2,1)S(1)} collective-permute-done((bf16[1,4,256,128]{2,3,1,0:T(8,128)(2,1)S(1)}, bf16[1,4,256,128]{2,3,1,0:T(8,128)(2,1)S(1)}, u32[]{:S(2)}, u32[]{:S(2)}) %collective-permute-start.2) | collective-permute-done | bytes 262176 | tf_op jit(solution)/shard_map/ppermute | solution.py:18
  139.5 10.5 %collective-permute-start.6 = (bf16[256,4]{0,1:T(4,128)(2,1)S(1)}, bf16[256,4]{0,1:T(4,128)(2,1)S(1)}, u32[]{:S(2)}, u32[]{:S(2)}) collective-permute-start(bf16[256,4]{0,1:T(4,128)(2,1)S(1)} %fusion.75), channel_id=1, source_target_pairs={{0,1},{1,0},{2,3},{3,2},{4,5},{5,4},{6,7},{7,6},{8,9},{9,8},{10,11... | collective-permute-start | bytes 6152 | tf_op jit(solution)/shard_map/ppermute | solution.py:18
  157.4 3.0 collective-permute-start.8
  163.4 4.0 %collective-permute-start.10 = (bf16[256,4]{0,1:T(4,128)(2,1)}, bf16[256,4]{0,1:T(4,128)(2,1)S(1)}, u32[]{:S(2)}, u32[]{:S(2)}) collective-permute-start(bf16[256,4]{0,1:T(4,128)(2,1)} %fusion.77), channel_id=1, source_target_pairs={{0,4},{1,5},{2,6},{3,7},{4,0},{5,1},{6,2},{7,3},{8,12},{9,13},{10,... | collective-permute-start | bytes 6152 | tf_op jit(solution)/shard_map/ppermute | solution.py:18
  180.3 3.0 collective-permute-start.9
  183.4 2.7 collective-permute-done.9
  187.2 4.0 %collective-permute-start.11 = (bf16[256,1,128]{2,0,1:T(8,128)(2,1)S(1)}, bf16[256,1,128]{2,0,1:T(8,128)(2,1)S(1)}, u32[]{:S(2)}, u32[]{:S(2)}) collective-permute-start(bf16[256,1,128]{2,0,1:T(8,128)(2,1)S(1)} %dynamic-slice_convert_fusion.2), channel_id=1, source_target_pairs={{0,4},{1,5},{2,6},{3,7},{4,0},{5,1},{6,2},{7,3},{8,12},{9,13},{10,... | collective-permute-start | bytes 196616 | tf_op jit(solution)/shard_map/ppermute | solution.py:18
  193.1 2.6 convolution_convert_fusion.1
  195.7 10.7 %all-to-all-start.1 = ((bf16[16,16,2048]{2,1,0:T(8,128)(2,1)}), bf16[16,16,2048]{2,1,0:T(8,128)(2,1)S(1)}, u32[]{:S(2)}, u32[]{:S(2)}) async-start(bf16[16,16,2048]{2,1,0:T(8,128)(2,1)} %bitcast.50), calls=%async_computation.1 | async-start | bytes 2097152 | tf_op jit(solution)/shard_map/all_to_all | solution.py:54
  206.5 28.0 %all-to-all-done.1 = bf16[16,16,2048]{2,1,0:T(8,128)(2,1)S(1)} async-done(((bf16[16,16,2048]{2,1,0:T(8,128)(2,1)}), bf16[16,16,2048]{2,1,0:T(8,128)(2,1)S(1)}, u32[]{:S(2)}, u32[]{:S(2)}) %all-to-all-start.1) | async-done | bytes 1048608 | tf_op jit(solution)/shard_map/all_to_all | solution.py:54
  235.2 31.7 %all_to_all.20 = bf16[16,16,2048]{2,1,0:T(8,128)(2,1)S(1)} all-to-all(bf16[16,16,2048]{2,1,0:T(8,128)(2,1)S(1)} %broadcast_in_dim.168), channel_id=1, replica_groups=mesh['grp'=2,'sp'=16,'tp'=16] {'tp'}, dimensions={0} | all-to-all | bytes 2097152 | tf_op jit(solution)/shard_map/all_to_all | solution.py:29
  273.6 4.6 %collective-permute-done.16 = bf16[1,2,256,128]{2,3,1,0:T(8,128)(2,1)S(1)} collective-permute-done((bf16[1,2,256,128]{2,3,1,0:T(8,128)(2,1)}, bf16[1,2,256,128]{2,3,1,0:T(8,128)(2,1)S(1)}, u32[]{:S(2)}, u32[]{:S(2)}) %collective-permute-start.16) | collective-permute-done | bytes 131104 | tf_op jit(solution)/shard_map/ppermute | solution.py:18
  284.7 11.2 %collective-permute-done.17 = bf16[1,4,256,128]{2,3,1,0:T(8,128)(2,1)} collective-permute-done((bf16[1,4,256,128]{2,3,1,0:T(8,128)(2,1)}, bf16[1,4,256,128]{2,3,1,0:T(8,128)(2,1)}, u32[]{:S(2)}, u32[]{:S(2)}) %collective-permute-start.17) | collective-permute-done | bytes 262176 | tf_op jit(solution)/shard_map/ppermute | solution.py:18
  309.3 3.4 collective-permute-start.25
  314.7 4.3 %collective-permute-start.26 = (bf16[256,4]{0,1:T(4,128)(2,1)S(1)}, bf16[256,4]{0,1:T(4,128)(2,1)S(1)}, u32[]{:S(2)}, u32[]{:S(2)}) collective-permute-start(bf16[256,4]{0,1:T(4,128)(2,1)S(1)} %get-tuple-element.22), channel_id=1, source_target_pairs={{0,4},{1,5},{2,6},{3,7},{4,0},{5,1},{6,2},{7,3},{8,12},{9,13},{10,... | collective-permute-start | bytes 6152 | tf_op jit(solution)/shard_map/ppermute | solution.py:18
  327.3 3.7 collective-permute-done.21
  334.4 4.3 %collective-permute-done.23 = bf16[256,1,128]{2,0,1:T(8,128)(2,1)S(1)} collective-permute-done((bf16[256,1,128]{2,0,1:T(8,128)(2,1)S(1)}, bf16[256,1,128]{2,0,1:T(8,128)(2,1)S(1)}, u32[]{:S(2)}, u32[]{:S(2)}) %collective-permute-start.23) | collective-permute-done | bytes 65568 | tf_op jit(solution)/shard_map/ppermute | solution.py:18
  340.3 34.1 %all_to_all.21 = bf16[16,16,2048]{2,1,0:T(8,128)(2,1)S(1)} all-to-all(bf16[16,16,2048]{2,1,0:T(8,128)(2,1)S(1)} %bitcast.214), channel_id=1, replica_groups=mesh['grp'=2,'sp'=16,'tp'=16] {'tp'}, dimensions={0} | all-to-all | bytes 2097152 | tf_op jit(solution)/shard_map/all_to_all | solution.py:54
  (218 shorter events, 94.3 us)
Async XLA Ops:
  6.5 130.9 %all-gather.2.cloned.1.call-start = ((), (), s32[]{:S(2)}) async-start(), calls=%async_computation.4 | async-start | bytes 2228224 | tf_op jit(solution)/shard_map/all_gather | solution.py:39
  13.1 44.5 %collective-permute-start.3 = (bf16[4,1,64,4,32]{2,4,3,1,0:T(8,128)(2,1)S(1)}, bf16[4,1,64,4,32]{2,4,3,1,0:T(8,128)(2,1)S(1)}, u32[]{:S(2)}, u32[]{:S(2)}) collective-permute-start(bf16[4,1,64,4,32]{2,4,3,1,0:T(8,128)(2,1)S(1)} %bitcast.245), channel_id=1, source_target_pairs={{0,1},{1,0},{2,3},{3,2},{4,5},{5,4},{6,7},{7,6},{8,9},{9,8},{10,11... | collective-permute-start | bytes 196616 | tf_op jit(solution)/shard_map/ppermute | solution.py:18
  57.7 6.6 %collective-permute-start.4 = (bf16[2,2,64,4,32]{2,4,3,1,0:T(8,128)(2,1)S(1)}, bf16[2,2,64,4,32]{2,4,3,1,0:T(8,128)(2,1)S(1)}, u32[]{:S(2)}, u32[]{:S(2)}) collective-permute-start(bf16[2,2,64,4,32]{2,4,3,1,0:T(8,128)(2,1)S(1)} %get-tuple-element.52), channel_id=1, source_target_pairs={{0,2},{1,3},{2,0},{3,1},{4,6},{5,7},{6,4},{7,5},{8,10},{9,11},{10,... | collective-permute-start | bytes 196616 | tf_op jit(solution)/shard_map/ppermute | solution.py:18
  64.4 11.0 %collective-permute-start.5 = (bf16[1,4,64,4,32]{2,4,3,1,0:T(8,128)(2,1)S(1)}, bf16[1,4,64,4,32]{2,4,3,1,0:T(8,128)(2,1)S(1)}, u32[]{:S(2)}, u32[]{:S(2)}) collective-permute-start(bf16[1,4,64,4,32]{2,4,3,1,0:T(8,128)(2,1)S(1)} %get-tuple-element.50), channel_id=1, source_target_pairs={{0,4},{1,5},{2,6},{3,7},{4,0},{5,1},{6,2},{7,3},{8,12},{9,13},{10,... | collective-permute-start | bytes 196616 | tf_op jit(solution)/shard_map/ppermute | solution.py:18
  77.9 32.1 %all-to-all-start = ((bf16[16,16,2048]{2,1,0:T(8,128)(2,1)}), bf16[16,16,2048]{2,1,0:T(8,128)(2,1)S(1)}, u32[]{:S(2)}, u32[]{:S(2)}) async-start(bf16[16,16,2048]{2,1,0:T(8,128)(2,1)} %broadcast_in_dim.145), calls=%async_computation | async-start | bytes 2097152 | tf_op jit(solution)/shard_map/all_to_all | solution.py:29
  113.6 6.9 %collective-permute-start.1 = (bf16[1,2,256,128]{2,3,1,0:T(8,128)(2,1)S(1)}, bf16[1,2,256,128]{2,3,1,0:T(8,128)(2,1)S(1)}, u32[]{:S(2)}, u32[]{:S(2)}) collective-permute-start(bf16[1,2,256,128]{2,3,1,0:T(8,128)(2,1)S(1)} %maximum_select_fusion.10), channel_id=1, source_target_pairs={{0,2},{1,3},{2,0},{3,1},{4,6},{5,7},{6,4},{7,5},{8,10},{9,11},{10,... | collective-permute-start | bytes 393224 | tf_op jit(solution)/shard_map/ppermute | solution.py:18
  120.6 16.8 %collective-permute-start.2 = (bf16[1,4,256,128]{2,3,1,0:T(8,128)(2,1)S(1)}, bf16[1,4,256,128]{2,3,1,0:T(8,128)(2,1)S(1)}, u32[]{:S(2)}, u32[]{:S(2)}) collective-permute-start(bf16[1,4,256,128]{2,3,1,0:T(8,128)(2,1)S(1)} %maximum_select_fusion.3), channel_id=1, source_target_pairs={{0,4},{1,5},{2,6},{3,7},{4,0},{5,1},{6,2},{7,3},{8,12},{9,13},{10,... | collective-permute-start | bytes 786440 | tf_op jit(solution)/shard_map/ppermute | solution.py:18
  139.5 17.8 %collective-permute-start.6 = (bf16[256,4]{0,1:T(4,128)(2,1)S(1)}, bf16[256,4]{0,1:T(4,128)(2,1)S(1)}, u32[]{:S(2)}, u32[]{:S(2)}) collective-permute-start(bf16[256,4]{0,1:T(4,128)(2,1)S(1)} %fusion.75), channel_id=1, source_target_pairs={{0,1},{1,0},{2,3},{3,2},{4,5},{5,4},{6,7},{7,6},{8,9},{9,8},{10,11... | collective-permute-start | bytes 6152 | tf_op jit(solution)/shard_map/ppermute | solution.py:18
  150.9 9.5 %collective-permute-start.12 = (bf16[256,4]{0,1:T(4,128)(2,1)S(1)}, bf16[256,4]{0,1:T(4,128)(2,1)S(1)}, u32[]{:S(2)}, u32[]{:S(2)}) collective-permute-start(bf16[256,4]{0,1:T(4,128)(2,1)S(1)} %convert_element_type.210), channel_id=1, source_target_pairs={{0,1},{1,0},{2,3},{3,2},{4,5},{5,4},{6,7},{7,6},{8,9},{9,8},{10,11... | collective-permute-start | bytes 6152 | tf_op jit(solution)/shard_map/ppermute | solution.py:18
  154.9 23.8 %collective-permute-start.7 = (bf16[256,4,128]{2,0,1:T(8,128)(2,1)}, bf16[256,4,128]{2,0,1:T(8,128)(2,1)}, u32[]{:S(2)}, u32[]{:S(2)}) collective-permute-start(bf16[256,4,128]{2,0,1:T(8,128)(2,1)} %bitcast.241), channel_id=1, source_target_pairs={{0,1},{1,0},{2,3},{3,2},{4,5},{5,4},{6,7},{7,6},{8,9},{9,8},{10,11... | collective-permute-start | bytes 786440 | tf_op jit(solution)/shard_map/ppermute | solution.py:18
  160.4 7.0 %collective-permute-start.13 = (bf16[256,4]{0,1:T(4,128)(2,1)S(1)}, bf16[256,4]{0,1:T(4,128)(2,1)S(1)}, u32[]{:S(2)}, u32[]{:S(2)}) collective-permute-start(bf16[256,4]{0,1:T(4,128)(2,1)S(1)} %get-tuple-element.39), channel_id=1, source_target_pairs={{0,2},{1,3},{2,0},{3,1},{4,6},{5,7},{6,4},{7,5},{8,10},{9,11},{10,... | collective-permute-start | bytes 6152 | tf_op jit(solution)/shard_map/ppermute | solution.py:18
  163.4 15.3 %collective-permute-start.10 = (bf16[256,4]{0,1:T(4,128)(2,1)}, bf16[256,4]{0,1:T(4,128)(2,1)S(1)}, u32[]{:S(2)}, u32[]{:S(2)}) collective-permute-start(bf16[256,4]{0,1:T(4,128)(2,1)} %fusion.77), channel_id=1, source_target_pairs={{0,4},{1,5},{2,6},{3,7},{4,0},{5,1},{6,2},{7,3},{8,12},{9,13},{10,... | collective-permute-start | bytes 6152 | tf_op jit(solution)/shard_map/ppermute | solution.py:18
  167.4 11.2 %collective-permute-start.14 = (bf16[256,4]{0,1:T(4,128)(2,1)S(1)}, bf16[256,4]{0,1:T(4,128)(2,1)S(1)}, u32[]{:S(2)}, u32[]{:S(2)}) collective-permute-start(bf16[256,4]{0,1:T(4,128)(2,1)S(1)} %get-tuple-element.35), channel_id=1, source_target_pairs={{0,4},{1,5},{2,6},{3,7},{4,0},{5,1},{6,2},{7,3},{8,12},{9,13},{10,... | collective-permute-start | bytes 6152 | tf_op jit(solution)/shard_map/ppermute | solution.py:18
  180.3 5.7 %collective-permute-start.9 = (bf16[256,2,128]{2,0,1:T(8,128)(2,1)S(1)}, bf16[256,2,128]{2,0,1:T(8,128)(2,1)S(1)}, u32[]{:S(2)}, u32[]{:S(2)}) collective-permute-start(bf16[256,2,128]{2,0,1:T(8,128)(2,1)S(1)} %fusion.54), channel_id=1, source_target_pairs={{0,2},{1,3},{2,0},{3,1},{4,6},{5,7},{6,4},{7,5},{8,10},{9,11},{10,... | collective-permute-start | bytes 393224 | tf_op jit(solution)/shard_map/ppermute | solution.py:18
  187.2 5.9 %collective-permute-start.11 = (bf16[256,1,128]{2,0,1:T(8,128)(2,1)S(1)}, bf16[256,1,128]{2,0,1:T(8,128)(2,1)S(1)}, u32[]{:S(2)}, u32[]{:S(2)}) collective-permute-start(bf16[256,1,128]{2,0,1:T(8,128)(2,1)S(1)} %dynamic-slice_convert_fusion.2), channel_id=1, source_target_pairs={{0,4},{1,5},{2,6},{3,7},{4,0},{5,1},{6,2},{7,3},{8,12},{9,13},{10,... | collective-permute-start | bytes 196616 | tf_op jit(solution)/shard_map/ppermute | solution.py:18
  195.7 38.7 %all-to-all-start.1 = ((bf16[16,16,2048]{2,1,0:T(8,128)(2,1)}), bf16[16,16,2048]{2,1,0:T(8,128)(2,1)S(1)}, u32[]{:S(2)}, u32[]{:S(2)}) async-start(bf16[16,16,2048]{2,1,0:T(8,128)(2,1)} %bitcast.50), calls=%async_computation.1 | async-start | bytes 2097152 | tf_op jit(solution)/shard_map/all_to_all | solution.py:54
  271.2 7.0 %collective-permute-start.16 = (bf16[1,2,256,128]{2,3,1,0:T(8,128)(2,1)}, bf16[1,2,256,128]{2,3,1,0:T(8,128)(2,1)S(1)}, u32[]{:S(2)}, u32[]{:S(2)}) collective-permute-start(bf16[1,2,256,128]{2,3,1,0:T(8,128)(2,1)} %maximum_select_fusion.12), channel_id=1, source_target_pairs={{0,2},{1,3},{2,0},{3,1},{4,6},{5,7},{6,4},{7,5},{8,10},{9,11},{10,... | collective-permute-start | bytes 393224 | tf_op jit(solution)/shard_map/ppermute | solution.py:18
  278.9 17.0 %collective-permute-start.17 = (bf16[1,4,256,128]{2,3,1,0:T(8,128)(2,1)}, bf16[1,4,256,128]{2,3,1,0:T(8,128)(2,1)}, u32[]{:S(2)}, u32[]{:S(2)}) collective-permute-start(bf16[1,4,256,128]{2,3,1,0:T(8,128)(2,1)} %maximum_select_fusion.8), channel_id=1, source_target_pairs={{0,4},{1,5},{2,6},{3,7},{4,0},{5,1},{6,2},{7,3},{8,12},{9,13},{10,... | collective-permute-start | bytes 786440 | tf_op jit(solution)/shard_map/ppermute | solution.py:18
  297.9 9.4 %collective-permute-start.18 = (bf16[256,4]{0,1:T(4,128)(2,1)S(1)}, bf16[256,4]{0,1:T(4,128)(2,1)S(1)}, u32[]{:S(2)}, u32[]{:S(2)}) collective-permute-start(bf16[256,4]{0,1:T(4,128)(2,1)S(1)} %fusion.76), channel_id=1, source_target_pairs={{0,1},{1,0},{2,3},{3,2},{4,5},{5,4},{6,7},{7,6},{8,9},{9,8},{10,11... | collective-permute-start | bytes 6152 | tf_op jit(solution)/shard_map/ppermute | solution.py:18
  301.3 8.0 %collective-permute-start.24 = (bf16[256,4]{0,1:T(4,128)(2,1)S(1)}, bf16[256,4]{0,1:T(4,128)(2,1)S(1)}, u32[]{:S(2)}, u32[]{:S(2)}) collective-permute-start(bf16[256,4]{0,1:T(4,128)(2,1)S(1)} %convert_element_type.239), channel_id=1, source_target_pairs={{0,1},{1,0},{2,3},{3,2},{4,5},{5,4},{6,7},{7,6},{8,9},{9,8},{10,11... | collective-permute-start | bytes 6152 | tf_op jit(solution)/shard_map/ppermute | solution.py:18
  304.8 19.2 %collective-permute-start.19 = (bf16[256,4,128]{2,0,1:T(8,128)(2,1)}, bf16[256,4,128]{2,0,1:T(8,128)(2,1)}, u32[]{:S(2)}, u32[]{:S(2)}) collective-permute-start(bf16[256,4,128]{2,0,1:T(8,128)(2,1)} %fusion.42), channel_id=1, source_target_pairs={{0,1},{1,0},{2,3},{3,2},{4,5},{5,4},{6,7},{7,6},{8,9},{9,8},{10,11... | collective-permute-start | bytes 786440 | tf_op jit(solution)/shard_map/ppermute | solution.py:18
  312.7 11.3 %collective-permute-start.22 = (bf16[256,4]{0,1:T(4,128)(2,1)S(1)}, bf16[256,4]{0,1:T(4,128)(2,1)S(1)}, u32[]{:S(2)}, u32[]{:S(2)}) collective-permute-start(bf16[256,4]{0,1:T(4,128)(2,1)S(1)} %fusion.78), channel_id=1, source_target_pairs={{0,4},{1,5},{2,6},{3,7},{4,0},{5,1},{6,2},{7,3},{8,12},{9,13},{10,... | collective-permute-start | bytes 6152 | tf_op jit(solution)/shard_map/ppermute | solution.py:18
  314.7 9.3 %collective-permute-start.26 = (bf16[256,4]{0,1:T(4,128)(2,1)S(1)}, bf16[256,4]{0,1:T(4,128)(2,1)S(1)}, u32[]{:S(2)}, u32[]{:S(2)}) collective-permute-start(bf16[256,4]{0,1:T(4,128)(2,1)S(1)} %get-tuple-element.22), channel_id=1, source_target_pairs={{0,4},{1,5},{2,6},{3,7},{4,0},{5,1},{6,2},{7,3},{8,12},{9,13},{10,... | collective-permute-start | bytes 6152 | tf_op jit(solution)/shard_map/ppermute | solution.py:18
  332.1 6.6 %collective-permute-start.23 = (bf16[256,1,128]{2,0,1:T(8,128)(2,1)S(1)}, bf16[256,1,128]{2,0,1:T(8,128)(2,1)S(1)}, u32[]{:S(2)}, u32[]{:S(2)}) collective-permute-start(bf16[256,1,128]{2,0,1:T(8,128)(2,1)S(1)} %dynamic-slice_convert_fusion.1), channel_id=1, source_target_pairs={{0,4},{1,5},{2,6},{3,7},{4,0},{5,1},{6,2},{7,3},{8,12},{9,13},{10,... | collective-permute-start | bytes 196616 | tf_op jit(solution)/shard_map/ppermute | solution.py:18
  (19 other events, 627.2 us)
Sparse Core Ops, SparseCore 0:
  76.8 59.4 all-gather.1
where the time goes:
time: 384 us; the launch traced here: 382 us
  starting transfers between devices  130 us (34%)
  waiting for transfers between devices  118 us (31%)
  blocking collectives  65.7 us (17%)
  local copies, waits for them, and re-layouts  24.4 us (6%)
  between operations  16.5 us (4%)
  other arithmetic  15.1 us (4%)
  matrix products  12.4 us (3%)
    ppermute x27, starting transfers between devices, swapped(): return lax.ppermute(value, axis, pairs)  115 us
    ppermute x27, waiting for transfers between devices, swapped(): return lax.ppermute(value, axis, pairs)  62.2 us
    all_to_all x1, blocking collectives, sum_at_owner(): lax.all_to_all(blocks, axis, split_axis=0, concat_axis=0, tiled=True)  34.1 us
    all_to_all x1, blocking collectives, sent_to_all(): return lax.all_to_all(copies, axis, split_axis=0, concat_axis=0, tiled=True)  31.7 us
    all_to_all x1, waiting for transfers between devices, sum_at_owner(): lax.all_to_all(blocks, axis, split_axis=0, concat_axis=0, tiled=True)  28 us
    all_to_all x1, waiting for transfers between devices, sent_to_all(): return lax.all_to_all(copies, axis, split_axis=0, concat_axis=0, tiled=True)  27.8 us
    all_to_all x1, starting transfers between devices, sum_at_owner(): lax.all_to_all(blocks, axis, split_axis=0, concat_axis=0, tiled=True)  10.7 us
    gather x8, local copies, waits for them, and re-layouts, spread_heads(): return jnp.take(pieces, piece_index, axis=1)  8.13 us
  transfers between devices with their start and end apart: 30, of which 15 were waited for; matrix products, arithmetic and copies ran while one was open for 7% of the time, Pallas kernels for 0%

commit v1 on v0

v1 whole, which is shorter than its diff:
```python
import jax
import jax.numpy as jnp
from jax import lax
from jax.experimental import pallas as pl
from jax.experimental.pallas import tpu as pltpu
from jax.sharding import Mesh
from jax.sharding import PartitionSpec as P

HD = 256
QH = 8
KVH = 2
LAYERS = 2
HERE = QH // KVH
EPSILON = 1e-06
STATS = 16

CHIPS = ("kv", "quarter")
GROUP = ("quarter", "core")
BF16 = jnp.bfloat16
F32 = jnp.float32


def dot(a, b, contract=((1,), (0,))):
    return lax.dot_general(a, b, (contract, ((), ())), preferred_element_type=F32)


def scaled(values, gain):
    inverse = lax.rsqrt(jnp.mean(values * values, axis=-1, keepdims=True) + EPSILON)
    return values * inverse * gain


def held_in_vmem(*arrays):
    return [pltpu.with_memory_space_constraint(a, pltpu.VMEM) for a in arrays]


def vmem_out(shape):
    return pltpu.VMEM(tuple(shape), BF16)


def in_vmem(count):
    return [pl.BlockSpec(memory_space=pltpu.VMEM)] * count


def source_kernel(source_ref, gain_ref, key_ref, value_ref, out_ref, weight_ref):
    width = key_ref.shape[2]

    @pl.when(pl.program_id(0) == 0)
    def _():
        for layer in range(LAYERS):
            weight_ref[:, layer * width : (layer + 1) * width] = key_ref[layer]
            weight_ref[:, (LAYERS + layer) * width : (LAYERS + layer + 1) * width] = value_ref[layer]

    normed = scaled(source_ref[...].astype(F32), gain_ref[...]).astype(BF16)
    columns = dot(normed, weight_ref[...]).T.astype(BF16)
    out_ref[...] = columns.reshape(out_ref.shape)


def source_columns(source, gain, key_weight, value_weight, quarters):
    rows, features = source.shape
    width = key_weight.shape[2]
    block = rows // quarters
    return pl.pallas_call(
        source_kernel,
        grid=(quarters,),
        in_specs=[
            pl.BlockSpec((block, features), lambda i: (i, 0)),
            pl.BlockSpec((1, features), lambda i: (0, 0)),
            pl.BlockSpec(key_weight.shape, lambda i: (0, 0, 0)),
            pl.BlockSpec(value_weight.shape, lambda i: (0, 0, 0)),
        ],
        out_specs=pl.BlockSpec((1, 2, LAYERS * width, block), lambda i: (i, 0, 0, 0)),
        out_shape=jax.ShapeDtypeStruct((quarters, 2, LAYERS * width, block), BF16),
        scratch_shapes=[pltpu.VMEM((features, 2 * LAYERS * width), BF16)],
        name="source_columns",
    )(source, gain, key_weight, value_weight)


def norm_kernel(rows_ref, gain_ref, out_ref):
    out_ref[...] = scaled(rows_ref[...].astype(F32), gain_ref[...]).astype(BF16)


def first_norm(rows, gain):
    return pl.pallas_call(
        norm_kernel,
        in_specs=in_vmem(2),
        out_specs=in_vmem(1)[0],
        out_shape=vmem_out(rows.shape),
        name="first_norm",
    )(*held_in_vmem(rows, gain))


def query_kernel(core_ref, rows_ref, mine_ref, other_ref, out_ref):
    chips, block, features = rows_ref.shape
    rows = rows_ref[...].reshape(chips * block, features)
    mine = dot(rows, mine_ref[...]).astype(BF16)
    other = dot(rows, other_ref[...]).astype(BF16)
    first = core_ref[0] == 0
    width = mine.shape[1]
    out_ref[:, :width] = jnp.where(first, mine, other)
    out_ref[:, width:] = jnp.where(first, other, mine)


def project_queries(core, rows, mine, other):
    chips, block, _ = rows.shape
    return pl.pallas_call(
        query_kernel,
        in_specs=[pl.BlockSpec(memory_space=pltpu.SMEM)] + in_vmem(3),
        out_specs=in_vmem(1)[0],
        out_shape=vmem_out((chips * block, 2 * mine.shape[1])),
        name="project_queries",
    )(core, *held_in_vmem(rows, mine, other))


def attend_kernel(core_ref, query_ref, mine_ref, other_ref, out_ref, score_ref):
    heads, rows, width = query_ref.shape
    blocks, _, block = mine_ref.shape
    queries = query_ref[...].reshape(heads * rows, width)
    scale = width ** (-0.5)

    def work(key_ref, value_ref):
        peak = None
        for b in range(0, blocks, 2):
            keys = jnp.concatenate([key_ref[b], key_ref[b + 1]], axis=1)
            scores = dot(queries, keys) * scale
            score_ref[:, b * block : (b + 2) * block] = scores
            top = jnp.max(scores, axis=1, keepdims=True)
            peak = top if peak is None else jnp.maximum(peak, top)
        total, mixed = None, None
        for b in range(0, blocks, 2):
            values = jnp.concatenate([value_ref[b], value_ref[b + 1]], axis=1)
            weights = jnp.exp(score_ref[:, b * block : (b + 2) * block] - peak)
            part = jnp.sum(weights, axis=1, keepdims=True)
            share = dot(weights.astype(BF16), values, ((1,), (1,)))
            total = part if total is None else total + part
            mixed = share if mixed is None else mixed + share
        out_ref[:, :rows, :] = (mixed / total).astype(BF16).reshape(heads, rows, width)
        level = peak + jnp.log(total)
        high = level.astype(BF16).astype(F32)
        low = level - high
        for h in range(heads):
            for part, at in ((high, 0), (low, rows)):
                column = jnp.broadcast_to(part[h * rows : (h + 1) * rows], (rows, rows))
                out_ref[h, rows:, at : at + rows] = column.T[:STATS].astype(BF16)

    @pl.when(core_ref[0] == 0)
    def _():
        work(mine_ref, other_ref)

    @pl.when(core_ref[0] != 0)
    def _():
        work(other_ref, mine_ref)


def attend(core, queries, mine, other):
    heads, rows, width = queries.shape
    blocks, _, block = mine.shape
    return pl.pallas_call(
        attend_kernel,
        in_specs=[pl.BlockSpec(memory_space=pltpu.SMEM)] + in_vmem(3),
        out_specs=in_vmem(1)[0],
        out_shape=vmem_out((heads, rows + STATS, width)),
        scratch_shapes=[pltpu.VMEM((heads * rows, blocks * block), F32)],
        name="attend",
    )(core, *held_in_vmem(queries, mine, other))


def merge_kernel(core_ref, part_ref, mine_ref, other_ref, out_ref):
    parts, extended, width = part_ref.shape
    rows = extended - STATS
    levels = []
    for s in range(parts):
        stats = part_ref[s, rows:, :].astype(F32)
        line = stats[:1, :rows] + stats[:1, rows:]
        levels.append(jnp.broadcast_to(line, (rows, rows)).T)
    peak = levels[0]
    for level in levels[1:]:
        peak = jnp.maximum(peak, level)
    shares = [jnp.exp(level - peak) for level in levels]
    total = shares[0]
    for share in shares[1:]:
        total = total + share
    half = mine_ref.shape[0]
    halves = []
    for at in (0, half):
        mixed = None
        for s in range(parts):
            term = part_ref[s, :rows, at : at + half].astype(F32) * shares[s]
            mixed = term if mixed is None else mixed + term
        halves.append((mixed / total).astype(BF16))
    first = core_ref[0] == 0
    mine = jnp.where(first, halves[0], halves[1])
    other = jnp.where(first, halves[1], halves[0])
    projected = dot(mine, mine_ref[...]) + dot(other, other_ref[...])
    out_ref[...] = projected.astype(BF16).reshape(out_ref.shape)


def merge_and_project(core, parts, mine, other, chips):
    rows = parts.shape[1] - STATS
    return pl.pallas_call(
        merge_kernel,
        in_specs=[pl.BlockSpec(memory_space=pltpu.SMEM)] + in_vmem(3),
        out_specs=in_vmem(1)[0],
        out_shape=vmem_out((chips, rows // chips, mine.shape[1])),
        name="merge_and_project",
    )(core, *held_in_vmem(parts, mine, other))


def finish_kernel(part_ref, residual_ref, out_gain_ref, *rest):
    summed = jnp.sum(part_ref[...].astype(F32), axis=0)
    residual = (residual_ref[...].astype(F32) + scaled(summed, out_gain_ref[...])).astype(BF16)
    if len(rest) == 1:
        rest[0][...] = residual
    else:
        rest[1][...] = residual
        rest[2][...] = scaled(residual.astype(F32), rest[0][...]).astype(BF16)


def finish(parts, residual, out_gain, next_gain=None):
    shape = jax.ShapeDtypeStruct(residual.shape, BF16)
    extra = () if next_gain is None else (next_gain,)
    return pl.pallas_call(
        finish_kernel,
        in_specs=in_vmem(3 + len(extra)),
        out_specs=in_vmem(1 + len(extra)),
        out_shape=[shape] * (1 + len(extra)),
        name="finish",
    )(*held_in_vmem(parts, residual, out_gain, *extra))


def exchange(value, axis):
    return lax.all_to_all(value, axis, split_axis=0, concat_axis=0, tiled=True)


def to_all(value, axis, peers):
    return exchange(jnp.broadcast_to(value, (peers, *value.shape)), axis)


def swap(value):
    return lax.ppermute(value, "core", [(0, 1), (1, 0)])


def body(
    target,
    source,
    source_gain,
    query_gain,
    out_gain,
    query_weight,
    key_weight,
    value_weight,
    out_weight,
):
    quarters = lax.axis_size("quarter")
    chips = quarters * lax.axis_size("kv")
    stages = lax.axis_size("sp")
    core = lax.axis_index("core").astype(jnp.int32).reshape(1)
    width = key_weight.shape[2]

    columns = source_columns(source, source_gain[None], key_weight, value_weight, quarters)
    columns = columns.reshape(quarters * 2, LAYERS * width, -1)
    held = exchange(columns, GROUP)
    normed = first_norm(target, query_gain[:1])
    near = []
    for layer in range(LAYERS):
        block = held[:, layer * width : (layer + 1) * width].reshape(HD, -1)
        near.append(lax.all_gather(block, "sp", axis=0))
    far = [swap(part) for part in near]
    query_other = swap(query_weight)
    out_other = swap(out_weight)

    residual = target
    for layer in range(LAYERS):
        rows = to_all(normed, CHIPS, chips)
        mine = project_queries(core, rows, query_weight[layer], query_other[layer])
        queries = to_all(mine, "quarter", quarters)
        parts = attend(core, queries, near[layer], far[layer])
        parts = exchange(parts, "quarter")
        projected = merge_and_project(core, parts, out_weight[layer], out_other[layer], chips)
        arrived = exchange(projected, CHIPS)
        if layer + 1 < LAYERS:
            residual, normed = finish(
                arrived, residual, out_gain[layer : layer + 1], query_gain[layer + 1 : layer + 2]
            )
        else:
            (residual,) = finish(arrived, residual, out_gain[layer : layer + 1])
    return residual


def solution(mesh):
    groups, stages, devices = mesh.devices.shape
    own = Mesh(
        mesh.devices.reshape(groups, stages, KVH, devices // (2 * KVH), 2),
        ("grp", "sp", "kv", "quarter", "core"),
    )
    every = ("grp", "sp", "kv", "quarter", "core")
    tp = ("kv", "quarter", "core")
    in_specs = (
        P(every, None),
        P(("grp", "sp"), None),
        P(),
        P(),
        P(),
        P(None, None, tp),
        P(None, None, tp),
        P(None, None, tp),
        P(None, tp, None),
    )
    return jax.shard_map(body, mesh=own, in_specs=in_specs, out_specs=P(every, None), check_vma=False)
```

time: 384 us -> 269 us (0.70)
  starting transfers between devices: 130 us -> 58.2 us
  waiting for transfers between devices: 118 us -> 76.1 us
  Pallas kernels: 0 us -> 18.7 us
  blocking collectives: 65.7 us -> 81.8 us
  other arithmetic: 15.1 us -> 0 us
  matrix products: 12.4 us -> 0 us
  local copies, waits for them, and re-layouts: 24.4 us -> 16.9 us
    ppermute x27 -> x4, starting transfers between devices: 115 us -> 31 us  [swap(): return lax.ppermute(value, 'core', [(0, 1), (1, 0)])]
    ppermute x27 -> x4, waiting for transfers between devices: 62.2 us -> 0.01 us  [swap(): return lax.ppermute(value, 'core', [(0, 1), (1, 0)])]
    all_gather x1 -> x2, waiting for transfers between devices: 0.02 us -> 47.5 us  [body(): near.append(lax.all_gather(block, 'sp', axis=0))]
    all_to_all x2 -> x6, waiting for transfers between devices: 55.8 us -> 28.5 us  [exchange(): return lax.all_to_all(value, axis, split_axis=0, concat_axis=0, tiled=True)]
    pallas_call x0 -> x10, Pallas kernels: none -> 18.7 us  [the longest x2 8.01 us: attend(): pl.pallas_call(attend_kernel, in_specs=[pl.BlockSpec(memory_space=pltpu.S...]
    all_to_all x2 -> x3, blocking collectives: 65.7 us -> 81.8 us  [exchange(): return lax.all_to_all(value, axis, split_axis=0, concat_axis=0, tiled=True)]
    all_to_all x2 -> x6, starting transfers between devices: 14.7 us -> 27.1 us  [exchange(): return lax.all_to_all(value, axis, split_axis=0, concat_axis=0, tiled=True)]
    dot_general x9 -> x0, matrix products: 12.4 us -> none  [the longest x2 4.15 us: body(): jnp.dot(attended, out_layer, preferred_element_type=jnp.float32)]
  transfers between devices with their start and end apart: 30 -> 12, of which waited for: 15 -> 6; matrix products, arithmetic and copies ran while one was open for 7% -> 4% of each run, Pallas kernels for 0% -> 3%
where the time goes in v1:
time: 269 us; the launch traced here: 265 us
  blocking collectives  81.8 us (30%)
  waiting for transfers between devices  76.1 us (28%)
  starting transfers between devices  58.2 us (22%)
  Pallas kernels  18.7 us (7%)
  local copies, waits for them, and re-layouts  16.9 us (6%)
  between operations  13.7 us (5%)
    all_to_all x3, blocking collectives, exchange(): return lax.all_to_all(value, axis, split_axis=0, concat_axis=0, tiled=True)  81.8 us
    all_gather x2, waiting for transfers between devices, body(): near.append(lax.all_gather(block, 'sp', axis=0))  47.5 us
    ppermute x4, starting transfers between devices, swap(): return lax.ppermute(value, 'core', [(0, 1), (1, 0)])  31 us
    all_to_all x6, waiting for transfers between devices, exchange(): return lax.all_to_all(value, axis, split_axis=0, concat_axis=0, tiled=True)  28.5 us
    all_to_all x6, starting transfers between devices, exchange(): return lax.all_to_all(value, axis, split_axis=0, concat_axis=0, tiled=True)  27.1 us
    pallas_call x2, Pallas kernels, attend(): pl.pallas_call(attend_kernel, in_specs=[pl.BlockSpec(memory_space=pltpu.S...  8.01 us
    pallas_call x1, Pallas kernels, source_columns(): pl.pallas_call(source_kernel, grid=(quarters,), in_specs=[pl.BlockSpec((b...  6.02 us
    unnamed x24, local copies, waits for them, and re-layouts  5.62 us
  transfers between devices with their start and end apart: 12, of which 6 were waited for; matrix products, arithmetic and copies ran while one was open for 4% of the time, Pallas kernels for 3%

profile of v1, /device:TPU:65, one launch (start us, length us, event | category | flops | bytes accessed | tf_op | source)
XLA Modules:
  0.0 265.3 jit_solution(7594705966712183789)
XLA Ops:
  6.6 2.3 copy.12.key_ref
  8.8 2.3 copy.13.value_ref
  11.1 6.0 %source_columns.1 = bf16[4,2,64,128]{3,2,1,0:T(8,128)(2,1)} custom-call(bf16[512,2048]{1,0:T(8,128)(2,1)} %source_ref.1, f32[1,2048]{1,0:T(1,128)} %bitcast.24, bf16[2,2048,32]{2,1,0:T(8,128)(2,1)} %copy.12.key_ref, bf16[2,2048,32]{2,1,0:T(8,128)(2,1)} %copy.13.value_ref), custom_call_target="tpu_custom_call" | custom-call | tf_op jit(solution)/shard_map/source_columns/pallas_call | solution.py:62
  17.1 50.6 %all_to_all.45 = bf16[8,64,128]{2,1,0:T(8,128)(2,1)S(1)} all-to-all(bf16[8,64,128]{2,1,0:T(8,128)(2,1)} %bitcast.21), channel_id=1, replica_groups=mesh['grp'=2,'sp'=16,'kv'=2,'quarter'=4,'core'=2] {'quarter','core'}, dimensions={0} | all-to-all | bytes 262144 | tf_op jit(solution)/shard_map/all_to_all | solution.py:231
  68.4 2.9 %collective-permute-start = (bf16[2,2048,128]{2,1,0:T(8,128)(2,1)S(1)}, bf16[2,2048,128]{2,1,0:T(8,128)(2,1)}, u32[]{:S(2)}, u32[]{:S(2)}) collective-permute-start(bf16[2,2048,128]{2,1,0:T(8,128)(2,1)S(1)} %copy-done.8), channel_id=1, source_target_pairs={{0,1},{1,0},{2,3},{3,2},{4,5},{5,4},{6,7},{7,6},{8,9},{9,8},{10,11... | collective-permute-start | bytes 3145736 | tf_op jit(solution)/shard_map/ppermute | solution.py:239
  72.4 3.7 %all-to-all-start = ((bf16[8,16,2048]{2,1,0:T(8,128)(2,1)}), bf16[8,16,2048]{2,1,0:T(8,128)(2,1)S(1)}, u32[]{:S(2)}, u32[]{:S(2)}) async-start(bf16[8,16,2048]{2,1,0:T(8,128)(2,1)} %broadcast_in_dim.15), calls=%async_computation | async-start | bytes 1048576 | tf_op jit(solution)/shard_map/all_to_all | solution.py:231
  78.1 47.0 %all-gather.3.cloned.1.call-done.mine_ref = bf16[16,256,128]{2,1,0:T(8,128)(2,1)} async-done(((bf16[1,256,128]{2,1,0:T(8,128)(2,1)}), bf16[16,256,128]{2,1,0:T(8,128)(2,1)}) %all-gather.3.cloned.1.call-update) | async-done | bytes 1048592 | tf_op jit(solution)/shard_map/all_gather | solution.py:266
  125.2 12.9 %collective-permute-start.1 = (bf16[16,256,128]{2,1,0:T(8,128)(2,1)}, bf16[16,256,128]{2,1,0:T(8,128)(2,1)}, u32[]{:S(2)}, u32[]{:S(2)}) collective-permute-start(bf16[16,256,128]{2,1,0:T(8,128)(2,1)} %all-gather.3.cloned.1.call-done.mine_ref), channel_id=1, source_target_pairs={{0,1},{1,0},{2,3},{3,2},{4,5},{5,4},{6,7},{7,6},{8,9},{9,8},{10,11... | collective-permute-start | bytes 3145736 | tf_op jit(solution)/shard_map/ppermute | solution.py:239
  141.5 4.3 %all-to-all-start.1 = ((bf16[4,128,256]{2,1,0:T(8,128)(2,1)}), bf16[4,128,256]{2,1,0:T(8,128)(2,1)S(1)}, u32[]{:S(2)}, u32[]{:S(2)}) async-start(bf16[4,128,256]{2,1,0:T(8,128)(2,1)} %broadcast_in_dim.16), calls=%async_computation.1 | async-start | bytes 524288 | tf_op jit(solution)/shard_map/all_to_all | solution.py:231
  145.8 2.3 slice_bitcast_fusion.4
  148.1 5.2 %all-to-all-done.1.query_ref = bf16[4,128,256]{2,1,0:T(8,128)(2,1)S(1)} async-done(((bf16[4,128,256]{2,1,0:T(8,128)(2,1)}), bf16[4,128,256]{2,1,0:T(8,128)(2,1)S(1)}, u32[]{:S(2)}, u32[]{:S(2)}) %all-to-all-start.1) | async-done | bytes 262176 | tf_op jit(solution)/shard_map/all_to_all | solution.py:231
  153.3 4.3 %attend.2 = bf16[4,144,256]{2,1,0:T(8,128)(2,1)} custom-call(s32[1]{0:T(128)} %bitcast.core_ref, bf16[4,128,256]{2,1,0:T(8,128)(2,1)S(1)} %all-to-all-done.1.query_ref, bf16[16,256,128]{2,1,0:T(8,128)(2,1)S(1)} %copy-done.5, bf16[16,256,128]{2,1,0:T(8,128)(2,1)} %collective-permute-done.1.other_ref), custom_call_target="tpu_custom_call" | custom-call | tf_op jit(solution)/shard_map/attend/pallas_call | solution.py:157
  157.6 3.7 %all-to-all-start.3 = ((bf16[4,144,256]{2,1,0:T(8,128)(2,1)}), bf16[4,144,256]{2,1,0:T(8,128)(2,1)S(1)}, u32[]{:S(2)}, u32[]{:S(2)}) async-start(bf16[4,144,256]{2,1,0:T(8,128)(2,1)} %attend.2), calls=%async_computation.3 | async-start | bytes 589824 | tf_op jit(solution)/shard_map/all_to_all | solution.py:231
  161.3 2.1 slice_bitcast_fusion
  163.4 3.7 %all-to-all-done.3.part_ref = bf16[4,144,256]{2,1,0:T(8,128)(2,1)S(1)} async-done(((bf16[4,144,256]{2,1,0:T(8,128)(2,1)}), bf16[4,144,256]{2,1,0:T(8,128)(2,1)S(1)}, u32[]{:S(2)}, u32[]{:S(2)}) %all-to-all-start.3) | async-done | bytes 294944 | tf_op jit(solution)/shard_map/all_to_all | solution.py:231
  168.5 7.4 %all-to-all-start.4 = ((bf16[8,16,2048]{2,1,0:T(8,128)(2,1)}), bf16[8,16,2048]{2,1,0:T(8,128)(2,1)S(1)}, u32[]{:S(2)}, u32[]{:S(2)}) async-start(bf16[8,16,2048]{2,1,0:T(8,128)(2,1)} %merge_and_project.2), calls=%async_computation.4 | async-start | bytes 1048576 | tf_op jit(solution)/shard_map/all_to_all | solution.py:231
  175.9 14.0 %all-to-all-done.4.part_ref = bf16[8,16,2048]{2,1,0:T(8,128)(2,1)S(1)} async-done(((bf16[8,16,2048]{2,1,0:T(8,128)(2,1)}), bf16[8,16,2048]{2,1,0:T(8,128)(2,1)S(1)}, u32[]{:S(2)}, u32[]{:S(2)}) %all-to-all-start.4) | async-done | bytes 524320 | tf_op jit(solution)/shard_map/all_to_all | solution.py:231
  192.5 3.7 %all-to-all-start.5 = ((bf16[8,16,2048]{2,1,0:T(8,128)(2,1)}), bf16[8,16,2048]{2,1,0:T(8,128)(2,1)S(1)}, u32[]{:S(2)}, u32[]{:S(2)}) async-start(bf16[8,16,2048]{2,1,0:T(8,128)(2,1)} %broadcast_in_dim.18), calls=%async_computation.5 | async-start | bytes 1048576 | tf_op jit(solution)/shard_map/all_to_all | solution.py:231
  196.7 13.2 %collective-permute-start.3 = (bf16[16,256,128]{2,1,0:T(8,128)(2,1)}, bf16[16,256,128]{2,1,0:T(8,128)(2,1)}, u32[]{:S(2)}, u32[]{:S(2)}) collective-permute-start(bf16[16,256,128]{2,1,0:T(8,128)(2,1)} %all-gather.5.cloned.1.call-done.mine_ref), channel_id=1, source_target_pairs={{0,1},{1,0},{2,3},{3,2},{4,5},{5,4},{6,7},{7,6},{8,9},{9,8},{10,11... | collective-permute-start | bytes 3145736 | tf_op jit(solution)/shard_map/ppermute | solution.py:239
  211.1 4.4 %all-to-all-start.6 = ((bf16[4,128,256]{2,1,0:T(8,128)(2,1)}), bf16[4,128,256]{2,1,0:T(8,128)(2,1)S(1)}, u32[]{:S(2)}, u32[]{:S(2)}) async-start(bf16[4,128,256]{2,1,0:T(8,128)(2,1)} %broadcast_in_dim.19), calls=%async_computation.6 | async-start | bytes 524288 | tf_op jit(solution)/shard_map/all_to_all | solution.py:231
  215.5 5.6 %all-to-all-done.6.query_ref = bf16[4,128,256]{2,1,0:T(8,128)(2,1)S(1)} async-done(((bf16[4,128,256]{2,1,0:T(8,128)(2,1)}), bf16[4,128,256]{2,1,0:T(8,128)(2,1)S(1)}, u32[]{:S(2)}, u32[]{:S(2)}) %all-to-all-start.6) | async-done | bytes 262176 | tf_op jit(solution)/shard_map/all_to_all | solution.py:231
  221.1 3.7 %attend.3 = bf16[4,144,256]{2,1,0:T(8,128)(2,1)S(1)} custom-call(s32[1]{0:T(128)} %bitcast.core_ref, bf16[4,128,256]{2,1,0:T(8,128)(2,1)S(1)} %all-to-all-done.6.query_ref, bf16[16,256,128]{2,1,0:T(8,128)(2,1)S(1)} %copy-done.4, bf16[16,256,128]{2,1,0:T(8,128)(2,1)} %collective-permute-done.3.other_ref), custom_call_target="tpu_custom_call" | custom-call | tf_op jit(solution)/shard_map/attend/pallas_call | solution.py:157
  224.8 9.7 %all_to_all.46.part_ref = bf16[4,144,256]{2,1,0:T(8,128)(2,1)S(1)} all-to-all(bf16[4,144,256]{2,1,0:T(8,128)(2,1)S(1)} %attend.3), channel_id=1, replica_groups=mesh['grp'=2,'sp'=16,'kv'=2,'quarter'=4,'core'=2] {'quarter'}, dimensions={0} | all-to-all | bytes 589824 | tf_op jit(solution)/shard_map/all_to_all | solution.py:231
  236.2 21.5 %all_to_all.47.part_ref = bf16[8,16,2048]{2,1,0:T(8,128)(2,1)S(1)} all-to-all(bf16[8,16,2048]{2,1,0:T(8,128)(2,1)S(1)} %merge_and_project.3), channel_id=1, replica_groups=mesh['grp'=2,'sp'=16,'kv'=2,'quarter'=4,'core'=2] {'kv','quarter'}, dimensions={0} | all-to-all | bytes 1048576 | tf_op jit(solution)/shard_map/all_to_all | solution.py:231
  (50 shorter events, 15.1 us)
Async XLA Ops:
  6.5 118.6 %all-gather.3.cloned.1.call-start = ((), (), s32[]{:S(2)}) async-start(), calls=%async_computation.9 | async-start | bytes 1114112 | tf_op jit(solution)/shard_map/all_gather | solution.py:266
  11.1 57.4 %copy-start.8 = (bf16[2,2048,128]{2,1,0:T(8,128)(2,1)S(1)}, bf16[2,2048,128]{2,1,0:T(8,128)(2,1)}, u32[]{:S(2)}) copy-start(bf16[2,2048,128]{2,1,0:T(8,128)(2,1)} %param.14) | copy-start | bytes 3145732
  11.1 60.3 %copy-start.9 = (f32[2,2048]{1,0:T(2,128)S(1)}, f32[2,2048]{1,0:T(2,128)}, u32[]{:S(2)}) copy-start(f32[2,2048]{1,0:T(2,128)} %param.12) | copy-start | bytes 49156
  11.1 60.3 %copy-start.6 = (bf16[16,2048]{1,0:T(8,128)(2,1)S(1)}, bf16[16,2048]{1,0:T(8,128)(2,1)}, u32[]{:S(2)}) copy-start(bf16[16,2048]{1,0:T(8,128)(2,1)} %residual_ref.1) | copy-start | bytes 196612
  68.4 69.8 %collective-permute-start = (bf16[2,2048,128]{2,1,0:T(8,128)(2,1)S(1)}, bf16[2,2048,128]{2,1,0:T(8,128)(2,1)}, u32[]{:S(2)}, u32[]{:S(2)}) collective-permute-start(bf16[2,2048,128]{2,1,0:T(8,128)(2,1)S(1)} %copy-done.8), channel_id=1, source_target_pairs={{0,1},{1,0},{2,3},{3,2},{4,5},{5,4},{6,7},{7,6},{8,9},{9,8},{10,11... | collective-permute-start | bytes 3145736 | tf_op jit(solution)/shard_map/ppermute | solution.py:239
  72.4 67.9 %all-to-all-start = ((bf16[8,16,2048]{2,1,0:T(8,128)(2,1)}), bf16[8,16,2048]{2,1,0:T(8,128)(2,1)S(1)}, u32[]{:S(2)}, u32[]{:S(2)}) async-start(bf16[8,16,2048]{2,1,0:T(8,128)(2,1)} %broadcast_in_dim.15), calls=%async_computation | async-start | bytes 1048576 | tf_op jit(solution)/shard_map/all_to_all | solution.py:231
  76.1 120.6 %all-gather.5.cloned.1.call-start = ((), (), s32[]{:S(2)}) async-start(), calls=%async_computation.10 | async-start | bytes 1114112 | tf_op jit(solution)/shard_map/all_gather | solution.py:266
  76.2 85.1 %collective-permute-start.2 = (bf16[2,128,2048]{2,1,0:T(8,128)(2,1)}, bf16[2,128,2048]{2,1,0:T(8,128)(2,1)}, u32[]{:S(2)}, u32[]{:S(2)}) collective-permute-start(bf16[2,128,2048]{2,1,0:T(8,128)(2,1)} %param.17), channel_id=1, source_target_pairs={{0,1},{1,0},{2,3},{3,2},{4,5},{5,4},{6,7},{7,6},{8,9},{9,8},{10,11... | collective-permute-start | bytes 3145736 | tf_op jit(solution)/shard_map/ppermute | solution.py:239
  125.2 28.1 %collective-permute-start.1 = (bf16[16,256,128]{2,1,0:T(8,128)(2,1)}, bf16[16,256,128]{2,1,0:T(8,128)(2,1)}, u32[]{:S(2)}, u32[]{:S(2)}) collective-permute-start(bf16[16,256,128]{2,1,0:T(8,128)(2,1)} %all-gather.3.cloned.1.call-done.mine_ref), channel_id=1, source_target_pairs={{0,1},{1,0},{2,3},{3,2},{4,5},{5,4},{6,7},{7,6},{8,9},{9,8},{10,11... | collective-permute-start | bytes 3145736 | tf_op jit(solution)/shard_map/ppermute | solution.py:239
  140.8 12.5 %copy-start.5 = (bf16[16,256,128]{2,1,0:T(8,128)(2,1)S(1)}, bf16[16,256,128]{2,1,0:T(8,128)(2,1)}, u32[]{:S(2)}) copy-start(bf16[16,256,128]{2,1,0:T(8,128)(2,1)} %all-gather.3.cloned.1.call-done.mine_ref) | copy-start | bytes 3145732
  141.5 11.8 %all-to-all-start.1 = ((bf16[4,128,256]{2,1,0:T(8,128)(2,1)}), bf16[4,128,256]{2,1,0:T(8,128)(2,1)S(1)}, u32[]{:S(2)}, u32[]{:S(2)}) async-start(bf16[4,128,256]{2,1,0:T(8,128)(2,1)} %broadcast_in_dim.16), calls=%async_computation.1 | async-start | bytes 524288 | tf_op jit(solution)/shard_map/all_to_all | solution.py:231
  157.6 9.5 %copy-start.3 = (bf16[128,2048]{1,0:T(8,128)(2,1)S(1)}, bf16[128,2048]{1,0:T(8,128)(2,1)}, u32[]{:S(2)}) copy-start(bf16[128,2048]{1,0:T(8,128)(2,1)} %get-tuple-element.12.mine_ref) | copy-start | bytes 1572868
  157.6 9.5 %all-to-all-start.3 = ((bf16[4,144,256]{2,1,0:T(8,128)(2,1)}), bf16[4,144,256]{2,1,0:T(8,128)(2,1)S(1)}, u32[]{:S(2)}, u32[]{:S(2)}) async-start(bf16[4,144,256]{2,1,0:T(8,128)(2,1)} %attend.2), calls=%async_computation.3 | async-start | bytes 589824 | tf_op jit(solution)/shard_map/all_to_all | solution.py:231
  161.3 14.6 %copy-start.10 = (f32[2,2048]{1,0:T(2,128)S(1)}, f32[2,2048]{1,0:T(2,128)}, u32[]{:S(2)}) copy-start(f32[2,2048]{1,0:T(2,128)} %param.13) | copy-start | bytes 49156
  168.5 41.4 %copy-start = (bf16[2048,128]{1,0:T(8,128)(2,1)S(1)}, bf16[2048,128]{1,0:T(8,128)(2,1)}, u32[]{:S(2)}) copy-start(bf16[2048,128]{1,0:T(8,128)(2,1)} %get-tuple-element.13.other_ref) | copy-start | bytes 1572868
  168.5 21.4 %all-to-all-start.4 = ((bf16[8,16,2048]{2,1,0:T(8,128)(2,1)}), bf16[8,16,2048]{2,1,0:T(8,128)(2,1)S(1)}, u32[]{:S(2)}, u32[]{:S(2)}) async-start(bf16[8,16,2048]{2,1,0:T(8,128)(2,1)} %merge_and_project.2), calls=%async_computation.4 | async-start | bytes 1048576 | tf_op jit(solution)/shard_map/all_to_all | solution.py:231
  192.5 17.4 %all-to-all-start.5 = ((bf16[8,16,2048]{2,1,0:T(8,128)(2,1)}), bf16[8,16,2048]{2,1,0:T(8,128)(2,1)S(1)}, u32[]{:S(2)}, u32[]{:S(2)}) async-start(bf16[8,16,2048]{2,1,0:T(8,128)(2,1)} %broadcast_in_dim.18), calls=%async_computation.5 | async-start | bytes 1048576 | tf_op jit(solution)/shard_map/all_to_all | solution.py:231
  196.7 24.4 %copy-start.4 = (bf16[16,256,128]{2,1,0:T(8,128)(2,1)S(1)}, bf16[16,256,128]{2,1,0:T(8,128)(2,1)}, u32[]{:S(2)}) copy-start(bf16[16,256,128]{2,1,0:T(8,128)(2,1)} %all-gather.5.cloned.1.call-done.mine_ref) | copy-start | bytes 3145732
  196.7 18.8 %collective-permute-start.3 = (bf16[16,256,128]{2,1,0:T(8,128)(2,1)}, bf16[16,256,128]{2,1,0:T(8,128)(2,1)}, u32[]{:S(2)}, u32[]{:S(2)}) collective-permute-start(bf16[16,256,128]{2,1,0:T(8,128)(2,1)} %all-gather.5.cloned.1.call-done.mine_ref), channel_id=1, source_target_pairs={{0,1},{1,0},{2,3},{3,2},{4,5},{5,4},{6,7},{7,6},{8,9},{9,8},{10,11... | collective-permute-start | bytes 3145736 | tf_op jit(solution)/shard_map/ppermute | solution.py:239
  210.3 24.2 %copy-start.1 = (bf16[128,2048]{1,0:T(8,128)(2,1)S(1)}, bf16[128,2048]{1,0:T(8,128)(2,1)}, u32[]{:S(2)}) copy-start(bf16[128,2048]{1,0:T(8,128)(2,1)} %get-tuple-element.11.mine_ref) | copy-start | bytes 1572868
  211.1 10.0 %all-to-all-start.6 = ((bf16[4,128,256]{2,1,0:T(8,128)(2,1)}), bf16[4,128,256]{2,1,0:T(8,128)(2,1)S(1)}, u32[]{:S(2)}, u32[]{:S(2)}) async-start(bf16[4,128,256]{2,1,0:T(8,128)(2,1)} %broadcast_in_dim.19), calls=%async_computation.6 | async-start | bytes 524288 | tf_op jit(solution)/shard_map/all_to_all | solution.py:231
  224.8 32.8 %copy-start.7 = (bf16[16,2048]{1,0:T(8,128)(2,1)S(1)}, bf16[16,2048]{1,0:T(8,128)(2,1)}, u32[]{:S(2)}) copy-start(bf16[16,2048]{1,0:T(8,128)(2,1)} %get-tuple-element.8.residual_ref) | copy-start | bytes 196612
  234.5 1.0 copy-start.2
Sparse Core Ops, SparseCore 0:
  68.6 56.5 all-gather.2
  138.4 58.2 all-gather.4

commit v2 on v1

v2 whole, which is shorter than its diff:
```python
import functools

import jax
import jax.numpy as jnp
from jax import lax
from jax.experimental import pallas as pl
from jax.experimental.pallas import tpu as pltpu
from jax.sharding import Mesh
from jax.sharding import PartitionSpec as P


HD = 256
KVH = 2
LAYERS = 2
EPSILON = 1e-06
STATS = 16

CHIPS = ("kv", "quarter")
GROUP = ("quarter", "core")
COPIES = (4, 0)
BF16 = jnp.bfloat16
F32 = jnp.float32


def dot(a, b, contract=((1,), (0,))):
    return lax.dot_general(a, b, (contract, ((), ())), preferred_element_type=F32)


def scaled(values, gain):
    inverse = lax.rsqrt(jnp.mean(values * values, axis=-1, keepdims=True) + EPSILON)
    return values * inverse * gain


def held_in_vmem(*arrays):
    return [pltpu.with_memory_space_constraint(a, pltpu.VMEM) for a in arrays]


def vmem_out(shape):
    return pltpu.VMEM(tuple(shape), BF16)


def in_vmem(count):
    return [pl.BlockSpec(memory_space=pltpu.VMEM)] * count


def source_kernel(source_ref, gain_ref, key_ref, value_ref, out_ref, weight_ref):
    width = key_ref.shape[1]

    @pl.when(pl.program_id(0) == 0)
    def _():
        for layer in range(LAYERS):
            weight_ref[layer * width : (layer + 1) * width, :] = key_ref[layer]
            weight_ref[(LAYERS + layer) * width : (LAYERS + layer + 1) * width, :] = value_ref[layer]

    normed = scaled(source_ref[...].astype(F32), gain_ref[...]).astype(BF16)
    columns = dot(weight_ref[...], normed, ((1,), (1,))).astype(BF16)
    out_ref[...] = columns.reshape(out_ref.shape)


def source_columns(source, gain, key_weight, value_weight, quarters):
    rows, features = source.shape
    key_weight = jnp.swapaxes(key_weight, 1, 2)
    value_weight = jnp.swapaxes(value_weight, 1, 2)
    width = key_weight.shape[1]
    block = rows // quarters
    return pl.pallas_call(
        source_kernel,
        grid=(quarters,),
        in_specs=[
            pl.BlockSpec((block, features), lambda i: (i, 0)),
            pl.BlockSpec((1, features), lambda i: (0, 0)),
            pl.BlockSpec(key_weight.shape, lambda i: (0, 0, 0)),
            pl.BlockSpec(value_weight.shape, lambda i: (0, 0, 0)),
        ],
        out_specs=pl.BlockSpec((1, 2, LAYERS * width, block), lambda i: (i, 0, 0, 0)),
        out_shape=jax.ShapeDtypeStruct((quarters, 2, LAYERS * width, block), BF16),
        scratch_shapes=[pltpu.VMEM((2 * LAYERS * width, features), BF16)],
        compiler_params=pltpu.CompilerParams(vmem_limit_bytes=12288 * 1024),
        name="source_columns",
    )(*[pltpu.with_memory_space_constraint(a, pltpu.HBM) for a in (source, gain, key_weight, value_weight)])


def norm_kernel(rows_ref, gain_ref, out_ref):
    normed = scaled(rows_ref[...].astype(F32), gain_ref[:1, :]).astype(BF16)
    for peer in range(out_ref.shape[0]):
        out_ref[peer] = normed


def first_norm(rows, gain, chips):
    return pl.pallas_call(
        norm_kernel,
        in_specs=in_vmem(2),
        out_specs=in_vmem(1)[0],
        out_shape=vmem_out((chips, *rows.shape)),
        compiler_params=pltpu.CompilerParams(vmem_limit_bytes=4096 * 1024),
        name="first_norm",
    )(*held_in_vmem(rows, gain))


def query_kernel(layer, core_ref, rows_ref, mine_ref, other_ref, out_ref):
    chips, block, features = rows_ref.shape
    rows = rows_ref[...].reshape(chips * block, features)
    mine = dot(rows, mine_ref[layer]).astype(BF16)
    other = dot(rows, other_ref[layer]).astype(BF16)
    first = core_ref[0] == 0
    width = mine.shape[1]
    low = jnp.where(first, mine, other)
    high = jnp.where(first, other, mine)
    for peer in range(out_ref.shape[0]):
        out_ref[peer, :, :width] = low
        out_ref[peer, :, width:] = high


def project_queries(layer, core, rows, mine, other, copies):
    chips, block, _ = rows.shape
    return pl.pallas_call(
        functools.partial(query_kernel, layer),
        in_specs=[pl.BlockSpec(memory_space=pltpu.SMEM)] + in_vmem(3),
        out_specs=in_vmem(1)[0],
        out_shape=vmem_out((copies, chips * block, 2 * mine.shape[2])),
        compiler_params=pltpu.CompilerParams(vmem_limit_bytes=8192 * 1024),
        name="project_queries",
    )(core, *held_in_vmem(rows, mine, other))


def attend_kernel(pieces, core_ref, query_ref, *refs):
    mine_refs, other_refs = refs[:pieces], refs[pieces : 2 * pieces]
    out_ref, score_ref = refs[2 * pieces :]
    heads, rows, width = query_ref.shape
    queries = query_ref[...].reshape(heads * rows, width)
    scale = width ** (-0.5)

    def pairs(piece_refs):
        for ref in piece_refs:
            for b in range(0, ref.shape[0], 2):
                yield jnp.concatenate([ref[b], ref[b + 1]], axis=1)

    def work(key_refs, value_refs):
        peak, at, spans = None, 0, []
        for keys in pairs(key_refs):
            scores = dot(queries, keys) * scale
            spans.append(slice(at, at + keys.shape[1]))
            score_ref[:, spans[-1]] = scores
            at += keys.shape[1]
            top = jnp.max(scores, axis=1, keepdims=True)
            peak = top if peak is None else jnp.maximum(peak, top)
        total, mixed = None, None
        for span, values in zip(spans, pairs(value_refs)):
            weights = jnp.exp(score_ref[:, span] - peak)
            part = jnp.sum(weights, axis=1, keepdims=True)
            share = dot(weights.astype(BF16), values, ((1,), (1,)))
            total = part if total is None else total + part
            mixed = share if mixed is None else mixed + share
        out_ref[:, :rows, :] = (mixed / total).astype(BF16).reshape(heads, rows, width)
        level = peak + jnp.log(total)
        high = level.astype(BF16).astype(F32)
        low = level - high
        for h in range(heads):
            for part, at in ((high, 0), (low, rows)):
                column = jnp.broadcast_to(part[h * rows : (h + 1) * rows], (rows, rows))
                out_ref[h, rows:, at : at + rows] = column.T[:STATS].astype(BF16)

    @pl.when(core_ref[0] == 0)
    def _():
        work(mine_refs, other_refs)

    @pl.when(core_ref[0] != 0)
    def _():
        work(other_refs, mine_refs)


def attend(core, queries, mine, other):
    heads, rows, width = queries.shape
    span = sum(piece.shape[0] * piece.shape[2] for piece in mine)
    return pl.pallas_call(
        functools.partial(attend_kernel, len(mine)),
        in_specs=[pl.BlockSpec(memory_space=pltpu.SMEM)] + in_vmem(1 + 2 * len(mine)),
        out_specs=in_vmem(1)[0],
        out_shape=vmem_out((heads, rows + STATS, width)),
        scratch_shapes=[pltpu.VMEM((heads * rows, span), F32)],
        compiler_params=pltpu.CompilerParams(vmem_limit_bytes=20480 * 1024),
        name="attend",
    )(core, *held_in_vmem(queries, *mine, *other))


def join_kernel(*refs):
    at = 0
    for ref in refs[:-1]:
        refs[-1][at : at + ref.shape[0]] = ref[...]
        at += ref.shape[0]


def join(*pieces):
    count = sum(piece.shape[0] for piece in pieces)
    return pl.pallas_call(
        join_kernel,
        in_specs=in_vmem(len(pieces)),
        out_specs=in_vmem(1)[0],
        out_shape=vmem_out((count, *pieces[0].shape[1:])),
        compiler_params=pltpu.CompilerParams(vmem_limit_bytes=4096 * 1024),
        name="join",
    )(*held_in_vmem(*pieces))


def merge_kernel(layer, core_ref, part_ref, mine_ref, other_ref, out_ref):
    parts, extended, _ = part_ref.shape
    rows = extended - STATS
    levels = []
    for s in range(parts):
        stats = part_ref[s, rows:, :].astype(F32)
        line = stats[:1, :rows] + stats[:1, rows:]
        levels.append(jnp.broadcast_to(line, (rows, rows)).T)
    peak = levels[0]
    for level in levels[1:]:
        peak = jnp.maximum(peak, level)
    shares = [jnp.exp(level - peak) for level in levels]
    total = shares[0]
    for share in shares[1:]:
        total = total + share
    half = mine_ref.shape[1]
    halves = []
    for at in (0, half):
        mixed = None
        for s in range(parts):
            term = part_ref[s, :rows, at : at + half].astype(F32) * shares[s]
            mixed = term if mixed is None else mixed + term
        halves.append((mixed / total).astype(BF16))
    first = core_ref[0] == 0
    mine = jnp.where(first, halves[0], halves[1])
    other = jnp.where(first, halves[1], halves[0])
    projected = dot(mine, mine_ref[layer]) + dot(other, other_ref[layer])
    out_ref[...] = projected.astype(BF16).reshape(out_ref.shape)


def merge_and_project(layer, core, parts, mine, other, chips):
    rows = parts.shape[1] - STATS
    return pl.pallas_call(
        functools.partial(merge_kernel, layer),
        in_specs=[pl.BlockSpec(memory_space=pltpu.SMEM)] + in_vmem(3),
        out_specs=in_vmem(1)[0],
        out_shape=vmem_out((chips, rows // chips, mine.shape[2])),
        compiler_params=pltpu.CompilerParams(vmem_limit_bytes=8192 * 1024),
        name="merge_and_project",
    )(core, *held_in_vmem(parts, mine, other))


def finish_kernel(layer, part_ref, residual_ref, out_gain_ref, query_gain_ref, *out_refs):
    summed = jnp.sum(part_ref[...].astype(F32), axis=0)
    change = scaled(summed, out_gain_ref[layer : layer + 1, :])
    residual = (residual_ref[...].astype(F32) + change).astype(BF16)
    out_refs[0][...] = residual
    if layer + 1 < LAYERS:
        normed = scaled(residual.astype(F32), query_gain_ref[layer + 1 : layer + 2, :]).astype(BF16)
        for peer in range(out_refs[1].shape[0]):
            out_refs[1][peer] = normed


def finish(layer, parts, residual, out_gain, query_gain):
    shapes = [residual.shape]
    if layer + 1 < LAYERS:
        shapes.append(parts.shape)
    return pl.pallas_call(
        functools.partial(finish_kernel, layer),
        in_specs=in_vmem(4),
        out_specs=in_vmem(len(shapes)),
        out_shape=[vmem_out(shape) for shape in shapes],
        compiler_params=pltpu.CompilerParams(vmem_limit_bytes=4096 * 1024),
        name="finish",
    )(*held_in_vmem(parts, residual, out_gain, query_gain))


def exchange(value, axis):
    return lax.all_to_all(value, axis, split_axis=0, concat_axis=0, tiled=True)


def shifted(value, distance, size):
    return lax.ppermute(value, "sp", [(z, (z + distance) % size) for z in range(size)])


def swap(value):
    return lax.ppermute(value, "core", [(0, 1), (1, 0)])


def after(value, *others):
    return lax.optimization_barrier((value, *others))[0]


def stride_step(block, stride, size):
    sent = [shifted(block, distance, size) for distance in (stride, -stride, 2 * stride)]
    return sent[0], block, sent[1], sent[2]


def near_step(own, size):
    return (
        shifted(own, 1, size),
        shifted(own, -1, size),
        shifted(own[:2], 2, size),
        shifted(own[1:3], -2, size),
    )


def layers(
    target,
    source,
    source_gain,
    query_gain,
    out_gain,
    query_weight,
    key_weight,
    value_weight,
    out_weight,
):
    quarters = lax.axis_size("quarter")
    chips = quarters * lax.axis_size("kv")
    stages = lax.axis_size("sp")
    core = lax.axis_index("core").astype(jnp.int32).reshape(1)
    width = key_weight.shape[2]

    columns = source_columns(source, source_gain[None], key_weight, value_weight, quarters)
    columns = columns.reshape(quarters * 2, LAYERS * width, -1)
    held = exchange(columns, GROUP)
    blocks = [
        held[:, layer * width : (layer + 1) * width].reshape(1, HD, -1) for layer in range(LAYERS)
    ]
    near, far = [], []
    pieces = stride_step(blocks[0], stages // 4, stages)
    own = join(*pieces)
    pieces = near_step(own, stages)
    far_own = swap(own)
    rest = join(*pieces)
    far_rest = swap(rest)
    near.append((own, rest))
    far.append((far_own, far_rest))
    normed = after(first_norm(target, query_gain, chips), held)
    query_other = swap(query_weight)
    out_other = swap(out_weight)

    residual = target
    for layer in range(LAYERS):
        rows = exchange(normed, CHIPS)
        mine = project_queries(layer, core, rows, query_weight, query_other, COPIES[layer] or 1)
        if layer == 0:
            pieces = stride_step(after(blocks[1], mine), stages // 4, stages)
        if COPIES[layer]:
            queries = exchange(mine, "quarter")
        else:
            queries = lax.all_gather(mine[0], "quarter", axis=0)
        parts = attend(core, queries, near[layer], far[layer])
        if layer == 0:
            own = join(*after(pieces, parts))
            pieces = near_step(own, stages)
        parts = exchange(parts, "quarter")
        projected = merge_and_project(layer, core, parts, out_weight, out_other, chips)
        arrived = exchange(projected, CHIPS)
        if layer == 0:
            whole = join(own, *after(pieces, projected))
            far.append((swap(whole),))
            near.append((whole,))
        done = finish(layer, arrived, residual, out_gain, query_gain)
        residual = done[0]
        normed = done[-1]
    return residual


def solution(mesh):
    groups, stages, devices = mesh.devices.shape
    own = Mesh(
        mesh.devices.reshape(groups, stages, KVH, devices // (2 * KVH), 2),
        ("grp", "sp", "kv", "quarter", "core"),
    )
    every = ("grp", "sp", "kv", "quarter", "core")
    tp = ("kv", "quarter", "core")
    in_specs = (
        P(every, None),
        P(("grp", "sp"), None),
        P(),
        P(),
        P(),
        P(None, None, tp),
        P(None, None, tp),
        P(None, None, tp),
        P(None, tp, None),
    )
    return jax.shard_map(layers, mesh=own, in_specs=in_specs, out_specs=P(every, None), check_vma=False)
```

time: 269 us -> 277 us (1.030)
  the two profiles are of different devices: /device:TPU:65 before, /device:TPU:80 now
where the time goes in v2:
time: 277 us; the launch traced here: 275 us
  starting transfers between devices  139 us (50%)
  blocking collectives  65.7 us (24%)
  waiting for transfers between devices  42.7 us (15%)
  Pallas kernels  21.5 us (8%)
  local copies, waits for them, and re-layouts  6.06 us (2%)
    ppermute x14, starting transfers between devices, shifted(): lax.ppermute(value, 'sp', [(z, (z + distance) % size) for z in range(size)])  102 us
    all_to_all x3, blocking collectives, exchange(): return lax.all_to_all(value, axis, split_axis=0, concat_axis=0, tiled=True)  51.3 us
    all_to_all x5, starting transfers between devices, exchange(): return lax.all_to_all(value, axis, split_axis=0, concat_axis=0, tiled=True)  26.4 us
    ppermute x14, waiting for transfers between devices, shifted(): lax.ppermute(value, 'sp', [(z, (z + distance) % size) for z in range(size)])  24.7 us
    all_to_all x5, waiting for transfers between devices, exchange(): return lax.all_to_all(value, axis, split_axis=0, concat_axis=0, tiled=True)  16.5 us
    all_gather x1, blocking collectives, layers(): queries = lax.all_gather(mine[0], 'quarter', axis=0)  14.4 us
    ppermute x5, starting transfers between devices, swap(): return lax.ppermute(value, 'core', [(0, 1), (1, 0)])  10.7 us
    pallas_call x2, Pallas kernels, attend(): pl.pallas_call(functools.partial(attend_kernel, len(mine)), in_specs=[pl....  7.81 us
  transfers between devices with their start and end apart: 24, of which 10 were waited for; matrix products, arithmetic and copies ran while one was open for 0% of the time, Pallas kernels for 4%

profile of v2, /device:TPU:80, one launch (start us, length us, event | category | flops | bytes accessed | tf_op | source)
XLA Modules:
  0.0 275.2 jit_solution(14749252555118228626)
XLA Ops:
  0.0 4.6 %source_columns.1 = bf16[4,2,64,128]{3,2,1,0:T(8,128)(2,1)} custom-call(bf16[512,2048]{1,0:T(8,128)(2,1)} %source_ref.1, f32[1,2048]{1,0:T(1,128)} %bitcast.17, bf16[2,32,2048]{2,1,0:T(8,128)(2,1)} %bitcast.15, bf16[2,32,2048]{2,1,0:T(8,128)(2,1)} %bitcast.16), custom_call_target="tpu_custom_call" | custom-call | tf_op jit(solution)/shard_map/source_columns/pallas_call | solution.py:66
  4.6 5.0 %all-to-all-start = ((bf16[8,64,128]{2,1,0:T(8,128)(2,1)}), bf16[8,64,128]{2,1,0:T(8,128)(2,1)S(1)}, u32[]{:S(2)}, u32[]{:S(2)}) async-start(bf16[8,64,128]{2,1,0:T(8,128)(2,1)} %bitcast.4), calls=%async_computation | async-start | bytes 262144 | tf_op jit(solution)/shard_map/all_to_all | solution.py:273
  16.4 5.7 %all-to-all-start.1 = ((bf16[8,16,2048]{2,1,0:T(8,128)(2,1)}), bf16[8,16,2048]{2,1,0:T(8,128)(2,1)}, u32[]{:S(2)}, u32[]{:S(2)}) async-start(bf16[8,16,2048]{2,1,0:T(8,128)(2,1)} %first_norm.1), calls=%async_computation.1 | async-start | bytes 1048576 | tf_op jit(solution)/shard_map/all_to_all | solution.py:273
  22.7 17.8 %collective-permute-start.1 = (bf16[1,256,128]{2,1,0:T(8,128)(2,1)S(1)}, bf16[1,256,128]{2,1,0:T(8,128)(2,1)S(1)}, u32[]{:S(2)}, u32[]{:S(2)}) collective-permute-start(bf16[1,256,128]{2,1,0:T(8,128)(2,1)S(1)} %bitcast.11), channel_id=1, source_target_pairs={{0,64},{16,80},{32,96},{48,112},{64,128},{80,144},{96,160},{112,17... | collective-permute-start | bytes 196616 | tf_op jit(solution)/shard_map/ppermute | solution.py:277
  40.5 23.0 %collective-permute-start.2 = (bf16[1,256,128]{2,1,0:T(8,128)(2,1)S(1)}, bf16[1,256,128]{2,1,0:T(8,128)(2,1)S(1)}, u32[]{:S(2)}, u32[]{:S(2)}) collective-permute-start(bf16[1,256,128]{2,1,0:T(8,128)(2,1)S(1)} %bitcast.12), channel_id=1, source_target_pairs={{0,192},{16,208},{32,224},{48,240},{64,0},{80,16},{96,32},{112,48}... | collective-permute-start | bytes 196616 | tf_op jit(solution)/shard_map/ppermute | solution.py:277
  63.5 7.3 %collective-permute-start.3 = (bf16[1,256,128]{2,1,0:T(8,128)(2,1)S(1)}, bf16[1,256,128]{2,1,0:T(8,128)(2,1)S(1)}, u32[]{:S(2)}, u32[]{:S(2)}) collective-permute-start(bf16[1,256,128]{2,1,0:T(8,128)(2,1)S(1)} %bitcast.13), channel_id=1, source_target_pairs={{0,128},{16,144},{32,160},{48,176},{64,192},{80,208},{96,224},{112... | collective-permute-start | bytes 196616 | tf_op jit(solution)/shard_map/ppermute | solution.py:277
  70.8 7.6 %collective-permute-done.3.refs_3_ = bf16[1,256,128]{2,1,0:T(8,128)(2,1)S(1)} collective-permute-done((bf16[1,256,128]{2,1,0:T(8,128)(2,1)S(1)}, bf16[1,256,128]{2,1,0:T(8,128)(2,1)S(1)}, u32[]{:S(2)}, u32[]{:S(2)}) %collective-permute-start.3) | collective-permute-done | bytes 65568 | tf_op jit(solution)/shard_map/ppermute | solution.py:277
  78.4 6.0 %collective-permute-start.4 = (bf16[4,256,128]{2,1,0:T(8,128)(2,1)S(1)}, bf16[4,256,128]{2,1,0:T(8,128)(2,1)S(1)}, u32[]{:S(2)}, u32[]{:S(2)}) collective-permute-start(bf16[4,256,128]{2,1,0:T(8,128)(2,1)S(1)} %join.4.refs_0_), channel_id=1, source_target_pairs={{0,16},{16,32},{32,48},{48,64},{64,80},{80,96},{96,112},{112,128},... | collective-permute-start | bytes 786440 | tf_op jit(solution)/shard_map/ppermute | solution.py:277
  84.4 9.1 %collective-permute-start.5 = (bf16[4,256,128]{2,1,0:T(8,128)(2,1)S(1)}, bf16[4,256,128]{2,1,0:T(8,128)(2,1)S(1)}, u32[]{:S(2)}, u32[]{:S(2)}) collective-permute-start(bf16[4,256,128]{2,1,0:T(8,128)(2,1)S(1)} %join.4.refs_0_), channel_id=1, source_target_pairs={{0,240},{16,0},{32,16},{48,32},{64,48},{80,64},{96,80},{112,96},{1... | collective-permute-start | bytes 786440 | tf_op jit(solution)/shard_map/ppermute | solution.py:277
  95.5 6.1 %collective-permute-start.7 = (bf16[2,256,128]{2,1,0:T(8,128)(2,1)S(1)}, bf16[2,256,128]{2,1,0:T(8,128)(2,1)S(1)}, u32[]{:S(2)}, u32[]{:S(2)}) collective-permute-start(bf16[2,256,128]{2,1,0:T(8,128)(2,1)S(1)} %get-tuple-element.31), channel_id=1, source_target_pairs={{0,224},{16,240},{32,0},{48,16},{64,32},{80,48},{96,64},{112,80},{... | collective-permute-start | bytes 393224 | tf_op jit(solution)/shard_map/ppermute | solution.py:277
  112.8 5.7 %all-to-all-start.2 = ((bf16[4,128,256]{2,1,0:T(8,128)(2,1)}), bf16[4,128,256]{2,1,0:T(8,128)(2,1)}, u32[]{:S(2)}, u32[]{:S(2)}) async-start(bf16[4,128,256]{2,1,0:T(8,128)(2,1)} %copy-done.4), calls=%async_computation.2 | async-start | bytes 524288 | tf_op jit(solution)/shard_map/all_to_all | solution.py:273
  122.6 5.0 %all-to-all-done.2.query_ref = bf16[4,128,256]{2,1,0:T(8,128)(2,1)} async-done(((bf16[4,128,256]{2,1,0:T(8,128)(2,1)}), bf16[4,128,256]{2,1,0:T(8,128)(2,1)}, u32[]{:S(2)}, u32[]{:S(2)}) %all-to-all-start.2) | async-done | bytes 262176 | tf_op jit(solution)/shard_map/all_to_all | solution.py:273
  136.7 8.2 %all-to-all-done.3.part_ref = bf16[4,144,256]{2,1,0:T(8,128)(2,1)S(1)} async-done(((bf16[4,144,256]{2,1,0:T(8,128)(2,1)}), bf16[4,144,256]{2,1,0:T(8,128)(2,1)S(1)}, u32[]{:S(2)}, u32[]{:S(2)}) %all-to-all-start.3) | async-done | bytes 294944 | tf_op jit(solution)/shard_map/all_to_all | solution.py:273
  146.2 6.5 %all-to-all-start.4 = ((bf16[8,16,2048]{2,1,0:T(8,128)(2,1)}), bf16[8,16,2048]{2,1,0:T(8,128)(2,1)}, u32[]{:S(2)}, u32[]{:S(2)}) async-start(bf16[8,16,2048]{2,1,0:T(8,128)(2,1)} %copy-done.2), calls=%async_computation.4 | async-start | bytes 1048576 | tf_op jit(solution)/shard_map/all_to_all | solution.py:273
  155.1 7.4 %collective-permute-start.12 = (bf16[1,256,128]{2,1,0:T(8,128)(2,1)}, bf16[1,256,128]{2,1,0:T(8,128)(2,1)S(1)}, u32[]{:S(2)}, u32[]{:S(2)}) collective-permute-start(bf16[1,256,128]{2,1,0:T(8,128)(2,1)} %bitcast.8), channel_id=1, source_target_pairs={{0,192},{16,208},{32,224},{48,240},{64,0},{80,16},{96,32},{112,48}... | collective-permute-start | bytes 196616 | tf_op jit(solution)/shard_map/ppermute | solution.py:277
  162.5 4.4 %collective-permute-start.13 = (bf16[1,256,128]{2,1,0:T(8,128)(2,1)}, bf16[1,256,128]{2,1,0:T(8,128)(2,1)S(1)}, u32[]{:S(2)}, u32[]{:S(2)}) collective-permute-start(bf16[1,256,128]{2,1,0:T(8,128)(2,1)} %bitcast.9), channel_id=1, source_target_pairs={{0,128},{16,144},{32,160},{48,176},{64,192},{80,208},{96,224},{112... | collective-permute-start | bytes 196616 | tf_op jit(solution)/shard_map/ppermute | solution.py:277
  166.9 10.7 %collective-permute-done.13.refs_3_ = bf16[1,256,128]{2,1,0:T(8,128)(2,1)S(1)} collective-permute-done((bf16[1,256,128]{2,1,0:T(8,128)(2,1)}, bf16[1,256,128]{2,1,0:T(8,128)(2,1)S(1)}, u32[]{:S(2)}, u32[]{:S(2)}) %collective-permute-start.13) | collective-permute-done | bytes 65568 | tf_op jit(solution)/shard_map/ppermute | solution.py:277
  180.6 6.1 %collective-permute-start.15 = (bf16[4,256,128]{2,1,0:T(8,128)(2,1)S(1)}, bf16[4,256,128]{2,1,0:T(8,128)(2,1)S(1)}, u32[]{:S(2)}, u32[]{:S(2)}) collective-permute-start(bf16[4,256,128]{2,1,0:T(8,128)(2,1)S(1)} %join.6.refs_0_), channel_id=1, source_target_pairs={{0,240},{16,0},{32,16},{48,32},{64,48},{80,64},{96,80},{112,96},{1... | collective-permute-start | bytes 786440 | tf_op jit(solution)/shard_map/ppermute | solution.py:277
  188.7 6.1 %collective-permute-start.17 = (bf16[2,256,128]{2,1,0:T(8,128)(2,1)S(1)}, bf16[2,256,128]{2,1,0:T(8,128)(2,1)S(1)}, u32[]{:S(2)}, u32[]{:S(2)}) collective-permute-start(bf16[2,256,128]{2,1,0:T(8,128)(2,1)S(1)} %get-tuple-element.29), channel_id=1, source_target_pairs={{0,224},{16,240},{32,0},{48,16},{64,32},{80,48},{96,64},{112,80},{... | collective-permute-start | bytes 393224 | tf_op jit(solution)/shard_map/ppermute | solution.py:277
  202.3 25.2 %all_to_all.40.rows_ref = bf16[8,16,2048]{2,1,0:T(8,128)(2,1)S(1)} all-to-all(bf16[8,16,2048]{2,1,0:T(8,128)(2,1)S(1)} %get-tuple-element.18), channel_id=1, replica_groups=mesh['grp'=2,'sp'=16,'kv'=2,'quarter'=4,'core'=2] {'kv','quarter'}, dimensions={0} | all-to-all | bytes 1048576 | tf_op jit(solution)/shard_map/all_to_all | solution.py:273
  229.2 14.4 %all_gather.3.query_ref = bf16[4,128,256]{2,1,0:T(8,128)(2,1)S(1)} all-gather(bf16[1,128,256]{2,1,0:T(8,128)(2,1)S(1)} %project_queries.3), channel_id=1, replica_groups=mesh['grp'=2,'sp'=16,'kv'=2,'quarter'=4,'core'=2] {'quarter'}, dimensions={0}, use_global_device_ids=true | all-gather | bytes 327680 | tf_op jit(solution)/shard_map/all_gather | solution.py:347
  243.6 4.0 %attend.3 = bf16[4,144,256]{2,1,0:T(8,128)(2,1)S(1)} custom-call(s32[1]{0:T(128)} %bitcast.core_ref, bf16[4,128,256]{2,1,0:T(8,128)(2,1)S(1)} %all_gather.3.query_ref, bf16[16,256,128]{2,1,0:T(8,128)(2,1)} %join.7.refs_0_, bf16[16,256,128]{2,1,0:T(8,128)(2,1)} %collective-permute-done.18.refs_1_), custom_call_target="tpu_custom_call" | custom-call | tf_op jit(solution)/shard_map/attend/pallas_call | solution.py:175
  247.7 10.2 %all_to_all.41.part_ref = bf16[4,144,256]{2,1,0:T(8,128)(2,1)S(1)} all-to-all(bf16[4,144,256]{2,1,0:T(8,128)(2,1)S(1)} %attend.3), channel_id=1, replica_groups=mesh['grp'=2,'sp'=16,'kv'=2,'quarter'=4,'core'=2] {'quarter'}, dimensions={0} | all-to-all | bytes 589824 | tf_op jit(solution)/shard_map/all_to_all | solution.py:273
  258.4 15.9 %all_to_all.42.part_ref = bf16[8,16,2048]{2,1,0:T(8,128)(2,1)S(1)} all-to-all(bf16[8,16,2048]{2,1,0:T(8,128)(2,1)S(1)} %merge_and_project.3), channel_id=1, replica_groups=mesh['grp'=2,'sp'=16,'kv'=2,'quarter'=4,'core'=2] {'kv','quarter'}, dimensions={0} | all-to-all | bytes 1048576 | tf_op jit(solution)/shard_map/all_to_all | solution.py:273
  (68 shorter events, 52.9 us)
Async XLA Ops:
  4.6 11.8 %all-to-all-start = ((bf16[8,64,128]{2,1,0:T(8,128)(2,1)}), bf16[8,64,128]{2,1,0:T(8,128)(2,1)S(1)}, u32[]{:S(2)}, u32[]{:S(2)}) async-start(bf16[8,64,128]{2,1,0:T(8,128)(2,1)} %bitcast.4), calls=%async_computation | async-start | bytes 262144 | tf_op jit(solution)/shard_map/all_to_all | solution.py:273
  9.6 100.6 %collective-permute-start = (bf16[2,2048,128]{2,1,0:T(8,128)(2,1)S(1)}, bf16[2,2048,128]{2,1,0:T(8,128)(2,1)}, u32[]{:S(2)}, u32[]{:S(2)}) collective-permute-start(bf16[2,2048,128]{2,1,0:T(8,128)(2,1)S(1)} %copy-done.1), channel_id=1, source_target_pairs={{0,1},{1,0},{2,3},{3,2},{4,5},{5,4},{6,7},{7,6},{8,9},{9,8},{10,11... | collective-permute-start | bytes 3145736 | tf_op jit(solution)/shard_map/ppermute | solution.py:281
  16.4 93.8 %all-to-all-start.1 = ((bf16[8,16,2048]{2,1,0:T(8,128)(2,1)}), bf16[8,16,2048]{2,1,0:T(8,128)(2,1)}, u32[]{:S(2)}, u32[]{:S(2)}) async-start(bf16[8,16,2048]{2,1,0:T(8,128)(2,1)} %first_norm.1), calls=%async_computation.1 | async-start | bytes 1048576 | tf_op jit(solution)/shard_map/all_to_all | solution.py:273
  22.7 48.1 %collective-permute-start.1 = (bf16[1,256,128]{2,1,0:T(8,128)(2,1)S(1)}, bf16[1,256,128]{2,1,0:T(8,128)(2,1)S(1)}, u32[]{:S(2)}, u32[]{:S(2)}) collective-permute-start(bf16[1,256,128]{2,1,0:T(8,128)(2,1)S(1)} %bitcast.11), channel_id=1, source_target_pairs={{0,64},{16,80},{32,96},{48,112},{64,128},{80,144},{96,160},{112,17... | collective-permute-start | bytes 196616 | tf_op jit(solution)/shard_map/ppermute | solution.py:277
  40.5 30.3 %collective-permute-start.2 = (bf16[1,256,128]{2,1,0:T(8,128)(2,1)S(1)}, bf16[1,256,128]{2,1,0:T(8,128)(2,1)S(1)}, u32[]{:S(2)}, u32[]{:S(2)}) collective-permute-start(bf16[1,256,128]{2,1,0:T(8,128)(2,1)S(1)} %bitcast.12), channel_id=1, source_target_pairs={{0,192},{16,208},{32,224},{48,240},{64,0},{80,16},{96,32},{112,48}... | collective-permute-start | bytes 196616 | tf_op jit(solution)/shard_map/ppermute | solution.py:277
  63.5 14.9 %collective-permute-start.3 = (bf16[1,256,128]{2,1,0:T(8,128)(2,1)S(1)}, bf16[1,256,128]{2,1,0:T(8,128)(2,1)S(1)}, u32[]{:S(2)}, u32[]{:S(2)}) collective-permute-start(bf16[1,256,128]{2,1,0:T(8,128)(2,1)S(1)} %bitcast.13), channel_id=1, source_target_pairs={{0,128},{16,144},{32,160},{48,176},{64,192},{80,208},{96,224},{112... | collective-permute-start | bytes 196616 | tf_op jit(solution)/shard_map/ppermute | solution.py:277
  78.4 26.5 %collective-permute-start.4 = (bf16[4,256,128]{2,1,0:T(8,128)(2,1)S(1)}, bf16[4,256,128]{2,1,0:T(8,128)(2,1)S(1)}, u32[]{:S(2)}, u32[]{:S(2)}) collective-permute-start(bf16[4,256,128]{2,1,0:T(8,128)(2,1)S(1)} %join.4.refs_0_), channel_id=1, source_target_pairs={{0,16},{16,32},{32,48},{48,64},{64,80},{80,96},{96,112},{112,128},... | collective-permute-start | bytes 786440 | tf_op jit(solution)/shard_map/ppermute | solution.py:277
  84.4 20.5 %collective-permute-start.5 = (bf16[4,256,128]{2,1,0:T(8,128)(2,1)S(1)}, bf16[4,256,128]{2,1,0:T(8,128)(2,1)S(1)}, u32[]{:S(2)}, u32[]{:S(2)}) collective-permute-start(bf16[4,256,128]{2,1,0:T(8,128)(2,1)S(1)} %join.4.refs_0_), channel_id=1, source_target_pairs={{0,240},{16,0},{32,16},{48,32},{64,48},{80,64},{96,80},{112,96},{1... | collective-permute-start | bytes 786440 | tf_op jit(solution)/shard_map/ppermute | solution.py:277
  93.6 10.4 %collective-permute-start.6 = (bf16[2,256,128]{2,1,0:T(8,128)(2,1)S(1)}, bf16[2,256,128]{2,1,0:T(8,128)(2,1)S(1)}, u32[]{:S(2)}, u32[]{:S(2)}) collective-permute-start(bf16[2,256,128]{2,1,0:T(8,128)(2,1)S(1)} %get-tuple-element.32), channel_id=1, source_target_pairs={{0,32},{16,48},{32,64},{48,80},{64,96},{80,112},{96,128},{112,144}... | collective-permute-start | bytes 393224 | tf_op jit(solution)/shard_map/ppermute | solution.py:277
  95.5 9.3 %collective-permute-start.7 = (bf16[2,256,128]{2,1,0:T(8,128)(2,1)S(1)}, bf16[2,256,128]{2,1,0:T(8,128)(2,1)S(1)}, u32[]{:S(2)}, u32[]{:S(2)}) collective-permute-start(bf16[2,256,128]{2,1,0:T(8,128)(2,1)S(1)} %get-tuple-element.31), channel_id=1, source_target_pairs={{0,224},{16,240},{32,0},{48,16},{64,32},{80,48},{96,64},{112,80},{... | collective-permute-start | bytes 393224 | tf_op jit(solution)/shard_map/ppermute | solution.py:277
  105.8 16.9 %collective-permute-start.9 = (bf16[12,256,128]{2,1,0:T(8,128)(2,1)}, bf16[12,256,128]{2,1,0:T(8,128)(2,1)}, u32[]{:S(2)}, u32[]{:S(2)}) collective-permute-start(bf16[12,256,128]{2,1,0:T(8,128)(2,1)} %join.5.refs_1_), channel_id=1, source_target_pairs={{0,1},{1,0},{2,3},{3,2},{4,5},{5,4},{6,7},{7,6},{8,9},{9,8},{10,11... | collective-permute-start | bytes 2359304 | tf_op jit(solution)/shard_map/ppermute | solution.py:281
  107.7 28.9 %collective-permute-start.10 = (bf16[2,128,2048]{2,1,0:T(8,128)(2,1)S(1)}, bf16[2,128,2048]{2,1,0:T(8,128)(2,1)S(1)}, u32[]{:S(2)}, u32[]{:S(2)}) collective-permute-start(bf16[2,128,2048]{2,1,0:T(8,128)(2,1)S(1)} %copy-done), channel_id=1, source_target_pairs={{0,1},{1,0},{2,3},{3,2},{4,5},{5,4},{6,7},{7,6},{8,9},{9,8},{10,11... | collective-permute-start | bytes 3145736 | tf_op jit(solution)/shard_map/ppermute | solution.py:281
  112.8 14.9 %all-to-all-start.2 = ((bf16[4,128,256]{2,1,0:T(8,128)(2,1)}), bf16[4,128,256]{2,1,0:T(8,128)(2,1)}, u32[]{:S(2)}, u32[]{:S(2)}) async-start(bf16[4,128,256]{2,1,0:T(8,128)(2,1)} %copy-done.4), calls=%async_computation.2 | async-start | bytes 524288 | tf_op jit(solution)/shard_map/all_to_all | solution.py:273
  118.5 3.4 %collective-permute-start.8 = (bf16[4,256,128]{2,1,0:T(8,128)(2,1)S(1)}, bf16[4,256,128]{2,1,0:T(8,128)(2,1)S(1)}, u32[]{:S(2)}, u32[]{:S(2)}) collective-permute-start(bf16[4,256,128]{2,1,0:T(8,128)(2,1)S(1)} %join.4.refs_0_), channel_id=1, source_target_pairs={{0,1},{1,0},{2,3},{3,2},{4,5},{5,4},{6,7},{7,6},{8,9},{9,8},{10,11... | collective-permute-start | bytes 786440 | tf_op jit(solution)/shard_map/ppermute | solution.py:281
  133.1 11.7 %all-to-all-start.3 = ((bf16[4,144,256]{2,1,0:T(8,128)(2,1)}), bf16[4,144,256]{2,1,0:T(8,128)(2,1)S(1)}, u32[]{:S(2)}, u32[]{:S(2)}) async-start(bf16[4,144,256]{2,1,0:T(8,128)(2,1)} %copy-done.3), calls=%async_computation.3 | async-start | bytes 589824 | tf_op jit(solution)/shard_map/all_to_all | solution.py:273
  146.2 54.7 %all-to-all-start.4 = ((bf16[8,16,2048]{2,1,0:T(8,128)(2,1)}), bf16[8,16,2048]{2,1,0:T(8,128)(2,1)}, u32[]{:S(2)}, u32[]{:S(2)}) async-start(bf16[8,16,2048]{2,1,0:T(8,128)(2,1)} %copy-done.2), calls=%async_computation.4 | async-start | bytes 1048576 | tf_op jit(solution)/shard_map/all_to_all | solution.py:273
  152.7 14.3 %collective-permute-start.11 = (bf16[1,256,128]{2,1,0:T(8,128)(2,1)}, bf16[1,256,128]{2,1,0:T(8,128)(2,1)S(1)}, u32[]{:S(2)}, u32[]{:S(2)}) collective-permute-start(bf16[1,256,128]{2,1,0:T(8,128)(2,1)} %bitcast.7), channel_id=1, source_target_pairs={{0,64},{16,80},{32,96},{48,112},{64,128},{80,144},{96,160},{112,17... | collective-permute-start | bytes 196616 | tf_op jit(solution)/shard_map/ppermute | solution.py:277
  155.1 11.8 %collective-permute-start.12 = (bf16[1,256,128]{2,1,0:T(8,128)(2,1)}, bf16[1,256,128]{2,1,0:T(8,128)(2,1)S(1)}, u32[]{:S(2)}, u32[]{:S(2)}) collective-permute-start(bf16[1,256,128]{2,1,0:T(8,128)(2,1)} %bitcast.8), channel_id=1, source_target_pairs={{0,192},{16,208},{32,224},{48,240},{64,0},{80,16},{96,32},{112,48}... | collective-permute-start | bytes 196616 | tf_op jit(solution)/shard_map/ppermute | solution.py:277
  162.5 15.1 %collective-permute-start.13 = (bf16[1,256,128]{2,1,0:T(8,128)(2,1)}, bf16[1,256,128]{2,1,0:T(8,128)(2,1)S(1)}, u32[]{:S(2)}, u32[]{:S(2)}) collective-permute-start(bf16[1,256,128]{2,1,0:T(8,128)(2,1)} %bitcast.9), channel_id=1, source_target_pairs={{0,128},{16,144},{32,160},{48,176},{64,192},{80,208},{96,224},{112... | collective-permute-start | bytes 196616 | tf_op jit(solution)/shard_map/ppermute | solution.py:277
  178.5 19.5 %collective-permute-start.14 = (bf16[4,256,128]{2,1,0:T(8,128)(2,1)S(1)}, bf16[4,256,128]{2,1,0:T(8,128)(2,1)S(1)}, u32[]{:S(2)}, u32[]{:S(2)}) collective-permute-start(bf16[4,256,128]{2,1,0:T(8,128)(2,1)S(1)} %join.6.refs_0_), channel_id=1, source_target_pairs={{0,16},{16,32},{32,48},{48,64},{64,80},{80,96},{96,112},{112,128},... | collective-permute-start | bytes 786440 | tf_op jit(solution)/shard_map/ppermute | solution.py:277
  180.6 17.4 %collective-permute-start.15 = (bf16[4,256,128]{2,1,0:T(8,128)(2,1)S(1)}, bf16[4,256,128]{2,1,0:T(8,128)(2,1)S(1)}, u32[]{:S(2)}, u32[]{:S(2)}) collective-permute-start(bf16[4,256,128]{2,1,0:T(8,128)(2,1)S(1)} %join.6.refs_0_), channel_id=1, source_target_pairs={{0,240},{16,0},{32,16},{48,32},{64,48},{80,64},{96,80},{112,96},{1... | collective-permute-start | bytes 786440 | tf_op jit(solution)/shard_map/ppermute | solution.py:277
  186.7 10.4 %collective-permute-start.16 = (bf16[2,256,128]{2,1,0:T(8,128)(2,1)S(1)}, bf16[2,256,128]{2,1,0:T(8,128)(2,1)S(1)}, u32[]{:S(2)}, u32[]{:S(2)}) collective-permute-start(bf16[2,256,128]{2,1,0:T(8,128)(2,1)S(1)} %get-tuple-element.30), channel_id=1, source_target_pairs={{0,32},{16,48},{32,64},{48,80},{64,96},{80,112},{96,128},{112,144}... | collective-permute-start | bytes 393224 | tf_op jit(solution)/shard_map/ppermute | solution.py:277
  188.7 9.3 %collective-permute-start.17 = (bf16[2,256,128]{2,1,0:T(8,128)(2,1)S(1)}, bf16[2,256,128]{2,1,0:T(8,128)(2,1)S(1)}, u32[]{:S(2)}, u32[]{:S(2)}) collective-permute-start(bf16[2,256,128]{2,1,0:T(8,128)(2,1)S(1)} %get-tuple-element.29), channel_id=1, source_target_pairs={{0,224},{16,240},{32,0},{48,16},{64,32},{80,48},{96,64},{112,80},{... | collective-permute-start | bytes 393224 | tf_op jit(solution)/shard_map/ppermute | solution.py:277
  199.0 44.6 %collective-permute-start.18 = (bf16[16,256,128]{2,1,0:T(8,128)(2,1)}, bf16[16,256,128]{2,1,0:T(8,128)(2,1)}, u32[]{:S(2)}, u32[]{:S(2)}) collective-permute-start(bf16[16,256,128]{2,1,0:T(8,128)(2,1)} %join.7.refs_0_), channel_id=1, source_target_pairs={{0,1},{1,0},{2,3},{3,2},{4,5},{5,4},{6,7},{7,6},{8,9},{9,8},{10,11... | collective-permute-start | bytes 3145736 | tf_op jit(solution)/shard_map/ppermute | solution.py:281
  (11 other events, 187.9 us)

commit v3 on v2

--- a/solution.py
+++ b/solution.py
@@ -17,7 +17,6 @@
 
 CHIPS = ("kv", "quarter")
 GROUP = ("quarter", "core")
-COPIES = (4, 0)
 BF16 = jnp.bfloat16
 F32 = jnp.float32
 
@@ -91,7 +90,7 @@
         norm_kernel,
         in_specs=in_vmem(2),
         out_specs=in_vmem(1)[0],
-        out_shape=vmem_out((chips, *rows.shape)),
+        out_shape=pltpu.HBM((chips, *rows.shape), BF16),
         compiler_params=pltpu.CompilerParams(vmem_limit_bytes=4096 * 1024),
         name="first_norm",
     )(*held_in_vmem(rows, gain))
@@ -117,7 +116,7 @@
         functools.partial(query_kernel, layer),
         in_specs=[pl.BlockSpec(memory_space=pltpu.SMEM)] + in_vmem(3),
         out_specs=in_vmem(1)[0],
-        out_shape=vmem_out((copies, chips * block, 2 * mine.shape[2])),
+        out_shape=pltpu.HBM((copies, chips * block, 2 * mine.shape[2]), BF16),
         compiler_params=pltpu.CompilerParams(vmem_limit_bytes=8192 * 1024),
         name="project_queries",
     )(core, *held_in_vmem(rows, mine, other))
@@ -176,9 +175,9 @@
         functools.partial(attend_kernel, len(mine)),
         in_specs=[pl.BlockSpec(memory_space=pltpu.SMEM)] + in_vmem(1 + 2 * len(mine)),
         out_specs=in_vmem(1)[0],
-        out_shape=vmem_out((heads, rows + STATS, width)),
+        out_shape=pltpu.HBM((heads, rows + STATS, width), BF16),
         scratch_shapes=[pltpu.VMEM((heads * rows, span), F32)],
-        compiler_params=pltpu.CompilerParams(vmem_limit_bytes=20480 * 1024),
+        compiler_params=pltpu.CompilerParams(vmem_limit_bytes=14336 * 1024),
         name="attend",
     )(core, *held_in_vmem(queries, *mine, *other))
 
@@ -238,7 +237,7 @@
         functools.partial(merge_kernel, layer),
         in_specs=[pl.BlockSpec(memory_space=pltpu.SMEM)] + in_vmem(3),
         out_specs=in_vmem(1)[0],
-        out_shape=vmem_out((chips, rows // chips, mine.shape[2])),
+        out_shape=pltpu.HBM((chips, rows // chips, mine.shape[2]), BF16),
         compiler_params=pltpu.CompilerParams(vmem_limit_bytes=8192 * 1024),
         name="merge_and_project",
     )(core, *held_in_vmem(parts, mine, other))
@@ -263,7 +262,7 @@
         functools.partial(finish_kernel, layer),
         in_specs=in_vmem(4),
         out_specs=in_vmem(len(shapes)),
-        out_shape=[vmem_out(shape) for shape in shapes],
+        out_shape=[pltpu.HBM(shape, BF16) for shape in shapes],
         compiler_params=pltpu.CompilerParams(vmem_limit_bytes=4096 * 1024),
         name="finish",
     )(*held_in_vmem(parts, residual, out_gain, query_gain))
@@ -338,27 +337,24 @@
     residual = target
     for layer in range(LAYERS):
         rows = exchange(normed, CHIPS)
-        mine = project_queries(layer, core, rows, query_weight, query_other, COPIES[layer] or 1)
-        if layer == 0:
-            pieces = stride_step(after(blocks[1], mine), stages // 4, stages)
-        if COPIES[layer]:
-            queries = exchange(mine, "quarter")
-        else:
-            queries = lax.all_gather(mine[0], "quarter", axis=0)
+        mine = project_queries(layer, core, rows, query_weight, query_other, quarters)
+        queries = exchange(mine, "quarter")
         parts = attend(core, queries, near[layer], far[layer])
         if layer == 0:
-            own = join(*after(pieces, parts))
-            pieces = near_step(own, stages)
+            pieces = stride_step(after(blocks[1], parts), stages // 4, stages)
         parts = exchange(parts, "quarter")
         projected = merge_and_project(layer, core, parts, out_weight, out_other, chips)
+        if layer == 0:
+            own = join(*after(pieces, projected))
+            pieces = near_step(own, stages)
         arrived = exchange(projected, CHIPS)
-        if layer == 0:
-            whole = join(own, *after(pieces, projected))
-            far.append((swap(whole),))
-            near.append((whole,))
         done = finish(layer, arrived, residual, out_gain, query_gain)
         residual = done[0]
         normed = done[-1]
+        if layer == 0:
+            whole = join(own, *after(pieces, normed))
+            far.append((swap(whole),))
+            near.append((whole,))
     return residual
 
 

time: 277 us -> 268 us (0.968)
  the two profiles are of different devices: /device:TPU:80 before, /device:TPU:65 now
where the time goes in v3:
time: 268 us; the launch traced here: 262 us
  starting transfers between devices  151 us (56%)
  waiting for transfers between devices  46.6 us (17%)
  Pallas kernels  30.3 us (11%)
  blocking collectives  30.3 us (11%)
  local copies, waits for them, and re-layouts  3.21 us (1%)
    all_to_all x7, starting transfers between devices, exchange(): return lax.all_to_all(value, axis, split_axis=0, concat_axis=0, tiled=True)  75.3 us
    ppermute x14, starting transfers between devices, shifted(): lax.ppermute(value, 'sp', [(z, (z + distance) % size) for z in range(size)])  53.1 us
    all_to_all x2, blocking collectives, exchange(): return lax.all_to_all(value, axis, split_axis=0, concat_axis=0, tiled=True)  30.3 us
    ppermute x14, waiting for transfers between devices, shifted(): lax.ppermute(value, 'sp', [(z, (z + distance) % size) for z in range(size)])  26.4 us
    ppermute x5, starting transfers between devices, swap(): return lax.ppermute(value, 'core', [(0, 1), (1, 0)])  23 us
    all_to_all x7, waiting for transfers between devices, exchange(): return lax.all_to_all(value, axis, split_axis=0, concat_axis=0, tiled=True)  19 us
    pallas_call x2, Pallas kernels, attend(): pl.pallas_call(functools.partial(attend_kernel, len(mine)), in_specs=[pl....  9.26 us
  transfers between devices with their start and end apart: 26, of which 12 were waited for; matrix products, arithmetic and copies ran while one was open for 0% of the time, Pallas kernels for 6%

profile of v3, /device:TPU:65, one launch (start us, length us, event | category | flops | bytes accessed | tf_op | source)
XLA Modules:
  0.0 262.2 jit_solution(10902585724417685830)
XLA Ops:
  0.0 4.6 %source_columns.1 = bf16[4,2,64,128]{3,2,1,0:T(8,128)(2,1)} custom-call(bf16[512,2048]{1,0:T(8,128)(2,1)} %source_ref.1, f32[1,2048]{1,0:T(1,128)} %bitcast.17, bf16[2,32,2048]{2,1,0:T(8,128)(2,1)} %bitcast.15, bf16[2,32,2048]{2,1,0:T(8,128)(2,1)} %bitcast.16), custom_call_target="tpu_custom_call" | custom-call | tf_op jit(solution)/shard_map/source_columns/pallas_call | solution.py:65
  4.6 44.7 %all-to-all-start = ((bf16[8,64,128]{2,1,0:T(8,128)(2,1)}), bf16[8,64,128]{2,1,0:T(8,128)(2,1)S(1)}, u32[]{:S(2)}, u32[]{:S(2)}) async-start(bf16[8,64,128]{2,1,0:T(8,128)(2,1)} %bitcast.4), calls=%async_computation | async-start | bytes 262144 | tf_op jit(solution)/shard_map/all_to_all | solution.py:272
  55.2 4.3 %all-to-all-start.1 = ((bf16[8,16,2048]{2,1,0:T(8,128)(2,1)}), bf16[8,16,2048]{2,1,0:T(8,128)(2,1)}, u32[]{:S(2)}, u32[]{:S(2)}) async-start(bf16[8,16,2048]{2,1,0:T(8,128)(2,1)} %first_norm.1), calls=%async_computation.1 | async-start | bytes 1048576 | tf_op jit(solution)/shard_map/all_to_all | solution.py:272
  64.1 7.3 %collective-permute-start.1 = (bf16[1,256,128]{2,1,0:T(8,128)(2,1)S(1)}, bf16[1,256,128]{2,1,0:T(8,128)(2,1)S(1)}, u32[]{:S(2)}, u32[]{:S(2)}) collective-permute-start(bf16[1,256,128]{2,1,0:T(8,128)(2,1)S(1)} %bitcast.13), channel_id=1, source_target_pairs={{0,64},{16,80},{32,96},{48,112},{64,128},{80,144},{96,160},{112,17... | collective-permute-start | bytes 196616 | tf_op jit(solution)/shard_map/ppermute | solution.py:276
  74.3 5.9 %collective-permute-done.1.refs_0_ = bf16[1,256,128]{2,1,0:T(8,128)(2,1)S(1)} collective-permute-done((bf16[1,256,128]{2,1,0:T(8,128)(2,1)S(1)}, bf16[1,256,128]{2,1,0:T(8,128)(2,1)S(1)}, u32[]{:S(2)}, u32[]{:S(2)}) %collective-permute-start.1) | collective-permute-done | bytes 65568 | tf_op jit(solution)/shard_map/ppermute | solution.py:276
  80.2 6.2 %collective-permute-start.5 = (bf16[4,256,128]{2,1,0:T(8,128)(2,1)S(1)}, bf16[4,256,128]{2,1,0:T(8,128)(2,1)S(1)}, u32[]{:S(2)}, u32[]{:S(2)}) collective-permute-start(bf16[4,256,128]{2,1,0:T(8,128)(2,1)S(1)} %join.4.refs_0_), channel_id=1, source_target_pairs={{0,240},{16,0},{32,16},{48,32},{64,48},{80,64},{96,80},{112,96},{1... | collective-permute-start | bytes 786440 | tf_op jit(solution)/shard_map/ppermute | solution.py:276
  100.3 6.9 %collective-permute-start.9 = (bf16[12,256,128]{2,1,0:T(8,128)(2,1)}, bf16[12,256,128]{2,1,0:T(8,128)(2,1)}, u32[]{:S(2)}, u32[]{:S(2)}) collective-permute-start(bf16[12,256,128]{2,1,0:T(8,128)(2,1)} %join.5.refs_1_), channel_id=1, source_target_pairs={{0,1},{1,0},{2,3},{3,2},{4,5},{5,4},{6,7},{7,6},{8,9},{9,8},{10,11... | collective-permute-start | bytes 2359304 | tf_op jit(solution)/shard_map/ppermute | solution.py:280
  111.4 4.5 %all-to-all-start.2 = ((bf16[4,128,256]{2,1,0:T(8,128)(2,1)}), bf16[4,128,256]{2,1,0:T(8,128)(2,1)}, u32[]{:S(2)}, u32[]{:S(2)}) async-start(bf16[4,128,256]{2,1,0:T(8,128)(2,1)} %project_queries.2), calls=%async_computation.2 | async-start | bytes 524288 | tf_op jit(solution)/shard_map/all_to_all | solution.py:272
  124.4 4.5 %attend.2 = bf16[4,144,256]{2,1,0:T(8,128)(2,1)} custom-call(s32[1]{0:T(128)} %bitcast.core_ref, bf16[4,128,256]{2,1,0:T(8,128)(2,1)} %all-to-all-done.2.query_ref, bf16[4,256,128]{2,1,0:T(8,128)(2,1)S(1)} %join.4.refs_0_, bf16[12,256,128]{2,1,0:T(8,128)(2,1)} %join.5.refs_1_, bf16[4,256,128]{2,1,0:T(8,128)(2,1)S(1)} %copy-done.3, ...), custom_call_target="tpu_custom_call" | custom-call | tf_op jit(solution)/shard_map/attend/pallas_call | solution.py:174
  128.9 3.5 %all-to-all-start.3 = ((bf16[4,144,256]{2,1,0:T(8,128)(2,1)}), bf16[4,144,256]{2,1,0:T(8,128)(2,1)S(1)}, u32[]{:S(2)}, u32[]{:S(2)}) async-start(bf16[4,144,256]{2,1,0:T(8,128)(2,1)} %attend.2), calls=%async_computation.3 | async-start | bytes 589824 | tf_op jit(solution)/shard_map/all_to_all | solution.py:272
  132.5 5.8 %all-to-all-done.3.part_ref = bf16[4,144,256]{2,1,0:T(8,128)(2,1)S(1)} async-done(((bf16[4,144,256]{2,1,0:T(8,128)(2,1)}), bf16[4,144,256]{2,1,0:T(8,128)(2,1)S(1)}, u32[]{:S(2)}, u32[]{:S(2)}) %all-to-all-start.3) | async-done | bytes 294944 | tf_op jit(solution)/shard_map/all_to_all | solution.py:272
  140.9 6.9 %all-to-all-start.4 = ((bf16[8,16,2048]{2,1,0:T(8,128)(2,1)}), bf16[8,16,2048]{2,1,0:T(8,128)(2,1)}, u32[]{:S(2)}, u32[]{:S(2)}) async-start(bf16[8,16,2048]{2,1,0:T(8,128)(2,1)} %merge_and_project.2), calls=%async_computation.4 | async-start | bytes 1048576 | tf_op jit(solution)/shard_map/all_to_all | solution.py:272
  147.7 6.3 %collective-permute-start.13 = (bf16[1,256,128]{2,1,0:T(8,128)(2,1)}, bf16[1,256,128]{2,1,0:T(8,128)(2,1)S(1)}, u32[]{:S(2)}, u32[]{:S(2)}) collective-permute-start(bf16[1,256,128]{2,1,0:T(8,128)(2,1)} %bitcast.7), channel_id=1, source_target_pairs={{0,128},{16,144},{32,160},{48,176},{64,192},{80,208},{96,224},{112... | collective-permute-start | bytes 196616 | tf_op jit(solution)/shard_map/ppermute | solution.py:276
  157.3 6.4 %collective-permute-start.11 = (bf16[1,256,128]{2,1,0:T(8,128)(2,1)}, bf16[1,256,128]{2,1,0:T(8,128)(2,1)S(1)}, u32[]{:S(2)}, u32[]{:S(2)}) collective-permute-start(bf16[1,256,128]{2,1,0:T(8,128)(2,1)} %bitcast.9), channel_id=1, source_target_pairs={{0,64},{16,80},{32,96},{48,112},{64,128},{80,144},{96,160},{112,17... | collective-permute-start | bytes 196616 | tf_op jit(solution)/shard_map/ppermute | solution.py:276
  163.8 6.6 %collective-permute-done.12.refs_2_ = bf16[1,256,128]{2,1,0:T(8,128)(2,1)S(1)} collective-permute-done((bf16[1,256,128]{2,1,0:T(8,128)(2,1)}, bf16[1,256,128]{2,1,0:T(8,128)(2,1)S(1)}, u32[]{:S(2)}, u32[]{:S(2)}) %collective-permute-start.12) | collective-permute-done | bytes 65568 | tf_op jit(solution)/shard_map/ppermute | solution.py:276
  178.8 6.6 %all-to-all-start.5 = ((bf16[8,16,2048]{2,1,0:T(8,128)(2,1)}), bf16[8,16,2048]{2,1,0:T(8,128)(2,1)}, u32[]{:S(2)}, u32[]{:S(2)}) async-start(bf16[8,16,2048]{2,1,0:T(8,128)(2,1)} %get-tuple-element.18), calls=%async_computation.5 | async-start | bytes 1048576 | tf_op jit(solution)/shard_map/all_to_all | solution.py:272
  185.4 3.8 %collective-permute-start.17 = (bf16[2,256,128]{2,1,0:T(8,128)(2,1)S(1)}, bf16[2,256,128]{2,1,0:T(8,128)(2,1)S(1)}, u32[]{:S(2)}, u32[]{:S(2)}) collective-permute-start(bf16[2,256,128]{2,1,0:T(8,128)(2,1)S(1)} %get-tuple-element.29), channel_id=1, source_target_pairs={{0,224},{16,240},{32,0},{48,16},{64,32},{80,48},{96,64},{112,80},{... | collective-permute-start | bytes 393224 | tf_op jit(solution)/shard_map/ppermute | solution.py:276
  193.2 4.7 %collective-permute-done.16.refs_3_ = bf16[2,256,128]{2,1,0:T(8,128)(2,1)S(1)} collective-permute-done((bf16[2,256,128]{2,1,0:T(8,128)(2,1)S(1)}, bf16[2,256,128]{2,1,0:T(8,128)(2,1)S(1)}, u32[]{:S(2)}, u32[]{:S(2)}) %collective-permute-start.16) | collective-permute-done | bytes 131104 | tf_op jit(solution)/shard_map/ppermute | solution.py:276
  200.0 9.2 %collective-permute-start.18 = (bf16[16,256,128]{2,1,0:T(8,128)(2,1)}, bf16[16,256,128]{2,1,0:T(8,128)(2,1)}, u32[]{:S(2)}, u32[]{:S(2)}) collective-permute-start(bf16[16,256,128]{2,1,0:T(8,128)(2,1)} %join.7.refs_0_), channel_id=1, source_target_pairs={{0,1},{1,0},{2,3},{3,2},{4,5},{5,4},{6,7},{7,6},{8,9},{9,8},{10,11... | collective-permute-start | bytes 3145736 | tf_op jit(solution)/shard_map/ppermute | solution.py:280
  211.4 4.8 %all-to-all-start.6 = ((bf16[4,128,256]{2,1,0:T(8,128)(2,1)}), bf16[4,128,256]{2,1,0:T(8,128)(2,1)S(1)}, u32[]{:S(2)}, u32[]{:S(2)}) async-start(bf16[4,128,256]{2,1,0:T(8,128)(2,1)} %project_queries.3), calls=%async_computation.6 | async-start | bytes 524288 | tf_op jit(solution)/shard_map/all_to_all | solution.py:272
  216.2 7.5 %all-to-all-done.6.query_ref = bf16[4,128,256]{2,1,0:T(8,128)(2,1)S(1)} async-done(((bf16[4,128,256]{2,1,0:T(8,128)(2,1)}), bf16[4,128,256]{2,1,0:T(8,128)(2,1)S(1)}, u32[]{:S(2)}, u32[]{:S(2)}) %all-to-all-start.6) | async-done | bytes 262176 | tf_op jit(solution)/shard_map/all_to_all | solution.py:272
  223.7 4.8 %attend.3 = bf16[4,144,256]{2,1,0:T(8,128)(2,1)} custom-call(s32[1]{0:T(128)} %bitcast.core_ref, bf16[4,128,256]{2,1,0:T(8,128)(2,1)S(1)} %all-to-all-done.6.query_ref, bf16[16,256,128]{2,1,0:T(8,128)(2,1)} %join.7.refs_0_, bf16[16,256,128]{2,1,0:T(8,128)(2,1)} %collective-permute-done.18.refs_1_), custom_call_target="tpu_custom_call" | custom-call | tf_op jit(solution)/shard_map/attend/pallas_call | solution.py:174
  228.4 10.1 %all_to_all.45.part_ref = bf16[4,144,256]{2,1,0:T(8,128)(2,1)S(1)} all-to-all(bf16[4,144,256]{2,1,0:T(8,128)(2,1)} %attend.3), channel_id=1, replica_groups=mesh['grp'=2,'sp'=16,'kv'=2,'quarter'=4,'core'=2] {'quarter'}, dimensions={0} | all-to-all | bytes 589824 | tf_op jit(solution)/shard_map/all_to_all | solution.py:272
  241.2 20.2 %all_to_all.46.part_ref = bf16[8,16,2048]{2,1,0:T(8,128)(2,1)S(1)} all-to-all(bf16[8,16,2048]{2,1,0:T(8,128)(2,1)} %merge_and_project.3), channel_id=1, replica_groups=mesh['grp'=2,'sp'=16,'kv'=2,'quarter'=4,'core'=2] {'kv','quarter'}, dimensions={0} | all-to-all | bytes 1048576 | tf_op jit(solution)/shard_map/all_to_all | solution.py:272
  (65 shorter events, 65.8 us)
Async XLA Ops:
  4.6 50.6 %all-to-all-start = ((bf16[8,64,128]{2,1,0:T(8,128)(2,1)}), bf16[8,64,128]{2,1,0:T(8,128)(2,1)S(1)}, u32[]{:S(2)}, u32[]{:S(2)}) async-start(bf16[8,64,128]{2,1,0:T(8,128)(2,1)} %bitcast.4), calls=%async_computation | async-start | bytes 262144 | tf_op jit(solution)/shard_map/all_to_all | solution.py:272
  49.3 59.9 %collective-permute-start = (bf16[2,2048,128]{2,1,0:T(8,128)(2,1)S(1)}, bf16[2,2048,128]{2,1,0:T(8,128)(2,1)S(1)}, u32[]{:S(2)}, u32[]{:S(2)}) collective-permute-start(bf16[2,2048,128]{2,1,0:T(8,128)(2,1)S(1)} %copy-done), channel_id=1, source_target_pairs={{0,1},{1,0},{2,3},{3,2},{4,5},{5,4},{6,7},{7,6},{8,9},{9,8},{10,11... | collective-permute-start | bytes 3145736 | tf_op jit(solution)/shard_map/ppermute | solution.py:280
  55.2 54.0 %all-to-all-start.1 = ((bf16[8,16,2048]{2,1,0:T(8,128)(2,1)}), bf16[8,16,2048]{2,1,0:T(8,128)(2,1)}, u32[]{:S(2)}, u32[]{:S(2)}) async-start(bf16[8,16,2048]{2,1,0:T(8,128)(2,1)} %first_norm.1), calls=%async_computation.1 | async-start | bytes 1048576 | tf_op jit(solution)/shard_map/all_to_all | solution.py:272
  60.2 14.2 %collective-permute-start.3 = (bf16[1,256,128]{2,1,0:T(8,128)(2,1)S(1)}, bf16[1,256,128]{2,1,0:T(8,128)(2,1)S(1)}, u32[]{:S(2)}, u32[]{:S(2)}) collective-permute-start(bf16[1,256,128]{2,1,0:T(8,128)(2,1)S(1)} %bitcast.11), channel_id=1, source_target_pairs={{0,128},{16,144},{32,160},{48,176},{64,192},{80,208},{96,224},{112... | collective-permute-start | bytes 196616 | tf_op jit(solution)/shard_map/ppermute | solution.py:276
  62.1 12.2 %collective-permute-start.2 = (bf16[1,256,128]{2,1,0:T(8,128)(2,1)S(1)}, bf16[1,256,128]{2,1,0:T(8,128)(2,1)S(1)}, u32[]{:S(2)}, u32[]{:S(2)}) collective-permute-start(bf16[1,256,128]{2,1,0:T(8,128)(2,1)S(1)} %bitcast.12), channel_id=1, source_target_pairs={{0,192},{16,208},{32,224},{48,240},{64,0},{80,16},{96,32},{112,48}... | collective-permute-start | bytes 196616 | tf_op jit(solution)/shard_map/ppermute | solution.py:276
  64.1 16.1 %collective-permute-start.1 = (bf16[1,256,128]{2,1,0:T(8,128)(2,1)S(1)}, bf16[1,256,128]{2,1,0:T(8,128)(2,1)S(1)}, u32[]{:S(2)}, u32[]{:S(2)}) collective-permute-start(bf16[1,256,128]{2,1,0:T(8,128)(2,1)S(1)} %bitcast.13), channel_id=1, source_target_pairs={{0,64},{16,80},{32,96},{48,112},{64,128},{80,144},{96,160},{112,17... | collective-permute-start | bytes 196616 | tf_op jit(solution)/shard_map/ppermute | solution.py:276
  80.2 19.1 %collective-permute-start.5 = (bf16[4,256,128]{2,1,0:T(8,128)(2,1)S(1)}, bf16[4,256,128]{2,1,0:T(8,128)(2,1)S(1)}, u32[]{:S(2)}, u32[]{:S(2)}) collective-permute-start(bf16[4,256,128]{2,1,0:T(8,128)(2,1)S(1)} %join.4.refs_0_), channel_id=1, source_target_pairs={{0,240},{16,0},{32,16},{48,32},{64,48},{80,64},{96,80},{112,96},{1... | collective-permute-start | bytes 786440 | tf_op jit(solution)/shard_map/ppermute | solution.py:276
  86.4 13.0 %collective-permute-start.4 = (bf16[4,256,128]{2,1,0:T(8,128)(2,1)S(1)}, bf16[4,256,128]{2,1,0:T(8,128)(2,1)S(1)}, u32[]{:S(2)}, u32[]{:S(2)}) collective-permute-start(bf16[4,256,128]{2,1,0:T(8,128)(2,1)S(1)} %join.4.refs_0_), channel_id=1, source_target_pairs={{0,16},{16,32},{32,48},{48,64},{64,80},{80,96},{96,112},{112,128},... | collective-permute-start | bytes 786440 | tf_op jit(solution)/shard_map/ppermute | solution.py:276
  88.4 8.8 %collective-permute-start.7 = (bf16[2,256,128]{2,1,0:T(8,128)(2,1)S(1)}, bf16[2,256,128]{2,1,0:T(8,128)(2,1)S(1)}, u32[]{:S(2)}, u32[]{:S(2)}) collective-permute-start(bf16[2,256,128]{2,1,0:T(8,128)(2,1)S(1)} %get-tuple-element.31), channel_id=1, source_target_pairs={{0,224},{16,240},{32,0},{48,16},{64,32},{80,48},{96,64},{112,80},{... | collective-permute-start | bytes 393224 | tf_op jit(solution)/shard_map/ppermute | solution.py:276
  91.5 7.9 %collective-permute-start.6 = (bf16[2,256,128]{2,1,0:T(8,128)(2,1)S(1)}, bf16[2,256,128]{2,1,0:T(8,128)(2,1)S(1)}, u32[]{:S(2)}, u32[]{:S(2)}) collective-permute-start(bf16[2,256,128]{2,1,0:T(8,128)(2,1)S(1)} %get-tuple-element.32), channel_id=1, source_target_pairs={{0,32},{16,48},{32,64},{48,80},{64,96},{80,112},{96,128},{112,144}... | collective-permute-start | bytes 393224 | tf_op jit(solution)/shard_map/ppermute | solution.py:276
  100.3 20.1 %collective-permute-start.9 = (bf16[12,256,128]{2,1,0:T(8,128)(2,1)}, bf16[12,256,128]{2,1,0:T(8,128)(2,1)}, u32[]{:S(2)}, u32[]{:S(2)}) collective-permute-start(bf16[12,256,128]{2,1,0:T(8,128)(2,1)} %join.5.refs_1_), channel_id=1, source_target_pairs={{0,1},{1,0},{2,3},{3,2},{4,5},{5,4},{6,7},{7,6},{8,9},{9,8},{10,11... | collective-permute-start | bytes 2359304 | tf_op jit(solution)/shard_map/ppermute | solution.py:280
  107.2 25.2 %collective-permute-start.10 = (bf16[2,128,2048]{2,1,0:T(8,128)(2,1)S(1)}, bf16[2,128,2048]{2,1,0:T(8,128)(2,1)}, u32[]{:S(2)}, u32[]{:S(2)}) collective-permute-start(bf16[2,128,2048]{2,1,0:T(8,128)(2,1)S(1)} %copy-done.1), channel_id=1, source_target_pairs={{0,1},{1,0},{2,3},{3,2},{4,5},{5,4},{6,7},{7,6},{8,9},{9,8},{10,11... | collective-permute-start | bytes 3145736 | tf_op jit(solution)/shard_map/ppermute | solution.py:280
  111.4 12.1 %all-to-all-start.2 = ((bf16[4,128,256]{2,1,0:T(8,128)(2,1)}), bf16[4,128,256]{2,1,0:T(8,128)(2,1)}, u32[]{:S(2)}, u32[]{:S(2)}) async-start(bf16[4,128,256]{2,1,0:T(8,128)(2,1)} %project_queries.2), calls=%async_computation.2 | async-start | bytes 524288 | tf_op jit(solution)/shard_map/all_to_all | solution.py:272
  128.9 9.4 %all-to-all-start.3 = ((bf16[4,144,256]{2,1,0:T(8,128)(2,1)}), bf16[4,144,256]{2,1,0:T(8,128)(2,1)S(1)}, u32[]{:S(2)}, u32[]{:S(2)}) async-start(bf16[4,144,256]{2,1,0:T(8,128)(2,1)} %attend.2), calls=%async_computation.3 | async-start | bytes 589824 | tf_op jit(solution)/shard_map/all_to_all | solution.py:272
  140.9 35.8 %all-to-all-start.4 = ((bf16[8,16,2048]{2,1,0:T(8,128)(2,1)}), bf16[8,16,2048]{2,1,0:T(8,128)(2,1)}, u32[]{:S(2)}, u32[]{:S(2)}) async-start(bf16[8,16,2048]{2,1,0:T(8,128)(2,1)} %merge_and_project.2), calls=%async_computation.4 | async-start | bytes 1048576 | tf_op jit(solution)/shard_map/all_to_all | solution.py:272
  147.7 16.0 %collective-permute-start.13 = (bf16[1,256,128]{2,1,0:T(8,128)(2,1)}, bf16[1,256,128]{2,1,0:T(8,128)(2,1)S(1)}, u32[]{:S(2)}, u32[]{:S(2)}) collective-permute-start(bf16[1,256,128]{2,1,0:T(8,128)(2,1)} %bitcast.7), channel_id=1, source_target_pairs={{0,128},{16,144},{32,160},{48,176},{64,192},{80,208},{96,224},{112... | collective-permute-start | bytes 196616 | tf_op jit(solution)/shard_map/ppermute | solution.py:276
  154.1 16.3 %collective-permute-start.12 = (bf16[1,256,128]{2,1,0:T(8,128)(2,1)}, bf16[1,256,128]{2,1,0:T(8,128)(2,1)S(1)}, u32[]{:S(2)}, u32[]{:S(2)}) collective-permute-start(bf16[1,256,128]{2,1,0:T(8,128)(2,1)} %bitcast.8), channel_id=1, source_target_pairs={{0,192},{16,208},{32,224},{48,240},{64,0},{80,16},{96,32},{112,48}... | collective-permute-start | bytes 196616 | tf_op jit(solution)/shard_map/ppermute | solution.py:276
  157.3 13.1 %collective-permute-start.11 = (bf16[1,256,128]{2,1,0:T(8,128)(2,1)}, bf16[1,256,128]{2,1,0:T(8,128)(2,1)S(1)}, u32[]{:S(2)}, u32[]{:S(2)}) collective-permute-start(bf16[1,256,128]{2,1,0:T(8,128)(2,1)} %bitcast.9), channel_id=1, source_target_pairs={{0,64},{16,80},{32,96},{48,112},{64,128},{80,144},{96,160},{112,17... | collective-permute-start | bytes 196616 | tf_op jit(solution)/shard_map/ppermute | solution.py:276
  171.3 26.6 %collective-permute-start.15 = (bf16[4,256,128]{2,1,0:T(8,128)(2,1)S(1)}, bf16[4,256,128]{2,1,0:T(8,128)(2,1)}, u32[]{:S(2)}, u32[]{:S(2)}) collective-permute-start(bf16[4,256,128]{2,1,0:T(8,128)(2,1)S(1)} %join.6.refs_0_), channel_id=1, source_target_pairs={{0,240},{16,0},{32,16},{48,32},{64,48},{80,64},{96,80},{112,96},{1... | collective-permute-start | bytes 786440 | tf_op jit(solution)/shard_map/ppermute | solution.py:276
  173.2 24.7 %collective-permute-start.14 = (bf16[4,256,128]{2,1,0:T(8,128)(2,1)S(1)}, bf16[4,256,128]{2,1,0:T(8,128)(2,1)}, u32[]{:S(2)}, u32[]{:S(2)}) collective-permute-start(bf16[4,256,128]{2,1,0:T(8,128)(2,1)S(1)} %join.6.refs_0_), channel_id=1, source_target_pairs={{0,16},{16,32},{32,48},{48,64},{64,80},{80,96},{96,112},{112,128},... | collective-permute-start | bytes 786440 | tf_op jit(solution)/shard_map/ppermute | solution.py:276
  178.8 30.4 %all-to-all-start.5 = ((bf16[8,16,2048]{2,1,0:T(8,128)(2,1)}), bf16[8,16,2048]{2,1,0:T(8,128)(2,1)}, u32[]{:S(2)}, u32[]{:S(2)}) async-start(bf16[8,16,2048]{2,1,0:T(8,128)(2,1)} %get-tuple-element.18), calls=%async_computation.5 | async-start | bytes 1048576 | tf_op jit(solution)/shard_map/all_to_all | solution.py:272
  189.3 8.6 %collective-permute-start.16 = (bf16[2,256,128]{2,1,0:T(8,128)(2,1)S(1)}, bf16[2,256,128]{2,1,0:T(8,128)(2,1)S(1)}, u32[]{:S(2)}, u32[]{:S(2)}) collective-permute-start(bf16[2,256,128]{2,1,0:T(8,128)(2,1)S(1)} %get-tuple-element.30), channel_id=1, source_target_pairs={{0,32},{16,48},{32,64},{48,80},{64,96},{80,112},{96,128},{112,144}... | collective-permute-start | bytes 393224 | tf_op jit(solution)/shard_map/ppermute | solution.py:276
  200.0 16.2 %collective-permute-start.18 = (bf16[16,256,128]{2,1,0:T(8,128)(2,1)}, bf16[16,256,128]{2,1,0:T(8,128)(2,1)}, u32[]{:S(2)}, u32[]{:S(2)}) collective-permute-start(bf16[16,256,128]{2,1,0:T(8,128)(2,1)} %join.7.refs_0_), channel_id=1, source_target_pairs={{0,1},{1,0},{2,3},{3,2},{4,5},{5,4},{6,7},{7,6},{8,9},{9,8},{10,11... | collective-permute-start | bytes 3145736 | tf_op jit(solution)/shard_map/ppermute | solution.py:280
  211.4 12.3 %all-to-all-start.6 = ((bf16[4,128,256]{2,1,0:T(8,128)(2,1)}), bf16[4,128,256]{2,1,0:T(8,128)(2,1)S(1)}, u32[]{:S(2)}, u32[]{:S(2)}) async-start(bf16[4,128,256]{2,1,0:T(8,128)(2,1)} %project_queries.3), calls=%async_computation.6 | async-start | bytes 524288 | tf_op jit(solution)/shard_map/all_to_all | solution.py:272
  (11 other events, 288.3 us)

commit v4 on v3

--- a/solution.py
+++ b/solution.py
@@ -9,7 +9,6 @@
 from jax.sharding import PartitionSpec as P
 
 
-HD = 256
 KVH = 2
 LAYERS = 2
 EPSILON = 1e-06
@@ -44,8 +43,10 @@
 
 def source_kernel(source_ref, gain_ref, key_ref, value_ref, out_ref, weight_ref):
     width = key_ref.shape[1]
-
-    @pl.when(pl.program_id(0) == 0)
+    quarters = out_ref.shape[0]
+    step = pl.program_id(0)
+
+    @pl.when(step == 0)
     def _():
         for layer in range(LAYERS):
             weight_ref[layer * width : (layer + 1) * width, :] = key_ref[layer]
@@ -53,7 +54,17 @@
 
     normed = scaled(source_ref[...].astype(F32), gain_ref[...]).astype(BF16)
     columns = dot(weight_ref[...], normed, ((1,), (1,))).astype(BF16)
-    out_ref[...] = columns.reshape(out_ref.shape)
+    for block in range(quarters):
+
+        @pl.when(step == block)
+        def _():
+            half, at = block // 2, width * (1 + block % 2)
+            for core in range(2):
+                first = columns[2 * core * width : (2 * core + 1) * width]
+                later = columns[(2 * core + 1) * width : (2 * core + 2) * width]
+                out_ref[block, core, :width, :] = first
+                for quarter in range(half, quarters, 2):
+                    out_ref[quarter, core, at : at + width, :] = later
 
 
 def source_columns(source, gain, key_weight, value_weight, quarters):
@@ -62,6 +73,8 @@
     value_weight = jnp.swapaxes(value_weight, 1, 2)
     width = key_weight.shape[1]
     block = rows // quarters
+    shape = (quarters, 2, 3 * width, block)
+    operands = (source, gain, key_weight, value_weight)
     return pl.pallas_call(
         source_kernel,
         grid=(quarters,),
@@ -71,12 +84,12 @@
             pl.BlockSpec(key_weight.shape, lambda i: (0, 0, 0)),
             pl.BlockSpec(value_weight.shape, lambda i: (0, 0, 0)),
         ],
-        out_specs=pl.BlockSpec((1, 2, LAYERS * width, block), lambda i: (i, 0, 0, 0)),
-        out_shape=jax.ShapeDtypeStruct((quarters, 2, LAYERS * width, block), BF16),
+        out_specs=pl.BlockSpec(shape, lambda i: (0, 0, 0, 0)),
+        out_shape=pltpu.HBM(shape, BF16),
         scratch_shapes=[pltpu.VMEM((2 * LAYERS * width, features), BF16)],
         compiler_params=pltpu.CompilerParams(vmem_limit_bytes=12288 * 1024),
         name="source_columns",
-    )(*[pltpu.with_memory_space_constraint(a, pltpu.HBM) for a in (source, gain, key_weight, value_weight)])
+    )(*[pltpu.with_memory_space_constraint(a, pltpu.HBM) for a in operands])
 
 
 def norm_kernel(rows_ref, gain_ref, out_ref):
@@ -110,23 +123,25 @@
         out_ref[peer, :, width:] = high
 
 
-def project_queries(layer, core, rows, mine, other, copies):
+def project_queries(layer, core, rows, mine, other, copies, held):
     chips, block, _ = rows.shape
     return pl.pallas_call(
         functools.partial(query_kernel, layer),
         in_specs=[pl.BlockSpec(memory_space=pltpu.SMEM)] + in_vmem(3),
         out_specs=in_vmem(1)[0],
-        out_shape=pltpu.HBM((copies, chips * block, 2 * mine.shape[2]), BF16),
+        out_shape=held((copies, chips * block, 2 * mine.shape[2]), BF16),
         compiler_params=pltpu.CompilerParams(vmem_limit_bytes=8192 * 1024),
         name="project_queries",
-    )(core, *held_in_vmem(rows, mine, other))
-
-
-def attend_kernel(pieces, core_ref, query_ref, *refs):
+    )(core, pltpu.with_memory_space_constraint(rows, pltpu.HBM), *held_in_vmem(mine, other))
+
+
+def attend_kernel(groups, pieces, core_ref, *refs):
+    query_refs, refs = refs[:groups], refs[groups:]
     mine_refs, other_refs = refs[:pieces], refs[pieces : 2 * pieces]
-    out_ref, score_ref = refs[2 * pieces :]
-    heads, rows, width = query_ref.shape
-    queries = query_ref[...].reshape(heads * rows, width)
+    out_refs, score_ref = refs[2 * pieces : -1], refs[-1]
+    heads, rows, width = query_refs[0].shape
+    queries = [ref[...].reshape(heads * rows, width) for ref in query_refs]
+    queries = queries[0] if groups == 1 else jnp.concatenate(queries, axis=0)
     scale = width ** (-0.5)
 
     def pairs(piece_refs):
@@ -150,14 +165,16 @@
             share = dot(weights.astype(BF16), values, ((1,), (1,)))
             total = part if total is None else total + part
             mixed = share if mixed is None else mixed + share
-        out_ref[:, :rows, :] = (mixed / total).astype(BF16).reshape(heads, rows, width)
+        attended = (mixed / total).astype(BF16)
         level = peak + jnp.log(total)
         high = level.astype(BF16).astype(F32)
         low = level - high
-        for h in range(heads):
+        for h in range(heads * groups):
+            out_ref, own = out_refs[h // heads], slice(h * rows, (h + 1) * rows)
+            out_ref[h % heads, :rows, :] = attended[own]
             for part, at in ((high, 0), (low, rows)):
-                column = jnp.broadcast_to(part[h * rows : (h + 1) * rows], (rows, rows))
-                out_ref[h, rows:, at : at + rows] = column.T[:STATS].astype(BF16)
+                column = jnp.broadcast_to(part[own], (rows, rows))
+                out_ref[h % heads, rows:, at : at + rows] = column.T[:STATS].astype(BF16)
 
     @pl.when(core_ref[0] == 0)
     def _():
@@ -169,17 +186,65 @@
 
 
 def attend(core, queries, mine, other):
-    heads, rows, width = queries.shape
+    heads, rows, width = queries[0].shape
+    groups = len(queries)
     span = sum(piece.shape[0] * piece.shape[2] for piece in mine)
     return pl.pallas_call(
-        functools.partial(attend_kernel, len(mine)),
-        in_specs=[pl.BlockSpec(memory_space=pltpu.SMEM)] + in_vmem(1 + 2 * len(mine)),
-        out_specs=in_vmem(1)[0],
-        out_shape=pltpu.HBM((heads, rows + STATS, width), BF16),
-        scratch_shapes=[pltpu.VMEM((heads * rows, span), F32)],
-        compiler_params=pltpu.CompilerParams(vmem_limit_bytes=14336 * 1024),
+        functools.partial(attend_kernel, groups, len(mine)),
+        in_specs=[pl.BlockSpec(memory_space=pltpu.SMEM)] + in_vmem(groups + 2 * len(mine)),
+        out_specs=in_vmem(groups),
+        out_shape=[vmem_out((heads, rows + STATS, width))] * groups,
+        scratch_shapes=[pltpu.VMEM((groups * heads * rows, span), F32)],
+        compiler_params=pltpu.CompilerParams(vmem_limit_bytes=16384 * 1024),
         name="attend",
-    )(core, *held_in_vmem(queries, *mine, *other))
+    )(core, *held_in_vmem(*queries, *mine, *other))
+
+
+def split_kernel(held_ref, first_ref, later_ref):
+    devices, width, _ = held_ref.shape
+    width //= 3
+    for device in range(devices):
+        columns = slice(device * width, (device + 1) * width)
+        first_ref[0, columns, :] = held_ref[device, :width, :]
+        for half in range(2):
+            at = width * (1 + half)
+            later_ref[half, columns, :] = held_ref[device, at : at + width, :]
+
+
+def split(held):
+    devices, width, block = held.shape
+    column = devices * width // 3
+    return pl.pallas_call(
+        split_kernel,
+        in_specs=in_vmem(1),
+        out_specs=in_vmem(2),
+        out_shape=[vmem_out((1, column, block)), pltpu.HBM((2, column, block), BF16)],
+        compiler_params=pltpu.CompilerParams(vmem_limit_bytes=2048 * 1024),
+        name="split",
+    )(*held_in_vmem(held))
+
+
+def four_kernel(*refs):
+    pieces, (own_ref, low_ref, middle_ref) = refs[:4], refs[4:]
+    for at, ref in enumerate(pieces):
+        block = ref[0]
+        own_ref[at] = block
+        if at < 2:
+            low_ref[at] = block
+        if 1 <= at < 3:
+            middle_ref[at - 1] = block
+
+
+def join_four(*pieces):
+    shape = pieces[0].shape[1:]
+    return pl.pallas_call(
+        four_kernel,
+        in_specs=in_vmem(4),
+        out_specs=in_vmem(3),
+        out_shape=[vmem_out((count, *shape)) for count in (4, 2, 2)],
+        compiler_params=pltpu.CompilerParams(vmem_limit_bytes=2048 * 1024),
+        name="join_four",
+    )(*held_in_vmem(*pieces))
 
 
 def join_kernel(*refs):
@@ -201,12 +266,13 @@
     )(*held_in_vmem(*pieces))
 
 
-def merge_kernel(layer, core_ref, part_ref, mine_ref, other_ref, out_ref):
-    parts, extended, _ = part_ref.shape
-    rows = extended - STATS
+def merge_kernel(layer, core_ref, *refs):
+    part_refs, (mine_ref, other_ref, out_ref) = refs[:-3], refs[-3:]
+    parts = [ref.at[s] for ref in part_refs for s in range(ref.shape[0])]
+    rows = parts[0].shape[0] - STATS
     levels = []
-    for s in range(parts):
-        stats = part_ref[s, rows:, :].astype(F32)
+    for part in parts:
+        stats = part[rows:, :].astype(F32)
         line = stats[:1, :rows] + stats[:1, rows:]
         levels.append(jnp.broadcast_to(line, (rows, rows)).T)
     peak = levels[0]
@@ -220,8 +286,8 @@
     halves = []
     for at in (0, half):
         mixed = None
-        for s in range(parts):
-            term = part_ref[s, :rows, at : at + half].astype(F32) * shares[s]
+        for part, share in zip(parts, shares):
+            term = part[:rows, at : at + half].astype(F32) * share
             mixed = term if mixed is None else mixed + term
         halves.append((mixed / total).astype(BF16))
     first = core_ref[0] == 0
@@ -232,15 +298,15 @@
 
 
 def merge_and_project(layer, core, parts, mine, other, chips):
-    rows = parts.shape[1] - STATS
+    rows = parts[0].shape[1] - STATS
     return pl.pallas_call(
         functools.partial(merge_kernel, layer),
-        in_specs=[pl.BlockSpec(memory_space=pltpu.SMEM)] + in_vmem(3),
+        in_specs=[pl.BlockSpec(memory_space=pltpu.SMEM)] + in_vmem(len(parts) + 2),
         out_specs=in_vmem(1)[0],
-        out_shape=pltpu.HBM((chips, rows // chips, mine.shape[2]), BF16),
+        out_shape=vmem_out((chips, rows // chips, mine.shape[2])),
         compiler_params=pltpu.CompilerParams(vmem_limit_bytes=8192 * 1024),
         name="merge_and_project",
-    )(core, *held_in_vmem(parts, mine, other))
+    )(core, *held_in_vmem(*parts, mine, other))
 
 
 def finish_kernel(layer, part_ref, residual_ref, out_gain_ref, query_gain_ref, *out_refs):
@@ -262,7 +328,7 @@
         functools.partial(finish_kernel, layer),
         in_specs=in_vmem(4),
         out_specs=in_vmem(len(shapes)),
-        out_shape=[pltpu.HBM(shape, BF16) for shape in shapes],
+        out_shape=[jax.ShapeDtypeStruct(shapes[0], BF16)] + [pltpu.HBM(shape, BF16) for shape in shapes[1:]],
         compiler_params=pltpu.CompilerParams(vmem_limit_bytes=4096 * 1024),
         name="finish",
     )(*held_in_vmem(parts, residual, out_gain, query_gain))
@@ -280,6 +346,10 @@
     return lax.ppermute(value, "core", [(0, 1), (1, 0)])
 
 
+def beside(value, quarters):
+    return lax.ppermute(value, "quarter", [(q, q ^ 1) for q in range(quarters)])
+
+
 def after(value, *others):
     return lax.optimization_barrier((value, *others))[0]
 
@@ -289,12 +359,12 @@
     return sent[0], block, sent[1], sent[2]
 
 
-def near_step(own, size):
+def near_step(own, low, middle, size):
     return (
         shifted(own, 1, size),
         shifted(own, -1, size),
-        shifted(own[:2], 2, size),
-        shifted(own[1:3], -2, size),
+        shifted(low, 2, size),
+        shifted(middle, -2, size),
     )
 
 
@@ -316,45 +386,38 @@
     width = key_weight.shape[2]
 
     columns = source_columns(source, source_gain[None], key_weight, value_weight, quarters)
-    columns = columns.reshape(quarters * 2, LAYERS * width, -1)
+    columns = columns.reshape(quarters * 2, 3 * width, -1)
     held = exchange(columns, GROUP)
-    blocks = [
-        held[:, layer * width : (layer + 1) * width].reshape(1, HD, -1) for layer in range(LAYERS)
-    ]
-    near, far = [], []
-    pieces = stride_step(blocks[0], stages // 4, stages)
-    own = join(*pieces)
-    pieces = near_step(own, stages)
-    far_own = swap(own)
-    rest = join(*pieces)
-    far_rest = swap(rest)
-    near.append((own, rest))
-    far.append((far_own, far_rest))
+    first, later = split(held)
+    pieces = stride_step(first, stages // 4, stages)
+    own, low, middle = join_four(*pieces)
+    pieces = near_step(own, low, middle, stages)
+    near = join(own, *pieces)
+    far = swap(near)
     normed = after(first_norm(target, query_gain, chips), held)
     query_other = swap(query_weight)
     out_other = swap(out_weight)
-
-    residual = target
-    for layer in range(LAYERS):
-        rows = exchange(normed, CHIPS)
-        mine = project_queries(layer, core, rows, query_weight, query_other, quarters)
-        queries = exchange(mine, "quarter")
-        parts = attend(core, queries, near[layer], far[layer])
-        if layer == 0:
-            pieces = stride_step(after(blocks[1], parts), stages // 4, stages)
-        parts = exchange(parts, "quarter")
-        projected = merge_and_project(layer, core, parts, out_weight, out_other, chips)
-        if layer == 0:
-            own = join(*after(pieces, projected))
-            pieces = near_step(own, stages)
-        arrived = exchange(projected, CHIPS)
-        done = finish(layer, arrived, residual, out_gain, query_gain)
-        residual = done[0]
-        normed = done[-1]
-        if layer == 0:
-            whole = join(own, *after(pieces, normed))
-            far.append((swap(whole),))
-            near.append((whole,))
+    near_later = lax.all_gather(after(later, near), "sp", axis=0, tiled=True)
+
+    rows = exchange(normed, CHIPS)
+    mine = project_queries(0, core, rows, query_weight, query_other, quarters, pltpu.HBM)
+    queries = exchange(mine, "quarter")
+    (parts,) = attend(core, [queries], [near], [far])
+    parts, out_other = lax.optimization_barrier((parts, out_other))
+    parts = exchange(parts, "quarter")
+    projected = merge_and_project(0, core, [parts], out_weight, out_other, chips)
+    arrived = exchange(projected, CHIPS)
+    residual, normed = finish(0, arrived, target, out_gain, query_gain)
+
+    rows = exchange(normed, CHIPS)
+    far_later = swap(near_later)
+    mine = project_queries(1, core, rows, query_weight, query_other, 1, pltpu.VMEM)
+    theirs = beside(mine, quarters)
+    kept, sent = attend(core, [mine, theirs], [near_later], [far_later])
+    came = beside(sent, quarters)
+    projected = merge_and_project(1, core, [kept, came], out_weight, out_other, chips)
+    arrived = exchange(projected, CHIPS)
+    (residual,) = finish(1, arrived, residual, out_gain, query_gain)
     return residual
 
 

time: 268 us -> 274 us (1.022)
  blocking collectives: 30.3 us -> 124 us
  starting transfers between devices: 151 us -> 61.4 us
  between operations: 0.31 us -> 13.6 us
  Pallas kernels: 30.3 us -> 22.5 us
    all_to_all x2 -> x5, blocking collectives: 30.3 us -> 124 us  [exchange(): return lax.all_to_all(value, axis, split_axis=0, concat_axis=0, tiled=True)]
    all_to_all x7 -> x2, starting transfers between devices: 75.3 us -> 10.3 us  [exchange(): return lax.all_to_all(value, axis, split_axis=0, concat_axis=0, tiled=True)]
    ppermute x14 -> x7, starting transfers between devices: 53.1 us -> 25.3 us  [shifted(): lax.ppermute(value, 'sp', [(z, (z + distance) % size) for z in range(size)])]
    all_gather x0 -> x1, waiting for transfers between devices: none -> 12.2 us  [layers(): near_later = lax.all_gather(after(later, near), 'sp', axis=0, tiled=True)]
    ppermute x14 -> x7, waiting for transfers between devices: 26.4 us -> 16.1 us  [shifted(): lax.ppermute(value, 'sp', [(z, (z + distance) % size) for z in range(size)])]
    ppermute x0 -> x2, waiting for transfers between devices: none -> 6.25 us  [beside(): return lax.ppermute(value, 'quarter', [(q, q ^ 1) for q in range(quarters)])]
    all_to_all x7 -> x2, waiting for transfers between devices: 19 us -> 13.7 us  [exchange(): return lax.all_to_all(value, axis, split_axis=0, concat_axis=0, tiled=True)]
    pallas_call x2, Pallas kernels: 5.25 us -> 1.11 us  [merge_and_project(): pl.pallas_call(functools.partial(merge_kernel, layer), in_specs=[pl.Block...]
  transfers between devices with their start and end apart: 26 -> 16, of which waited for: 12 -> 7; matrix products, arithmetic and copies ran while one was open for 0% -> 0% of each run, Pallas kernels for 6% -> 4%
where the time goes in v4:
time: 274 us; the launch traced here: 271 us
  blocking collectives  124 us (45%)
  starting transfers between devices  61.4 us (22%)
  waiting for transfers between devices  48.3 us (18%)
  Pallas kernels  22.5 us (8%)
  between operations  13.6 us (5%)
    all_to_all x5, blocking collectives, exchange(): return lax.all_to_all(value, axis, split_axis=0, concat_axis=0, tiled=True)  124 us
    ppermute x7, starting transfers between devices, shifted(): lax.ppermute(value, 'sp', [(z, (z + distance) % size) for z in range(size)])  25.3 us
    ppermute x4, starting transfers between devices, swap(): return lax.ppermute(value, 'core', [(0, 1), (1, 0)])  21.8 us
    ppermute x7, waiting for transfers between devices, shifted(): lax.ppermute(value, 'sp', [(z, (z + distance) % size) for z in range(size)])  16.1 us
    all_to_all x2, waiting for transfers between devices, exchange(): return lax.all_to_all(value, axis, split_axis=0, concat_axis=0, tiled=True)  13.7 us
    all_gather x1, waiting for transfers between devices, layers(): near_later = lax.all_gather(after(later, near), 'sp', axis=0, tiled=True)  12.2 us
    all_to_all x2, starting transfers between devices, exchange(): return lax.all_to_all(value, axis, split_axis=0, concat_axis=0, tiled=True)  10.3 us
    pallas_call x2, Pallas kernels, attend(): pl.pallas_call(functools.partial(attend_kernel, groups, len(mine)), in_sp...  7.93 us
  transfers between devices with their start and end apart: 16, of which 7 were waited for; matrix products, arithmetic and copies ran while one was open for 0% of the time, Pallas kernels for 4%

profile of v4, /device:TPU:65, one launch (start us, length us, event | category | flops | bytes accessed | tf_op | source)
XLA Modules:
  0.0 270.5 jit_solution(15656482752556823858)
XLA Ops:
  6.6 4.5 %source_columns.1 = bf16[4,2,96,128]{3,2,1,0:T(8,128)(2,1)} custom-call(bf16[512,2048]{1,0:T(8,128)(2,1)} %source_ref.1, f32[1,2048]{1,0:T(1,128)} %bitcast.8, bf16[2,32,2048]{2,1,0:T(8,128)(2,1)} %bitcast.6, bf16[2,32,2048]{2,1,0:T(8,128)(2,1)} %bitcast.7), custom_call_target="tpu_custom_call" | custom-call | tf_op jit(solution)/shard_map/source_columns/pallas_call | solution.py:78
  11.0 51.4 %all_to_all.35.held_ref = bf16[8,96,128]{2,1,0:T(8,128)(2,1)S(1)} all-to-all(bf16[8,96,128]{2,1,0:T(8,128)(2,1)} %bitcast.5), channel_id=1, replica_groups=mesh['grp'=2,'sp'=16,'kv'=2,'quarter'=4,'core'=2] {'quarter','core'}, dimensions={0} | all-to-all | bytes 393216 | tf_op jit(solution)/shard_map/all_to_all | solution.py:338
  63.1 2.1 collective-permute-start.1
  65.2 7.3 %collective-permute-start.2 = (bf16[1,256,128]{2,1,0:T(8,128)(2,1)S(1)}, bf16[1,256,128]{2,1,0:T(8,128)(2,1)S(1)}, u32[]{:S(2)}, u32[]{:S(2)}) collective-permute-start(bf16[1,256,128]{2,1,0:T(8,128)(2,1)S(1)} %get-tuple-element.19.refs_1_), channel_id=1, source_target_pairs={{0,192},{16,208},{32,224},{48,240},{64,0},{80,16},{96,32},{112,48}... | collective-permute-start | bytes 196616 | tf_op jit(solution)/shard_map/ppermute | solution.py:342
  74.5 13.8 %collective-permute-done.3.refs_3_ = bf16[1,256,128]{2,1,0:T(8,128)(2,1)S(1)} collective-permute-done((bf16[1,256,128]{2,1,0:T(8,128)(2,1)S(1)}, bf16[1,256,128]{2,1,0:T(8,128)(2,1)S(1)}, u32[]{:S(2)}, u32[]{:S(2)}) %collective-permute-start.3) | collective-permute-done | bytes 65568 | tf_op jit(solution)/shard_map/ppermute | solution.py:342
  90.3 4.6 %collective-permute-start.5 = (bf16[4,256,128]{2,1,0:T(8,128)(2,1)S(1)}, bf16[4,256,128]{2,1,0:T(8,128)(2,1)S(1)}, u32[]{:S(2)}, u32[]{:S(2)}) collective-permute-start(bf16[4,256,128]{2,1,0:T(8,128)(2,1)S(1)} %get-tuple-element.20.refs_0_), channel_id=1, source_target_pairs={{0,240},{16,0},{32,16},{48,32},{64,48},{80,64},{96,80},{112,96},{1... | collective-permute-start | bytes 786440 | tf_op jit(solution)/shard_map/ppermute | solution.py:342
  96.8 5.5 %collective-permute-start.7 = (bf16[2,256,128]{2,1,0:T(8,128)(2,1)S(1)}, bf16[2,256,128]{2,1,0:T(8,128)(2,1)S(1)}, u32[]{:S(2)}, u32[]{:S(2)}) collective-permute-start(bf16[2,256,128]{2,1,0:T(8,128)(2,1)S(1)} %get-tuple-element.22), channel_id=1, source_target_pairs={{0,224},{16,240},{32,0},{48,16},{64,32},{80,48},{96,64},{112,80},{... | collective-permute-start | bytes 393224 | tf_op jit(solution)/shard_map/ppermute | solution.py:342
  105.8 6.0 %collective-permute-start = (bf16[2,2048,128]{2,1,0:T(8,128)(2,1)S(1)}, bf16[2,2048,128]{2,1,0:T(8,128)(2,1)}, u32[]{:S(2)}, u32[]{:S(2)}) collective-permute-start(bf16[2,2048,128]{2,1,0:T(8,128)(2,1)S(1)} %copy-done), channel_id=1, source_target_pairs={{0,1},{1,0},{2,3},{3,2},{4,5},{5,4},{6,7},{7,6},{8,9},{9,8},{10,11... | collective-permute-start | bytes 3145736 | tf_op jit(solution)/shard_map/ppermute | solution.py:346
  112.7 6.2 %all-to-all-start.1 = ((bf16[8,16,2048]{2,1,0:T(8,128)(2,1)}), bf16[8,16,2048]{2,1,0:T(8,128)(2,1)}, u32[]{:S(2)}, u32[]{:S(2)}) async-start(bf16[8,16,2048]{2,1,0:T(8,128)(2,1)} %first_norm.1), calls=%async_computation.1 | async-start | bytes 1048576 | tf_op jit(solution)/shard_map/all_to_all | solution.py:338
  119.0 2.2 collective-permute-start.8
  121.2 2.2 collective-permute-start.9
  123.4 13.7 %all-to-all-done.1.rows_ref = bf16[8,16,2048]{2,1,0:T(8,128)(2,1)} async-done(((bf16[8,16,2048]{2,1,0:T(8,128)(2,1)}), bf16[8,16,2048]{2,1,0:T(8,128)(2,1)}, u32[]{:S(2)}, u32[]{:S(2)}) %all-to-all-start.1) | async-done | bytes 524320 | tf_op jit(solution)/shard_map/all_to_all | solution.py:338
  137.1 2.5 project_queries.2
  139.7 10.5 %all_to_all.36.refs_0_ = bf16[4,128,256]{2,1,0:T(8,128)(2,1)S(1)} all-to-all(bf16[4,128,256]{2,1,0:T(8,128)(2,1)} %project_queries.2), channel_id=1, replica_groups=mesh['grp'=2,'sp'=16,'kv'=2,'quarter'=4,'core'=2] {'quarter'}, dimensions={0} | all-to-all | bytes 524288 | tf_op jit(solution)/shard_map/all_to_all | solution.py:338
  150.2 3.9 %attend.2 = bf16[4,144,256]{2,1,0:T(8,128)(2,1)S(1)} custom-call(s32[1]{0:T(128)} %bitcast.core_ref, bf16[4,128,256]{2,1,0:T(8,128)(2,1)S(1)} %all_to_all.36.refs_0_, bf16[16,256,128]{2,1,0:T(8,128)(2,1)} %join.1.refs_1_, bf16[16,256,128]{2,1,0:T(8,128)(2,1)} %collective-permute-done.8.refs_2_), custom_call_target="tpu_custom_call" | custom-call | tf_op jit(solution)/shard_map/attend/pallas_call | solution.py:192
  154.8 4.1 %all-to-all-start.3 = ((bf16[4,144,256]{2,1,0:T(8,128)(2,1)}), bf16[4,144,256]{2,1,0:T(8,128)(2,1)S(1)}, u32[]{:S(2)}, u32[]{:S(2)}) async-start(bf16[4,144,256]{2,1,0:T(8,128)(2,1)} %copy-done.3), calls=%async_computation.3 | async-start | bytes 589824 | tf_op jit(solution)/shard_map/all_to_all | solution.py:338
  158.9 12.2 %all-gather.2.cloned.1.call-done.refs_2_ = bf16[32,256,128]{2,1,0:T(8,128)(2,1)} async-done(((bf16[2,256,128]{2,1,0:T(8,128)(2,1)}), bf16[32,256,128]{2,1,0:T(8,128)(2,1)}) %all-gather.2.cloned.1.call-update) | async-done | bytes 2097168 | tf_op jit(solution)/shard_map/all_gather | solution.py:400
  171.1 11.5 %collective-permute-start.11 = (bf16[32,256,128]{2,1,0:T(8,128)(2,1)}, bf16[32,256,128]{2,1,0:T(8,128)(2,1)}, u32[]{:S(2)}, u32[]{:S(2)}) collective-permute-start(bf16[32,256,128]{2,1,0:T(8,128)(2,1)} %all-gather.2.cloned.1.call-done.refs_2_), channel_id=1, source_target_pairs={{0,1},{1,0},{2,3},{3,2},{4,5},{5,4},{6,7},{7,6},{8,9},{9,8},{10,11... | collective-permute-start | bytes 6291464 | tf_op jit(solution)/shard_map/ppermute | solution.py:346
  183.2 24.4 %all_to_all.37.part_ref = bf16[8,16,2048]{2,1,0:T(8,128)(2,1)S(1)} all-to-all(bf16[8,16,2048]{2,1,0:T(8,128)(2,1)S(1)} %merge_and_project.2), channel_id=1, replica_groups=mesh['grp'=2,'sp'=16,'kv'=2,'quarter'=4,'core'=2] {'kv','quarter'}, dimensions={0} | all-to-all | bytes 1048576 | tf_op jit(solution)/shard_map/all_to_all | solution.py:338
  208.7 21.7 %all_to_all.38.rows_ref = bf16[8,16,2048]{2,1,0:T(8,128)(2,1)} all-to-all(bf16[8,16,2048]{2,1,0:T(8,128)(2,1)} %get-tuple-element.25), channel_id=1, replica_groups=mesh['grp'=2,'sp'=16,'kv'=2,'quarter'=4,'core'=2] {'kv','quarter'}, dimensions={0} | all-to-all | bytes 1048576 | tf_op jit(solution)/shard_map/all_to_all | solution.py:338
  234.1 3.1 %collective-permute-done.10.refs_1_ = bf16[1,128,256]{2,1,0:T(8,128)(2,1)S(1)} collective-permute-done((bf16[1,128,256]{2,1,0:T(8,128)(2,1)S(1)}, bf16[1,128,256]{2,1,0:T(8,128)(2,1)S(1)}, u32[]{:S(2)}, u32[]{:S(2)}) %collective-permute-start.10) | collective-permute-done | bytes 65568 | tf_op jit(solution)/shard_map/ppermute | solution.py:350
  237.2 4.1 %attend.3 = (bf16[1,144,256]{2,1,0:T(8,128)(2,1)S(1)}, bf16[1,144,256]{2,1,0:T(8,128)(2,1)S(1)}) custom-call(s32[1]{0:T(128)} %bitcast.core_ref, bf16[1,128,256]{2,1,0:T(8,128)(2,1)S(1)} %project_queries.3.refs_0_, bf16[1,128,256]{2,1,0:T(8,128)(2,1)S(1)} %collective-permute-done.10.refs_1_, bf16[32,256,128]{2,1,0:T(8,128)(2,1)S(1)} %copy-done.2, ...), custom_call_target="tpu_custom_call" | custom-call | tf_op jit(solution)/shard_map/attend/pallas_call | solution.py:192
  243.3 3.2 %collective-permute-done.12.refs_1_ = bf16[1,144,256]{2,1,0:T(8,128)(2,1)S(1)} collective-permute-done((bf16[1,144,256]{2,1,0:T(8,128)(2,1)S(1)}, bf16[1,144,256]{2,1,0:T(8,128)(2,1)S(1)}, u32[]{:S(2)}, u32[]{:S(2)}) %collective-permute-start.12) | collective-permute-done | bytes 73760 | tf_op jit(solution)/shard_map/ppermute | solution.py:350
  247.0 15.9 %all_to_all.39.part_ref = bf16[8,16,2048]{2,1,0:T(8,128)(2,1)S(1)} all-to-all(bf16[8,16,2048]{2,1,0:T(8,128)(2,1)S(1)} %merge_and_project.3), channel_id=1, replica_groups=mesh['grp'=2,'sp'=16,'kv'=2,'quarter'=4,'core'=2] {'kv','quarter'}, dimensions={0} | all-to-all | bytes 1048576 | tf_op jit(solution)/shard_map/all_to_all | solution.py:338
  (41 shorter events, 20.5 us)
Async XLA Ops:
  6.5 164.5 %all-gather.2.cloned.1.call-start = ((), (), s32[]{:S(2)}) async-start(), calls=%async_computation.7 | async-start | bytes 2228224 | tf_op jit(solution)/shard_map/all_gather | solution.py:400
  11.0 94.8 %copy-start = (bf16[2,2048,128]{2,1,0:T(8,128)(2,1)S(1)}, bf16[2,2048,128]{2,1,0:T(8,128)(2,1)}, u32[]{:S(2)}) copy-start(bf16[2,2048,128]{2,1,0:T(8,128)(2,1)} %mine_ref.3) | copy-start | bytes 3145732
  11.0 100.7 %copy-start.4 = (bf16[16,2048]{1,0:T(8,128)(2,1)S(1)}, bf16[16,2048]{1,0:T(8,128)(2,1)}, u32[]{:S(2)}) copy-start(bf16[16,2048]{1,0:T(8,128)(2,1)} %residual_ref.1) | copy-start | bytes 196612
  11.0 100.8 %copy-start.5 = (f32[2,2048]{1,0:T(2,128)S(1)}, f32[2,2048]{1,0:T(2,128)}, u32[]{:S(2)}) copy-start(f32[2,2048]{1,0:T(2,128)} %query_gain_ref.3) | copy-start | bytes 49156
  63.1 58.1 %copy-start.1 = (bf16[2,128,2048]{2,1,0:T(8,128)(2,1)S(1)}, bf16[2,128,2048]{2,1,0:T(8,128)(2,1)}, u32[]{:S(2)}) copy-start(bf16[2,128,2048]{2,1,0:T(8,128)(2,1)} %refs_2_.1) | copy-start | bytes 3145732
  63.1 11.3 %collective-permute-start.1 = (bf16[1,256,128]{2,1,0:T(8,128)(2,1)S(1)}, bf16[1,256,128]{2,1,0:T(8,128)(2,1)S(1)}, u32[]{:S(2)}, u32[]{:S(2)}) collective-permute-start(bf16[1,256,128]{2,1,0:T(8,128)(2,1)S(1)} %get-tuple-element.19.refs_1_), channel_id=1, source_target_pairs={{0,64},{16,80},{32,96},{48,112},{64,128},{80,144},{96,160},{112,17... | collective-permute-start | bytes 196616 | tf_op jit(solution)/shard_map/ppermute | solution.py:342
  65.2 9.3 %collective-permute-start.2 = (bf16[1,256,128]{2,1,0:T(8,128)(2,1)S(1)}, bf16[1,256,128]{2,1,0:T(8,128)(2,1)S(1)}, u32[]{:S(2)}, u32[]{:S(2)}) collective-permute-start(bf16[1,256,128]{2,1,0:T(8,128)(2,1)S(1)} %get-tuple-element.19.refs_1_), channel_id=1, source_target_pairs={{0,192},{16,208},{32,224},{48,240},{64,0},{80,16},{96,32},{112,48}... | collective-permute-start | bytes 196616 | tf_op jit(solution)/shard_map/ppermute | solution.py:342
  72.5 15.7 %collective-permute-start.3 = (bf16[1,256,128]{2,1,0:T(8,128)(2,1)S(1)}, bf16[1,256,128]{2,1,0:T(8,128)(2,1)S(1)}, u32[]{:S(2)}, u32[]{:S(2)}) collective-permute-start(bf16[1,256,128]{2,1,0:T(8,128)(2,1)S(1)} %get-tuple-element.19.refs_1_), channel_id=1, source_target_pairs={{0,128},{16,144},{32,160},{48,176},{64,192},{80,208},{96,224},{112... | collective-permute-start | bytes 196616 | tf_op jit(solution)/shard_map/ppermute | solution.py:342
  88.3 16.3 %collective-permute-start.4 = (bf16[4,256,128]{2,1,0:T(8,128)(2,1)S(1)}, bf16[4,256,128]{2,1,0:T(8,128)(2,1)S(1)}, u32[]{:S(2)}, u32[]{:S(2)}) collective-permute-start(bf16[4,256,128]{2,1,0:T(8,128)(2,1)S(1)} %get-tuple-element.20.refs_0_), channel_id=1, source_target_pairs={{0,16},{16,32},{32,48},{48,64},{64,80},{80,96},{96,112},{112,128},... | collective-permute-start | bytes 786440 | tf_op jit(solution)/shard_map/ppermute | solution.py:342
  90.3 14.4 %collective-permute-start.5 = (bf16[4,256,128]{2,1,0:T(8,128)(2,1)S(1)}, bf16[4,256,128]{2,1,0:T(8,128)(2,1)S(1)}, u32[]{:S(2)}, u32[]{:S(2)}) collective-permute-start(bf16[4,256,128]{2,1,0:T(8,128)(2,1)S(1)} %get-tuple-element.20.refs_0_), channel_id=1, source_target_pairs={{0,240},{16,0},{32,16},{48,32},{64,48},{80,64},{96,80},{112,96},{1... | collective-permute-start | bytes 786440 | tf_op jit(solution)/shard_map/ppermute | solution.py:342
  94.9 9.1 %collective-permute-start.6 = (bf16[2,256,128]{2,1,0:T(8,128)(2,1)S(1)}, bf16[2,256,128]{2,1,0:T(8,128)(2,1)S(1)}, u32[]{:S(2)}, u32[]{:S(2)}) collective-permute-start(bf16[2,256,128]{2,1,0:T(8,128)(2,1)S(1)} %get-tuple-element.21), channel_id=1, source_target_pairs={{0,32},{16,48},{32,64},{48,80},{64,96},{80,112},{96,128},{112,144}... | collective-permute-start | bytes 393224 | tf_op jit(solution)/shard_map/ppermute | solution.py:342
  96.8 7.8 %collective-permute-start.7 = (bf16[2,256,128]{2,1,0:T(8,128)(2,1)S(1)}, bf16[2,256,128]{2,1,0:T(8,128)(2,1)S(1)}, u32[]{:S(2)}, u32[]{:S(2)}) collective-permute-start(bf16[2,256,128]{2,1,0:T(8,128)(2,1)S(1)} %get-tuple-element.22), channel_id=1, source_target_pairs={{0,224},{16,240},{32,0},{48,16},{64,32},{80,48},{96,64},{112,80},{... | collective-permute-start | bytes 393224 | tf_op jit(solution)/shard_map/ppermute | solution.py:342
  105.8 17.6 %collective-permute-start = (bf16[2,2048,128]{2,1,0:T(8,128)(2,1)S(1)}, bf16[2,2048,128]{2,1,0:T(8,128)(2,1)}, u32[]{:S(2)}, u32[]{:S(2)}) collective-permute-start(bf16[2,2048,128]{2,1,0:T(8,128)(2,1)S(1)} %copy-done), channel_id=1, source_target_pairs={{0,1},{1,0},{2,3},{3,2},{4,5},{5,4},{6,7},{7,6},{8,9},{9,8},{10,11... | collective-permute-start | bytes 3145736 | tf_op jit(solution)/shard_map/ppermute | solution.py:346
  112.7 24.4 %all-to-all-start.1 = ((bf16[8,16,2048]{2,1,0:T(8,128)(2,1)}), bf16[8,16,2048]{2,1,0:T(8,128)(2,1)}, u32[]{:S(2)}, u32[]{:S(2)}) async-start(bf16[8,16,2048]{2,1,0:T(8,128)(2,1)} %first_norm.1), calls=%async_computation.1 | async-start | bytes 1048576 | tf_op jit(solution)/shard_map/all_to_all | solution.py:338
  119.0 31.2 %collective-permute-start.8 = (bf16[16,256,128]{2,1,0:T(8,128)(2,1)}, bf16[16,256,128]{2,1,0:T(8,128)(2,1)}, u32[]{:S(2)}, u32[]{:S(2)}) collective-permute-start(bf16[16,256,128]{2,1,0:T(8,128)(2,1)} %join.1.refs_1_), channel_id=1, source_target_pairs={{0,1},{1,0},{2,3},{3,2},{4,5},{5,4},{6,7},{7,6},{8,9},{9,8},{10,11... | collective-permute-start | bytes 3145736 | tf_op jit(solution)/shard_map/ppermute | solution.py:346
  121.2 33.6 %collective-permute-start.9 = (bf16[2,128,2048]{2,1,0:T(8,128)(2,1)S(1)}, bf16[2,128,2048]{2,1,0:T(8,128)(2,1)S(1)}, u32[]{:S(2)}, u32[]{:S(2)}) collective-permute-start(bf16[2,128,2048]{2,1,0:T(8,128)(2,1)S(1)} %copy-done.1), channel_id=1, source_target_pairs={{0,1},{1,0},{2,3},{3,2},{4,5},{5,4},{6,7},{7,6},{8,9},{9,8},{10,11... | collective-permute-start | bytes 3145736 | tf_op jit(solution)/shard_map/ppermute | solution.py:346
  154.1 0.7 copy-start.3
  154.8 27.8 %all-to-all-start.3 = ((bf16[4,144,256]{2,1,0:T(8,128)(2,1)}), bf16[4,144,256]{2,1,0:T(8,128)(2,1)S(1)}, u32[]{:S(2)}, u32[]{:S(2)}) async-start(bf16[4,144,256]{2,1,0:T(8,128)(2,1)} %copy-done.3), calls=%async_computation.3 | async-start | bytes 589824 | tf_op jit(solution)/shard_map/all_to_all | solution.py:338
  158.9 48.7 %copy-start.6 = (f32[2,2048]{1,0:T(2,128)S(1)}, f32[2,2048]{1,0:T(2,128)}, u32[]{:S(2)}) copy-start(f32[2,2048]{1,0:T(2,128)} %out_gain_ref.3) | copy-start | bytes 49156
  171.1 66.1 %collective-permute-start.11 = (bf16[32,256,128]{2,1,0:T(8,128)(2,1)}, bf16[32,256,128]{2,1,0:T(8,128)(2,1)}, u32[]{:S(2)}, u32[]{:S(2)}) collective-permute-start(bf16[32,256,128]{2,1,0:T(8,128)(2,1)} %all-gather.2.cloned.1.call-done.refs_2_), channel_id=1, source_target_pairs={{0,1},{1,0},{2,3},{3,2},{4,5},{5,4},{6,7},{7,6},{8,9},{9,8},{10,11... | collective-permute-start | bytes 6291464 | tf_op jit(solution)/shard_map/ppermute | solution.py:346
  207.6 29.7 %copy-start.2 = (bf16[32,256,128]{2,1,0:T(8,128)(2,1)S(1)}, bf16[32,256,128]{2,1,0:T(8,128)(2,1)}, u32[]{:S(2)}) copy-start(bf16[32,256,128]{2,1,0:T(8,128)(2,1)} %all-gather.2.cloned.1.call-done.refs_2_) | copy-start | bytes 6291460
  232.2 5.0 %collective-permute-start.10 = (bf16[1,128,256]{2,1,0:T(8,128)(2,1)S(1)}, bf16[1,128,256]{2,1,0:T(8,128)(2,1)S(1)}, u32[]{:S(2)}, u32[]{:S(2)}) collective-permute-start(bf16[1,128,256]{2,1,0:T(8,128)(2,1)S(1)} %project_queries.3.refs_0_), channel_id=1, source_target_pairs={{0,2},{2,0},{4,6},{6,4},{1,3},{3,1},{5,7},{7,5},{8,10},{10,8},{12,... | collective-permute-start | bytes 196616 | tf_op jit(solution)/shard_map/ppermute | solution.py:350
  241.3 5.1 %collective-permute-start.12 = (bf16[1,144,256]{2,1,0:T(8,128)(2,1)S(1)}, bf16[1,144,256]{2,1,0:T(8,128)(2,1)S(1)}, u32[]{:S(2)}, u32[]{:S(2)}) collective-permute-start(bf16[1,144,256]{2,1,0:T(8,128)(2,1)S(1)} %get-tuple-element.29), channel_id=1, source_target_pairs={{0,2},{2,0},{4,6},{6,4},{1,3},{3,1},{5,7},{7,5},{8,10},{10,8},{12,... | collective-permute-start | bytes 221192 | tf_op jit(solution)/shard_map/ppermute | solution.py:350
Sparse Core Ops, SparseCore 0:
  105.9 65.1 all-gather.1

commit v5 on v4

--- a/solution.py
+++ b/solution.py
@@ -16,6 +16,7 @@
 
 CHIPS = ("kv", "quarter")
 GROUP = ("quarter", "core")
+STAGES = ("far", "near")
 BF16 = jnp.bfloat16
 F32 = jnp.float32
 
@@ -197,7 +198,7 @@
         scratch_shapes=[pltpu.VMEM((groups * heads * rows, span), F32)],
         compiler_params=pltpu.CompilerParams(vmem_limit_bytes=16384 * 1024),
         name="attend",
-    )(core, *held_in_vmem(*queries, *mine, *other))
+    )(core, *held_in_vmem(*queries), *[pltpu.with_memory_space_constraint(a, pltpu.HBM) for a in (*mine, *other)])
 
 
 def split_kernel(held_ref, first_ref, later_ref):
@@ -205,46 +206,42 @@
     width //= 3
     for device in range(devices):
         columns = slice(device * width, (device + 1) * width)
-        first_ref[0, columns, :] = held_ref[device, :width, :]
+        for peer in range(first_ref.shape[0]):
+            first_ref[peer, columns, :] = held_ref[device, :width, :]
         for half in range(2):
             at = width * (1 + half)
             later_ref[half, columns, :] = held_ref[device, at : at + width, :]
 
 
-def split(held):
+def split(held, copies):
     devices, width, block = held.shape
     column = devices * width // 3
     return pl.pallas_call(
         split_kernel,
         in_specs=in_vmem(1),
         out_specs=in_vmem(2),
-        out_shape=[vmem_out((1, column, block)), pltpu.HBM((2, column, block), BF16)],
+        out_shape=[pltpu.HBM((count, column, block), BF16) for count in (copies, 2)],
         compiler_params=pltpu.CompilerParams(vmem_limit_bytes=2048 * 1024),
         name="split",
     )(*held_in_vmem(held))
 
 
-def four_kernel(*refs):
-    pieces, (own_ref, low_ref, middle_ref) = refs[:4], refs[4:]
-    for at, ref in enumerate(pieces):
-        block = ref[0]
-        own_ref[at] = block
-        if at < 2:
-            low_ref[at] = block
-        if 1 <= at < 3:
-            middle_ref[at - 1] = block
-
-
-def join_four(*pieces):
-    shape = pieces[0].shape[1:]
-    return pl.pallas_call(
-        four_kernel,
-        in_specs=in_vmem(4),
-        out_specs=in_vmem(3),
-        out_shape=[vmem_out((count, *shape)) for count in (4, 2, 2)],
+def halves_kernel(own_ref, low_ref, high_ref):
+    count = low_ref.shape[0]
+    low_ref[...] = own_ref[:count]
+    high_ref[...] = own_ref[count:]
+
+
+def halves(own):
+    shape = (own.shape[0] // 2, *own.shape[1:])
+    return pl.pallas_call(
+        halves_kernel,
+        in_specs=in_vmem(1),
+        out_specs=in_vmem(2),
+        out_shape=[vmem_out(shape)] * 2,
         compiler_params=pltpu.CompilerParams(vmem_limit_bytes=2048 * 1024),
-        name="join_four",
-    )(*held_in_vmem(*pieces))
+        name="halves",
+    )(*held_in_vmem(own))
 
 
 def join_kernel(*refs):
@@ -260,7 +257,7 @@
         join_kernel,
         in_specs=in_vmem(len(pieces)),
         out_specs=in_vmem(1)[0],
-        out_shape=vmem_out((count, *pieces[0].shape[1:])),
+        out_shape=pltpu.HBM((count, *pieces[0].shape[1:]), BF16),
         compiler_params=pltpu.CompilerParams(vmem_limit_bytes=4096 * 1024),
         name="join",
     )(*held_in_vmem(*pieces))
@@ -339,7 +336,7 @@
 
 
 def shifted(value, distance, size):
-    return lax.ppermute(value, "sp", [(z, (z + distance) % size) for z in range(size)])
+    return lax.ppermute(value, STAGES, [(z, (z + distance) % size) for z in range(size)])
 
 
 def swap(value):
@@ -354,18 +351,9 @@
     return lax.optimization_barrier((value, *others))[0]
 
 
-def stride_step(block, stride, size):
-    sent = [shifted(block, distance, size) for distance in (stride, -stride, 2 * stride)]
-    return sent[0], block, sent[1], sent[2]
-
-
-def near_step(own, low, middle, size):
-    return (
-        shifted(own, 1, size),
-        shifted(own, -1, size),
-        shifted(low, 2, size),
-        shifted(middle, -2, size),
-    )
+def near_step(own, size):
+    low, high = halves(own)
+    return shifted(own, 1, size), shifted(own, -1, size), shifted(low, -2, size), shifted(high, 2, size)
 
 
 def layers(
@@ -381,26 +369,24 @@
 ):
     quarters = lax.axis_size("quarter")
     chips = quarters * lax.axis_size("kv")
-    stages = lax.axis_size("sp")
+    stages = lax.axis_size("far") * lax.axis_size("near")
     core = lax.axis_index("core").astype(jnp.int32).reshape(1)
     width = key_weight.shape[2]
 
     columns = source_columns(source, source_gain[None], key_weight, value_weight, quarters)
     columns = columns.reshape(quarters * 2, 3 * width, -1)
     held = exchange(columns, GROUP)
-    first, later = split(held)
-    pieces = stride_step(first, stages // 4, stages)
-    own, low, middle = join_four(*pieces)
-    pieces = near_step(own, low, middle, stages)
-    near = join(own, *pieces)
-    far = swap(near)
-    normed = after(first_norm(target, query_gain, chips), held)
+    first, later = split(held, lax.axis_size("far"))
+    own = exchange(first, "far")
+    normed = after(first_norm(target, query_gain, chips), own)
+    pieces = near_step(own, stages)
     query_other = swap(query_weight)
     out_other = swap(out_weight)
-    near_later = lax.all_gather(after(later, near), "sp", axis=0, tiled=True)
-
     rows = exchange(normed, CHIPS)
     mine = project_queries(0, core, rows, query_weight, query_other, quarters, pltpu.HBM)
+    near_later = lax.all_gather(after(later, mine), STAGES, axis=0, tiled=True)
+    near = join(own, *after(pieces, mine))
+    far = swap(near)
     queries = exchange(mine, "quarter")
     (parts,) = attend(core, [queries], [near], [far])
     parts, out_other = lax.optimization_barrier((parts, out_other))
@@ -423,15 +409,16 @@
 
 def solution(mesh):
     groups, stages, devices = mesh.devices.shape
+    near = 4
     own = Mesh(
-        mesh.devices.reshape(groups, stages, KVH, devices // (2 * KVH), 2),
-        ("grp", "sp", "kv", "quarter", "core"),
+        mesh.devices.reshape(groups, stages // near, near, KVH, devices // (2 * KVH), 2),
+        ("grp", "far", "near", "kv", "quarter", "core"),
     )
-    every = ("grp", "sp", "kv", "quarter", "core")
+    every = ("grp", "far", "near", "kv", "quarter", "core")
     tp = ("kv", "quarter", "core")
     in_specs = (
         P(every, None),
-        P(("grp", "sp"), None),
+        P(("grp", "far", "near"), None),
         P(),
         P(),
         P(),

time: 274 us -> 273 us (level)
  waiting for transfers between devices: 48.3 us -> 42.6 us
  local copies, waits for them, and re-layouts: 0.75 us -> 4.77 us
    all_to_all x2 -> x3, waiting for transfers between devices: 13.7 us -> 20.3 us  [exchange(): return lax.all_to_all(value, axis, split_axis=0, concat_axis=0, tiled=True)]
    ppermute x7 -> x4, waiting for transfers between devices: 16.1 us -> 9.53 us  [shifted(): lax.ppermute(value, STAGES, [(z, (z + distance) % size) for z in range(si...]
    all_gather x1, waiting for transfers between devices: 12.2 us -> 6.43 us  [layers(): near_later = lax.all_gather(after(later, mine), STAGES, axis=0, tiled=True)]
    unnamed x14 -> x24, local copies, waits for them, and re-layouts: 0.75 us -> 4.77 us
    all_to_all x2 -> x3, starting transfers between devices: 10.3 us -> 12.6 us  [exchange(): return lax.all_to_all(value, axis, split_axis=0, concat_axis=0, tiled=True)]
    ppermute x7 -> x4, starting transfers between devices: 25.3 us -> 27.1 us  [shifted(): lax.ppermute(value, STAGES, [(z, (z + distance) % size) for z in range(si...]
  transfers between devices with their start and end apart: 16 -> 14, of which waited for: 7 -> 7; matrix products, arithmetic and copies ran while one was open for 0% -> 0% of each run, Pallas kernels for 4% -> 3%
where the time goes in v5:
time: 273 us; the launch traced here: 270 us
  blocking collectives  122 us (45%)
  starting transfers between devices  64.1 us (23%)
  waiting for transfers between devices  42.6 us (16%)
  Pallas kernels  22.7 us (8%)
  between operations  13.7 us (5%)
  local copies, waits for them, and re-layouts  4.77 us (2%)
    all_to_all x5, blocking collectives, exchange(): return lax.all_to_all(value, axis, split_axis=0, concat_axis=0, tiled=True)  122 us
    ppermute x4, starting transfers between devices, shifted(): lax.ppermute(value, STAGES, [(z, (z + distance) % size) for z in range(si...  27.1 us
    ppermute x4, starting transfers between devices, swap(): return lax.ppermute(value, 'core', [(0, 1), (1, 0)])  20.4 us
    all_to_all x3, waiting for transfers between devices, exchange(): return lax.all_to_all(value, axis, split_axis=0, concat_axis=0, tiled=True)  20.3 us
    all_to_all x3, starting transfers between devices, exchange(): return lax.all_to_all(value, axis, split_axis=0, concat_axis=0, tiled=True)  12.6 us
    ppermute x4, waiting for transfers between devices, shifted(): lax.ppermute(value, STAGES, [(z, (z + distance) % size) for z in range(si...  9.53 us
    pallas_call x2, Pallas kernels, attend(): pl.pallas_call(functools.partial(attend_kernel, groups, len(mine)), in_sp...  8.57 us
    all_gather x1, waiting for transfers between devices, layers(): near_later = lax.all_gather(after(later, mine), STAGES, axis=0, tiled=True)  6.43 us
  transfers between devices with their start and end apart: 14, of which 7 were waited for; matrix products, arithmetic and copies ran while one was open for 0% of the time, Pallas kernels for 3%

profile of v5, /device:TPU:65, one launch (start us, length us, event | category | flops | bytes accessed | tf_op | source)
XLA Modules:
  0.0 269.5 jit_solution(2295986153403365970)
XLA Ops:
  6.6 4.6 %source_columns.1 = bf16[4,2,96,128]{3,2,1,0:T(8,128)(2,1)} custom-call(bf16[512,2048]{1,0:T(8,128)(2,1)} %source_ref.1, f32[1,2048]{1,0:T(1,128)} %bitcast.8, bf16[2,32,2048]{2,1,0:T(8,128)(2,1)} %bitcast.6, bf16[2,32,2048]{2,1,0:T(8,128)(2,1)} %bitcast.7), custom_call_target="tpu_custom_call" | custom-call | tf_op jit(solution)/shard_map/source_columns/pallas_call | solution.py:79
  11.1 51.3 %all_to_all.40.held_ref = bf16[8,96,128]{2,1,0:T(8,128)(2,1)S(1)} all-to-all(bf16[8,96,128]{2,1,0:T(8,128)(2,1)} %bitcast.5), channel_id=1, replica_groups=mesh['grp'=2,'far'=4,'near'=4,'kv'=2,'quarter'=4,'core'=2] {'quarter','c..., dimensions={0} | all-to-all | bytes 393216 | tf_op jit(solution)/shard_map/all_to_all | solution.py:335
  63.2 3.5 %all-to-all-start.1 = ((bf16[4,256,128]{2,1,0:T(8,128)(2,1)}), bf16[4,256,128]{2,1,0:T(8,128)(2,1)S(1)}, u32[]{:S(2)}, u32[]{:S(2)}) async-start(bf16[4,256,128]{2,1,0:T(8,128)(2,1)} %get-tuple-element.21), calls=%async_computation.1 | async-start | bytes 524288 | tf_op jit(solution)/shard_map/all_to_all | solution.py:335
  66.7 3.8 %collective-permute-start = (bf16[2,2048,128]{2,1,0:T(8,128)(2,1)S(1)}, bf16[2,2048,128]{2,1,0:T(8,128)(2,1)S(1)}, u32[]{:S(2)}, u32[]{:S(2)}) collective-permute-start(bf16[2,2048,128]{2,1,0:T(8,128)(2,1)S(1)} %copy-done), channel_id=1, source_target_pairs={{0,1},{1,0},{2,3},{3,2},{4,5},{5,4},{6,7},{7,6},{8,9},{9,8},{10,11... | collective-permute-start | bytes 3145736 | tf_op jit(solution)/shard_map/ppermute | solution.py:343
  71.5 8.3 %all-to-all-done.1.own_ref.refs_0_ = bf16[4,256,128]{2,1,0:T(8,128)(2,1)S(1)} async-done(((bf16[4,256,128]{2,1,0:T(8,128)(2,1)}), bf16[4,256,128]{2,1,0:T(8,128)(2,1)S(1)}, u32[]{:S(2)}, u32[]{:S(2)}) %all-to-all-start.1) | async-done | bytes 262176 | tf_op jit(solution)/shard_map/all_to_all | solution.py:335
  79.8 4.5 %all-to-all-start.2 = ((bf16[8,16,2048]{2,1,0:T(8,128)(2,1)}), bf16[8,16,2048]{2,1,0:T(8,128)(2,1)S(1)}, u32[]{:S(2)}, u32[]{:S(2)}) async-start(bf16[8,16,2048]{2,1,0:T(8,128)(2,1)} %first_norm.1), calls=%async_computation.2 | async-start | bytes 1048576 | tf_op jit(solution)/shard_map/all_to_all | solution.py:335
  84.3 12.1 %all-to-all-done.2.rows_ref = bf16[8,16,2048]{2,1,0:T(8,128)(2,1)S(1)} async-done(((bf16[8,16,2048]{2,1,0:T(8,128)(2,1)}), bf16[8,16,2048]{2,1,0:T(8,128)(2,1)S(1)}, u32[]{:S(2)}, u32[]{:S(2)}) %all-to-all-start.2) | async-done | bytes 524320 | tf_op jit(solution)/shard_map/all_to_all | solution.py:335
  97.1 2.3 project_queries.2
  101.6 18.7 %collective-permute-start.2 = (bf16[4,256,128]{2,1,0:T(8,128)(2,1)S(1)}, bf16[4,256,128]{2,1,0:T(8,128)(2,1)S(1)}, u32[]{:S(2)}, u32[]{:S(2)}) collective-permute-start(bf16[4,256,128]{2,1,0:T(8,128)(2,1)S(1)} %all-to-all-done.1.own_ref.refs_0_), channel_id=1, source_target_pairs={{0,240},{16,0},{32,16},{48,32},{64,48},{80,64},{96,80},{112,96},{1... | collective-permute-start | bytes 786440 | tf_op jit(solution)/shard_map/ppermute | solution.py:339
  120.3 3.1 %collective-permute-start.3 = (bf16[2,256,128]{2,1,0:T(8,128)(2,1)S(1)}, bf16[2,256,128]{2,1,0:T(8,128)(2,1)S(1)}, u32[]{:S(2)}, u32[]{:S(2)}) collective-permute-start(bf16[2,256,128]{2,1,0:T(8,128)(2,1)S(1)} %get-tuple-element.23), channel_id=1, source_target_pairs={{0,224},{16,240},{32,0},{48,16},{64,32},{80,48},{96,64},{112,80},{... | collective-permute-start | bytes 393224 | tf_op jit(solution)/shard_map/ppermute | solution.py:339
  123.5 3.1 %collective-permute-start.4 = (bf16[2,256,128]{2,1,0:T(8,128)(2,1)S(1)}, bf16[2,256,128]{2,1,0:T(8,128)(2,1)S(1)}, u32[]{:S(2)}, u32[]{:S(2)}) collective-permute-start(bf16[2,256,128]{2,1,0:T(8,128)(2,1)S(1)} %get-tuple-element.24), channel_id=1, source_target_pairs={{0,32},{16,48},{32,64},{48,80},{64,96},{80,112},{96,128},{112,144}... | collective-permute-start | bytes 393224 | tf_op jit(solution)/shard_map/ppermute | solution.py:339
  126.6 9.0 %collective-permute-done.3.refs_3_ = bf16[2,256,128]{2,1,0:T(8,128)(2,1)S(1)} collective-permute-done((bf16[2,256,128]{2,1,0:T(8,128)(2,1)S(1)}, bf16[2,256,128]{2,1,0:T(8,128)(2,1)S(1)}, u32[]{:S(2)}, u32[]{:S(2)}) %collective-permute-start.3) | collective-permute-done | bytes 131104 | tf_op jit(solution)/shard_map/ppermute | solution.py:339
  137.2 3.7 %collective-permute-start.5 = (bf16[16,256,128]{2,1,0:T(8,128)(2,1)}, bf16[16,256,128]{2,1,0:T(8,128)(2,1)S(1)}, u32[]{:S(2)}, u32[]{:S(2)}) collective-permute-start(bf16[16,256,128]{2,1,0:T(8,128)(2,1)} %join.1.refs_1_), channel_id=1, source_target_pairs={{0,1},{1,0},{2,3},{3,2},{4,5},{5,4},{6,7},{7,6},{8,9},{9,8},{10,11... | collective-permute-start | bytes 3145736 | tf_op jit(solution)/shard_map/ppermute | solution.py:343
  142.8 9.5 %all_to_all.41.refs_0_ = bf16[4,128,256]{2,1,0:T(8,128)(2,1)S(1)} all-to-all(bf16[4,128,256]{2,1,0:T(8,128)(2,1)S(1)} %copy-done.10), channel_id=1, replica_groups=mesh['grp'=2,'far'=4,'near'=4,'kv'=2,'quarter'=4,'core'=2] {'quarter'}, dimensions={0} | all-to-all | bytes 524288 | tf_op jit(solution)/shard_map/all_to_all | solution.py:335
  153.3 3.9 %attend.2 = bf16[4,144,256]{2,1,0:T(8,128)(2,1)S(1)} custom-call(s32[1]{0:T(128)} %bitcast.core_ref, bf16[4,128,256]{2,1,0:T(8,128)(2,1)S(1)} %all_to_all.41.refs_0_, bf16[16,256,128]{2,1,0:T(8,128)(2,1)} %join.1.refs_1_, bf16[16,256,128]{2,1,0:T(8,128)(2,1)} %copy-done.11), custom_call_target="tpu_custom_call" | custom-call | tf_op jit(solution)/shard_map/attend/pallas_call | solution.py:193
  159.0 4.6 %all-to-all-start.4 = ((bf16[4,144,256]{2,1,0:T(8,128)(2,1)}), bf16[4,144,256]{2,1,0:T(8,128)(2,1)S(1)}, u32[]{:S(2)}, u32[]{:S(2)}) async-start(bf16[4,144,256]{2,1,0:T(8,128)(2,1)} %copy-done.5), calls=%async_computation.4 | async-start | bytes 589824 | tf_op jit(solution)/shard_map/all_to_all | solution.py:335
  163.6 6.4 %all-gather.2.cloned.1.call-done.refs_2_ = bf16[32,256,128]{2,1,0:T(8,128)(2,1)} async-done(((bf16[2,256,128]{2,1,0:T(8,128)(2,1)}), bf16[32,256,128]{2,1,0:T(8,128)(2,1)}) %all-gather.2.cloned.1.call-update) | async-done | bytes 2097168 | tf_op jit(solution)/shard_map/all_gather | solution.py:387
  170.0 11.0 %collective-permute-start.8 = (bf16[32,256,128]{2,1,0:T(8,128)(2,1)}, bf16[32,256,128]{2,1,0:T(8,128)(2,1)}, u32[]{:S(2)}, u32[]{:S(2)}) collective-permute-start(bf16[32,256,128]{2,1,0:T(8,128)(2,1)} %all-gather.2.cloned.1.call-done.refs_2_), channel_id=1, source_target_pairs={{0,1},{1,0},{2,3},{3,2},{4,5},{5,4},{6,7},{7,6},{8,9},{9,8},{10,11... | collective-permute-start | bytes 6291464 | tf_op jit(solution)/shard_map/ppermute | solution.py:343
  182.9 23.3 %all_to_all.42.part_ref = bf16[8,16,2048]{2,1,0:T(8,128)(2,1)S(1)} all-to-all(bf16[8,16,2048]{2,1,0:T(8,128)(2,1)S(1)} %merge_and_project.2), channel_id=1, replica_groups=mesh['grp'=2,'far'=4,'near'=4,'kv'=2,'quarter'=4,'core'=2] {'kv','quarter'}, dimensions={0} | all-to-all | bytes 1048576 | tf_op jit(solution)/shard_map/all_to_all | solution.py:335
  207.3 21.7 %all_to_all.43.rows_ref = bf16[8,16,2048]{2,1,0:T(8,128)(2,1)} all-to-all(bf16[8,16,2048]{2,1,0:T(8,128)(2,1)} %get-tuple-element.31), channel_id=1, replica_groups=mesh['grp'=2,'far'=4,'near'=4,'kv'=2,'quarter'=4,'core'=2] {'kv','quarter'}, dimensions={0} | all-to-all | bytes 1048576 | tf_op jit(solution)/shard_map/all_to_all | solution.py:335
  232.5 3.1 %collective-permute-done.7.refs_1_ = bf16[1,128,256]{2,1,0:T(8,128)(2,1)S(1)} collective-permute-done((bf16[1,128,256]{2,1,0:T(8,128)(2,1)S(1)}, bf16[1,128,256]{2,1,0:T(8,128)(2,1)S(1)}, u32[]{:S(2)}, u32[]{:S(2)}) %collective-permute-start.7) | collective-permute-done | bytes 65568 | tf_op jit(solution)/shard_map/ppermute | solution.py:347
  235.6 4.7 %attend.3 = (bf16[1,144,256]{2,1,0:T(8,128)(2,1)S(1)}, bf16[1,144,256]{2,1,0:T(8,128)(2,1)S(1)}) custom-call(s32[1]{0:T(128)} %bitcast.core_ref, bf16[1,128,256]{2,1,0:T(8,128)(2,1)S(1)} %project_queries.3.refs_0_, bf16[1,128,256]{2,1,0:T(8,128)(2,1)S(1)} %collective-permute-done.7.refs_1_, bf16[32,256,128]{2,1,0:T(8,128)(2,1)} %all-gather.2.cloned.1.call-done.refs_2_, ...), custom_call_target="tpu_custom_call" | custom-call | tf_op jit(solution)/shard_map/attend/pallas_call | solution.py:193
  242.3 3.2 %collective-permute-done.9.refs_1_ = bf16[1,144,256]{2,1,0:T(8,128)(2,1)S(1)} collective-permute-done((bf16[1,144,256]{2,1,0:T(8,128)(2,1)S(1)}, bf16[1,144,256]{2,1,0:T(8,128)(2,1)S(1)}, u32[]{:S(2)}, u32[]{:S(2)}) %collective-permute-start.9) | collective-permute-done | bytes 73760 | tf_op jit(solution)/shard_map/ppermute | solution.py:347
  246.0 15.9 %all_to_all.44.part_ref = bf16[8,16,2048]{2,1,0:T(8,128)(2,1)S(1)} all-to-all(bf16[8,16,2048]{2,1,0:T(8,128)(2,1)S(1)} %merge_and_project.3), channel_id=1, replica_groups=mesh['grp'=2,'far'=4,'near'=4,'kv'=2,'quarter'=4,'core'=2] {'kv','quarter'}, dimensions={0} | all-to-all | bytes 1048576 | tf_op jit(solution)/shard_map/all_to_all | solution.py:335
  (47 shorter events, 20.8 us)
Async XLA Ops:
  6.5 60.2 %copy-start = (bf16[2,2048,128]{2,1,0:T(8,128)(2,1)S(1)}, bf16[2,2048,128]{2,1,0:T(8,128)(2,1)}, u32[]{:S(2)}) copy-start(bf16[2,2048,128]{2,1,0:T(8,128)(2,1)} %mine_ref.3) | copy-start | bytes 3145732
  6.5 64.0 %copy-start.7 = (f32[2,2048]{1,0:T(2,128)S(1)}, f32[2,2048]{1,0:T(2,128)}, u32[]{:S(2)}) copy-start(f32[2,2048]{1,0:T(2,128)} %query_gain_ref.3) | copy-start | bytes 49156
  6.6 64.0 %copy-start.6 = (bf16[16,2048]{1,0:T(8,128)(2,1)S(1)}, bf16[16,2048]{1,0:T(8,128)(2,1)}, u32[]{:S(2)}) copy-start(bf16[16,2048]{1,0:T(8,128)(2,1)} %residual_ref.1) | copy-start | bytes 196612
  63.2 16.5 %all-to-all-start.1 = ((bf16[4,256,128]{2,1,0:T(8,128)(2,1)}), bf16[4,256,128]{2,1,0:T(8,128)(2,1)S(1)}, u32[]{:S(2)}, u32[]{:S(2)}) async-start(bf16[4,256,128]{2,1,0:T(8,128)(2,1)} %get-tuple-element.21), calls=%async_computation.1 | async-start | bytes 524288 | tf_op jit(solution)/shard_map/all_to_all | solution.py:335
  66.7 17.5 %collective-permute-start = (bf16[2,2048,128]{2,1,0:T(8,128)(2,1)S(1)}, bf16[2,2048,128]{2,1,0:T(8,128)(2,1)S(1)}, u32[]{:S(2)}, u32[]{:S(2)}) collective-permute-start(bf16[2,2048,128]{2,1,0:T(8,128)(2,1)S(1)} %copy-done), channel_id=1, source_target_pairs={{0,1},{1,0},{2,3},{3,2},{4,5},{5,4},{6,7},{7,6},{8,9},{9,8},{10,11... | collective-permute-start | bytes 3145736 | tf_op jit(solution)/shard_map/ppermute | solution.py:343
  79.8 16.6 %all-to-all-start.2 = ((bf16[8,16,2048]{2,1,0:T(8,128)(2,1)}), bf16[8,16,2048]{2,1,0:T(8,128)(2,1)S(1)}, u32[]{:S(2)}, u32[]{:S(2)}) async-start(bf16[8,16,2048]{2,1,0:T(8,128)(2,1)} %first_norm.1), calls=%async_computation.2 | async-start | bytes 1048576 | tf_op jit(solution)/shard_map/all_to_all | solution.py:335
  84.2 85.8 %all-gather.2.cloned.1.call-start = ((), (), s32[]{:S(2)}) async-start(), calls=%async_computation.8 | async-start | bytes 2228224 | tf_op jit(solution)/shard_map/all_gather | solution.py:387
  97.1 43.7 %copy-start.1 = (bf16[2,128,2048]{2,1,0:T(8,128)(2,1)S(1)}, bf16[2,128,2048]{2,1,0:T(8,128)(2,1)}, u32[]{:S(2)}) copy-start(bf16[2,128,2048]{2,1,0:T(8,128)(2,1)} %refs_2_.1) | copy-start | bytes 3145732
  99.5 43.4 %copy-start.10 = (bf16[4,128,256]{2,1,0:T(8,128)(2,1)S(1)}, bf16[4,128,256]{2,1,0:T(8,128)(2,1)}, u32[]{:S(2)}) copy-start(bf16[4,128,256]{2,1,0:T(8,128)(2,1)} %project_queries.2) | copy-start | bytes 786436
  99.5 36.6 %collective-permute-start.1 = (bf16[4,256,128]{2,1,0:T(8,128)(2,1)S(1)}, bf16[4,256,128]{2,1,0:T(8,128)(2,1)S(1)}, u32[]{:S(2)}, u32[]{:S(2)}) collective-permute-start(bf16[4,256,128]{2,1,0:T(8,128)(2,1)S(1)} %all-to-all-done.1.own_ref.refs_0_), channel_id=1, source_target_pairs={{0,16},{16,32},{32,48},{48,64},{64,80},{80,96},{96,112},{112,128},... | collective-permute-start | bytes 786440 | tf_op jit(solution)/shard_map/ppermute | solution.py:339
  101.6 34.6 %collective-permute-start.2 = (bf16[4,256,128]{2,1,0:T(8,128)(2,1)S(1)}, bf16[4,256,128]{2,1,0:T(8,128)(2,1)S(1)}, u32[]{:S(2)}, u32[]{:S(2)}) collective-permute-start(bf16[4,256,128]{2,1,0:T(8,128)(2,1)S(1)} %all-to-all-done.1.own_ref.refs_0_), channel_id=1, source_target_pairs={{0,240},{16,0},{32,16},{48,32},{64,48},{80,64},{96,80},{112,96},{1... | collective-permute-start | bytes 786440 | tf_op jit(solution)/shard_map/ppermute | solution.py:339
  120.3 15.2 %collective-permute-start.3 = (bf16[2,256,128]{2,1,0:T(8,128)(2,1)S(1)}, bf16[2,256,128]{2,1,0:T(8,128)(2,1)S(1)}, u32[]{:S(2)}, u32[]{:S(2)}) collective-permute-start(bf16[2,256,128]{2,1,0:T(8,128)(2,1)S(1)} %get-tuple-element.23), channel_id=1, source_target_pairs={{0,224},{16,240},{32,0},{48,16},{64,32},{80,48},{96,64},{112,80},{... | collective-permute-start | bytes 393224 | tf_op jit(solution)/shard_map/ppermute | solution.py:339
  123.5 12.7 %collective-permute-start.4 = (bf16[2,256,128]{2,1,0:T(8,128)(2,1)S(1)}, bf16[2,256,128]{2,1,0:T(8,128)(2,1)S(1)}, u32[]{:S(2)}, u32[]{:S(2)}) collective-permute-start(bf16[2,256,128]{2,1,0:T(8,128)(2,1)S(1)} %get-tuple-element.24), channel_id=1, source_target_pairs={{0,32},{16,48},{32,64},{48,80},{64,96},{80,112},{96,128},{112,144}... | collective-permute-start | bytes 393224 | tf_op jit(solution)/shard_map/ppermute | solution.py:339
  137.2 15.1 %collective-permute-start.5 = (bf16[16,256,128]{2,1,0:T(8,128)(2,1)}, bf16[16,256,128]{2,1,0:T(8,128)(2,1)S(1)}, u32[]{:S(2)}, u32[]{:S(2)}) collective-permute-start(bf16[16,256,128]{2,1,0:T(8,128)(2,1)} %join.1.refs_1_), channel_id=1, source_target_pairs={{0,1},{1,0},{2,3},{3,2},{4,5},{5,4},{6,7},{7,6},{8,9},{9,8},{10,11... | collective-permute-start | bytes 3145736 | tf_op jit(solution)/shard_map/ppermute | solution.py:343
  140.9 17.1 %collective-permute-start.6 = (bf16[2,128,2048]{2,1,0:T(8,128)(2,1)S(1)}, bf16[2,128,2048]{2,1,0:T(8,128)(2,1)S(1)}, u32[]{:S(2)}, u32[]{:S(2)}) collective-permute-start(bf16[2,128,2048]{2,1,0:T(8,128)(2,1)S(1)} %copy-done.1), channel_id=1, source_target_pairs={{0,1},{1,0},{2,3},{3,2},{4,5},{5,4},{6,7},{7,6},{8,9},{9,8},{10,11... | collective-permute-start | bytes 3145736 | tf_op jit(solution)/shard_map/ppermute | solution.py:343
  152.3 1.0 copy-start.11
  157.9 1.0 copy-start.2
  159.0 47.2 %copy-start.8 = (f32[2,2048]{1,0:T(2,128)S(1)}, f32[2,2048]{1,0:T(2,128)}, u32[]{:S(2)}) copy-start(f32[2,2048]{1,0:T(2,128)} %out_gain_ref.3) | copy-start | bytes 49156
  159.0 22.1 %all-to-all-start.4 = ((bf16[4,144,256]{2,1,0:T(8,128)(2,1)}), bf16[4,144,256]{2,1,0:T(8,128)(2,1)S(1)}, u32[]{:S(2)}, u32[]{:S(2)}) async-start(bf16[4,144,256]{2,1,0:T(8,128)(2,1)} %copy-done.5), calls=%async_computation.4 | async-start | bytes 589824 | tf_op jit(solution)/shard_map/all_to_all | solution.py:335
  170.0 65.6 %collective-permute-start.8 = (bf16[32,256,128]{2,1,0:T(8,128)(2,1)}, bf16[32,256,128]{2,1,0:T(8,128)(2,1)}, u32[]{:S(2)}, u32[]{:S(2)}) collective-permute-start(bf16[32,256,128]{2,1,0:T(8,128)(2,1)} %all-gather.2.cloned.1.call-done.refs_2_), channel_id=1, source_target_pairs={{0,1},{1,0},{2,3},{3,2},{4,5},{5,4},{6,7},{7,6},{8,9},{9,8},{10,11... | collective-permute-start | bytes 6291464 | tf_op jit(solution)/shard_map/ppermute | solution.py:343
  181.1 1.2 copy-start.3
  230.4 15.0 %copy-start.4 = (bf16[2,128,2048]{2,1,0:T(8,128)(2,1)S(1)}, bf16[2,128,2048]{2,1,0:T(8,128)(2,1)}, u32[]{:S(2)}) copy-start(bf16[2,128,2048]{2,1,0:T(8,128)(2,1)} %copy-done.2) | copy-start | bytes 3145732
  230.4 5.2 %collective-permute-start.7 = (bf16[1,128,256]{2,1,0:T(8,128)(2,1)S(1)}, bf16[1,128,256]{2,1,0:T(8,128)(2,1)S(1)}, u32[]{:S(2)}, u32[]{:S(2)}) collective-permute-start(bf16[1,128,256]{2,1,0:T(8,128)(2,1)S(1)} %project_queries.3.refs_0_), channel_id=1, source_target_pairs={{0,2},{2,0},{4,6},{6,4},{1,3},{3,1},{5,7},{7,5},{8,10},{10,8},{12,... | collective-permute-start | bytes 196616 | tf_op jit(solution)/shard_map/ppermute | solution.py:347
  240.3 5.1 %collective-permute-start.9 = (bf16[1,144,256]{2,1,0:T(8,128)(2,1)S(1)}, bf16[1,144,256]{2,1,0:T(8,128)(2,1)S(1)}, u32[]{:S(2)}, u32[]{:S(2)}) collective-permute-start(bf16[1,144,256]{2,1,0:T(8,128)(2,1)S(1)} %get-tuple-element.35), channel_id=1, source_target_pairs={{0,2},{2,0},{4,6},{6,4},{1,3},{3,1},{5,7},{7,5},{8,10},{10,8},{12,... | collective-permute-start | bytes 221192 | tf_op jit(solution)/shard_map/ppermute | solution.py:347
  (2 other events, 1.5 us)
Sparse Core Ops, SparseCore 0:
  99.6 70.4 all-gather.1

commit v6 on v4

--- a/solution.py
+++ b/solution.py
@@ -43,10 +43,8 @@
 
 def source_kernel(source_ref, gain_ref, key_ref, value_ref, out_ref, weight_ref):
     width = key_ref.shape[1]
-    quarters = out_ref.shape[0]
-    step = pl.program_id(0)
-
-    @pl.when(step == 0)
+
+    @pl.when(pl.program_id(0) == 0)
     def _():
         for layer in range(LAYERS):
             weight_ref[layer * width : (layer + 1) * width, :] = key_ref[layer]
@@ -54,17 +52,7 @@
 
     normed = scaled(source_ref[...].astype(F32), gain_ref[...]).astype(BF16)
     columns = dot(weight_ref[...], normed, ((1,), (1,))).astype(BF16)
-    for block in range(quarters):
-
-        @pl.when(step == block)
-        def _():
-            half, at = block // 2, width * (1 + block % 2)
-            for core in range(2):
-                first = columns[2 * core * width : (2 * core + 1) * width]
-                later = columns[(2 * core + 1) * width : (2 * core + 2) * width]
-                out_ref[block, core, :width, :] = first
-                for quarter in range(half, quarters, 2):
-                    out_ref[quarter, core, at : at + width, :] = later
+    out_ref[...] = columns.reshape(out_ref.shape)
 
 
 def source_columns(source, gain, key_weight, value_weight, quarters):
@@ -73,7 +61,7 @@
     value_weight = jnp.swapaxes(value_weight, 1, 2)
     width = key_weight.shape[1]
     block = rows // quarters
-    shape = (quarters, 2, 3 * width, block)
+    shape = (quarters, 2, LAYERS * width, block)
     operands = (source, gain, key_weight, value_weight)
     return pl.pallas_call(
         source_kernel,
@@ -84,7 +72,7 @@
             pl.BlockSpec(key_weight.shape, lambda i: (0, 0, 0)),
             pl.BlockSpec(value_weight.shape, lambda i: (0, 0, 0)),
         ],
-        out_specs=pl.BlockSpec(shape, lambda i: (0, 0, 0, 0)),
+        out_specs=pl.BlockSpec((1, *shape[1:]), lambda i: (i, 0, 0, 0)),
         out_shape=pltpu.HBM(shape, BF16),
         scratch_shapes=[pltpu.VMEM((2 * LAYERS * width, features), BF16)],
         compiler_params=pltpu.CompilerParams(vmem_limit_bytes=12288 * 1024),
@@ -109,11 +97,11 @@
     )(*held_in_vmem(rows, gain))
 
 
-def query_kernel(layer, core_ref, rows_ref, mine_ref, other_ref, out_ref):
+def query_kernel(core_ref, rows_ref, mine_ref, other_ref, out_ref):
     chips, block, features = rows_ref.shape
     rows = rows_ref[...].reshape(chips * block, features)
-    mine = dot(rows, mine_ref[layer]).astype(BF16)
-    other = dot(rows, other_ref[layer]).astype(BF16)
+    mine = dot(rows, mine_ref[0]).astype(BF16)
+    other = dot(rows, other_ref[0]).astype(BF16)
     first = core_ref[0] == 0
     width = mine.shape[1]
     low = jnp.where(first, mine, other)
@@ -123,16 +111,25 @@
         out_ref[peer, :, width:] = high
 
 
-def project_queries(layer, core, rows, mine, other, copies, held):
-    chips, block, _ = rows.shape
-    return pl.pallas_call(
-        functools.partial(query_kernel, layer),
-        in_specs=[pl.BlockSpec(memory_space=pltpu.SMEM)] + in_vmem(3),
-        out_specs=in_vmem(1)[0],
-        out_shape=held((copies, chips * block, 2 * mine.shape[2]), BF16),
+def project_queries(layer, core, rows, mine, other, copies):
+    chips, block, features = rows.shape
+    width = mine.shape[2]
+    weight = pl.BlockSpec((1, features, width), lambda i: (layer, 0, 0))
+    shape = (copies, chips * block, 2 * width)
+    return pl.pallas_call(
+        query_kernel,
+        grid=(1,),
+        in_specs=[
+            pl.BlockSpec(memory_space=pltpu.SMEM),
+            pl.BlockSpec(memory_space=pltpu.VMEM),
+            weight,
+            weight,
+        ],
+        out_specs=pl.BlockSpec(shape, lambda i: (0, 0, 0)),
+        out_shape=pltpu.HBM(shape, BF16),
         compiler_params=pltpu.CompilerParams(vmem_limit_bytes=8192 * 1024),
         name="project_queries",
-    )(core, pltpu.with_memory_space_constraint(rows, pltpu.HBM), *held_in_vmem(mine, other))
+    )(core, *held_in_vmem(rows), *[pltpu.with_memory_space_constraint(a, pltpu.HBM) for a in (mine, other)])
 
 
 def attend_kernel(groups, pieces, core_ref, *refs):
@@ -185,7 +182,7 @@
         work(other_refs, mine_refs)
 
 
-def attend(core, queries, mine, other):
+def attend(core, queries, mine, other, placed):
     heads, rows, width = queries[0].shape
     groups = len(queries)
     span = sum(piece.shape[0] * piece.shape[2] for piece in mine)
@@ -193,77 +190,60 @@
         functools.partial(attend_kernel, groups, len(mine)),
         in_specs=[pl.BlockSpec(memory_space=pltpu.SMEM)] + in_vmem(groups + 2 * len(mine)),
         out_specs=in_vmem(groups),
-        out_shape=[vmem_out((heads, rows + STATS, width))] * groups,
+        out_shape=[placed((heads, rows + STATS, width), BF16)] * groups,
         scratch_shapes=[pltpu.VMEM((groups * heads * rows, span), F32)],
         compiler_params=pltpu.CompilerParams(vmem_limit_bytes=16384 * 1024),
         name="attend",
-    )(core, *held_in_vmem(*queries, *mine, *other))
-
-
-def split_kernel(held_ref, first_ref, later_ref):
+    )(core, *held_in_vmem(*queries), *[pltpu.with_memory_space_constraint(a, pltpu.HBM) for a in (*mine, *other)])
+
+
+def split_kernel(held_ref, *layer_refs):
     devices, width, _ = held_ref.shape
-    width //= 3
+    width //= LAYERS
     for device in range(devices):
         columns = slice(device * width, (device + 1) * width)
-        first_ref[0, columns, :] = held_ref[device, :width, :]
-        for half in range(2):
-            at = width * (1 + half)
-            later_ref[half, columns, :] = held_ref[device, at : at + width, :]
+        for layer, ref in enumerate(layer_refs):
+            ref[0, columns, :] = held_ref[device, layer * width : (layer + 1) * width, :]
 
 
 def split(held):
     devices, width, block = held.shape
-    column = devices * width // 3
+    shape = (1, devices * width // LAYERS, block)
     return pl.pallas_call(
         split_kernel,
         in_specs=in_vmem(1),
-        out_specs=in_vmem(2),
-        out_shape=[vmem_out((1, column, block)), pltpu.HBM((2, column, block), BF16)],
+        out_specs=in_vmem(LAYERS),
+        out_shape=[vmem_out(shape)] + [pltpu.HBM(shape, BF16)] * (LAYERS - 1),
         compiler_params=pltpu.CompilerParams(vmem_limit_bytes=2048 * 1024),
         name="split",
     )(*held_in_vmem(held))
 
 
-def four_kernel(*refs):
-    pieces, (own_ref, low_ref, middle_ref) = refs[:4], refs[4:]
-    for at, ref in enumerate(pieces):
-        block = ref[0]
-        own_ref[at] = block
-        if at < 2:
-            low_ref[at] = block
-        if 1 <= at < 3:
-            middle_ref[at - 1] = block
-
-
-def join_four(*pieces):
-    shape = pieces[0].shape[1:]
-    return pl.pallas_call(
-        four_kernel,
-        in_specs=in_vmem(4),
-        out_specs=in_vmem(3),
-        out_shape=[vmem_out((count, *shape)) for count in (4, 2, 2)],
+def join_kernel(distance, stage_ref, mine_ref, came_ref, out_ref):
+    count = mine_ref.shape[0]
+    bit = stage_ref[0] & distance
+
+    @pl.when(bit == 0)
+    def _():
+        out_ref[:count] = mine_ref[...]
+        out_ref[count:] = came_ref[...]
+
+    @pl.when(bit != 0)
+    def _():
+        out_ref[:count] = came_ref[...]
+        out_ref[count:] = mine_ref[...]
+
+
+def join(distance, stage, mine, came, placed):
+    count, *rest = mine.shape
+    return pl.pallas_call(
+        functools.partial(join_kernel, distance),
+        in_specs=[pl.BlockSpec(memory_space=pltpu.SMEM)] + in_vmem(2),
+        out_specs=in_vmem(1)[0],
+        out_shape=placed((2 * count, *rest), BF16),
         compiler_params=pltpu.CompilerParams(vmem_limit_bytes=2048 * 1024),
-        name="join_four",
-    )(*held_in_vmem(*pieces))
-
-
-def join_kernel(*refs):
-    at = 0
-    for ref in refs[:-1]:
-        refs[-1][at : at + ref.shape[0]] = ref[...]
-        at += ref.shape[0]
-
-
-def join(*pieces):
-    count = sum(piece.shape[0] for piece in pieces)
-    return pl.pallas_call(
-        join_kernel,
-        in_specs=in_vmem(len(pieces)),
-        out_specs=in_vmem(1)[0],
-        out_shape=vmem_out((count, *pieces[0].shape[1:])),
-        compiler_params=pltpu.CompilerParams(vmem_limit_bytes=4096 * 1024),
         name="join",
-    )(*held_in_vmem(*pieces))
+    )(stage, mine, came)
 
 
 def merge_kernel(layer, core_ref, *refs):
@@ -297,13 +277,13 @@
     out_ref[...] = projected.astype(BF16).reshape(out_ref.shape)
 
 
-def merge_and_project(layer, core, parts, mine, other, chips):
+def merge_and_project(layer, core, parts, mine, other, chips, placed):
     rows = parts[0].shape[1] - STATS
     return pl.pallas_call(
         functools.partial(merge_kernel, layer),
         in_specs=[pl.BlockSpec(memory_space=pltpu.SMEM)] + in_vmem(len(parts) + 2),
         out_specs=in_vmem(1)[0],
-        out_shape=vmem_out((chips, rows // chips, mine.shape[2])),
+        out_shape=placed((chips, rows // chips, mine.shape[2]), BF16),
         compiler_params=pltpu.CompilerParams(vmem_limit_bytes=8192 * 1024),
         name="merge_and_project",
     )(core, *held_in_vmem(*parts, mine, other))
@@ -338,34 +318,21 @@
     return lax.all_to_all(value, axis, split_axis=0, concat_axis=0, tiled=True)
 
 
-def shifted(value, distance, size):
-    return lax.ppermute(value, "sp", [(z, (z + distance) % size) for z in range(size)])
+def passed(value, distance, stages):
+    pairs = [
+        (2 * stage + core, 2 * ((stage + (distance, -distance)[core]) % stages) + core)
+        for stage in range(stages)
+        for core in range(2)
+    ]
+    return lax.ppermute(value, ("sp", "core"), pairs)
 
 
 def swap(value):
     return lax.ppermute(value, "core", [(0, 1), (1, 0)])
 
 
-def beside(value, quarters):
-    return lax.ppermute(value, "quarter", [(q, q ^ 1) for q in range(quarters)])
-
-
 def after(value, *others):
     return lax.optimization_barrier((value, *others))[0]
-
-
-def stride_step(block, stride, size):
-    sent = [shifted(block, distance, size) for distance in (stride, -stride, 2 * stride)]
-    return sent[0], block, sent[1], sent[2]
-
-
-def near_step(own, low, middle, size):
-    return (
-        shifted(own, 1, size),
-        shifted(own, -1, size),
-        shifted(low, 2, size),
-        shifted(middle, -2, size),
-    )
 
 
 def layers(
@@ -383,41 +350,57 @@
     chips = quarters * lax.axis_size("kv")
     stages = lax.axis_size("sp")
     core = lax.axis_index("core").astype(jnp.int32).reshape(1)
+    stage = lax.axis_index("sp").astype(jnp.int32).reshape(1)
     width = key_weight.shape[2]
+    distances = [stages >> bit for bit in range(1, stages.bit_length())]
 
     columns = source_columns(source, source_gain[None], key_weight, value_weight, quarters)
-    columns = columns.reshape(quarters * 2, 3 * width, -1)
+    columns = columns.reshape(quarters * 2, LAYERS * width, -1)
     held = exchange(columns, GROUP)
     first, later = split(held)
-    pieces = stride_step(first, stages // 4, stages)
-    own, low, middle = join_four(*pieces)
-    pieces = near_step(own, low, middle, stages)
-    near = join(own, *pieces)
-    far = swap(near)
-    normed = after(first_norm(target, query_gain, chips), held)
     query_other = swap(query_weight)
     out_other = swap(out_weight)
-    near_later = lax.all_gather(after(later, near), "sp", axis=0, tiled=True)
-
-    rows = exchange(normed, CHIPS)
-    mine = project_queries(0, core, rows, query_weight, query_other, quarters, pltpu.HBM)
-    queries = exchange(mine, "quarter")
-    (parts,) = attend(core, [queries], [near], [far])
-    parts, out_other = lax.optimization_barrier((parts, out_other))
-    parts = exchange(parts, "quarter")
-    projected = merge_and_project(0, core, [parts], out_weight, out_other, chips)
-    arrived = exchange(projected, CHIPS)
-    residual, normed = finish(0, arrived, target, out_gain, query_gain)
-
-    rows = exchange(normed, CHIPS)
-    far_later = swap(near_later)
-    mine = project_queries(1, core, rows, query_weight, query_other, 1, pltpu.VMEM)
-    theirs = beside(mine, quarters)
-    kept, sent = attend(core, [mine, theirs], [near_later], [far_later])
-    came = beside(sent, quarters)
-    projected = merge_and_project(1, core, [kept, came], out_weight, out_other, chips)
-    arrived = exchange(projected, CHIPS)
-    (residual,) = finish(1, arrived, residual, out_gain, query_gain)
+    normed = after(first_norm(target, query_gain, chips), held)
+
+    near = first
+    for index, distance in enumerate(distances):
+        came = passed(near, distance, stages)
+        if index + 1 < len(distances):
+            near = join(distances[index], stage, near, came, pltpu.VMEM)
+    far = [swap(near)]
+    far.append(swap(came))
+    near = [near, came]
+
+    residual = target
+    for layer in range(LAYERS):
+        last = layer + 1 == LAYERS
+        rows = exchange(normed, CHIPS)
+        if last:
+            next_near = join(distances[2], stage, next_near, after(came, normed), pltpu.HBM)
+            came = passed(next_near, distances[3], stages)
+            far = [swap(next_near)]
+            near = [next_near, came]
+        mine = project_queries(layer, core, rows, query_weight, query_other, quarters)
+        queries = exchange(mine, "quarter")
+        if last:
+            far.append(swap(after(came, mine)))
+        else:
+            came = passed(after(later, near[1]), distances[0], stages)
+        placed = pltpu.VMEM if last else pltpu.HBM
+        (parts,) = attend(core, [queries], near, far, placed)
+        if not last:
+            parts, out_other = lax.optimization_barrier((parts, out_other))
+            next_near = join(distances[0], stage, later, after(came, parts), pltpu.HBM)
+            came = passed(next_near, distances[1], stages)
+        parts = exchange(parts, "quarter")
+        projected = merge_and_project(layer, core, [parts], out_weight, out_other, chips, placed)
+        if not last:
+            next_near = join(distances[1], stage, next_near, after(came, projected), pltpu.HBM)
+            came = passed(next_near, distances[2], stages)
+        arrived = exchange(projected, CHIPS)
+        done = finish(layer, arrived, residual, out_gain, query_gain)
+        residual = done[0]
+        normed = done[-1]
     return residual
 
 

time: 274 us -> 262 us (0.956)
  blocking collectives: 124 us -> 91.4 us
  starting transfers between devices: 61.4 us -> 84.2 us
  between operations: 13.6 us -> 0.29 us
  waiting for transfers between devices: 48.3 us -> 55.1 us
  Pallas kernels: 22.5 us -> 25.5 us
    all_to_all x5 -> x4, blocking collectives: 124 us -> 91.4 us  [exchange(): return lax.all_to_all(value, axis, split_axis=0, concat_axis=0, tiled=True)]
    ppermute x9 -> x8, waiting for transfers between devices: 22.3 us -> 39.7 us  [passed(): return lax.ppermute(value, ('sp', 'core'), pairs)]
    ppermute x4 -> x6, starting transfers between devices: 21.8 us -> 37.7 us  [swap(): return lax.ppermute(value, 'core', [(0, 1), (1, 0)])]
    all_gather x1 -> x0, waiting for transfers between devices: 12.2 us -> none  [layers(): near_later = lax.all_gather(after(later, near), 'sp', axis=0, tiled=True)]
    all_to_all x2 -> x5, starting transfers between devices: 10.3 us -> 21.7 us  [exchange(): return lax.all_to_all(value, axis, split_axis=0, concat_axis=0, tiled=True)]
    ppermute x9 -> x8, starting transfers between devices: 29.2 us -> 24.8 us  [passed(): return lax.ppermute(value, ('sp', 'core'), pairs)]
    all_to_all x2 -> x5, waiting for transfers between devices: 13.7 us -> 15.4 us  [exchange(): return lax.all_to_all(value, axis, split_axis=0, concat_axis=0, tiled=True)]
    pallas_call x5 -> x9, Pallas kernels: 6.14 us -> 7.61 us  [the longest x2 4.68 us: project_queries(): pl.pallas_call(query_kernel, grid=(1,), in_specs=[pl.BlockSpec(memory_spa...]
  transfers between devices with their start and end apart: 16 -> 19, of which waited for: 7 -> 8; matrix products, arithmetic and copies ran while one was open for 0% -> 0% of each run, Pallas kernels for 4% -> 5%
where the time goes in v6:
time: 262 us; the launch traced here: 258 us
  blocking collectives  91.4 us (35%)
  starting transfers between devices  84.2 us (32%)
  waiting for transfers between devices  55.1 us (21%)
  Pallas kernels  25.5 us (10%)
    all_to_all x4, blocking collectives, exchange(): return lax.all_to_all(value, axis, split_axis=0, concat_axis=0, tiled=True)  91.4 us
    ppermute x8, waiting for transfers between devices, passed(): return lax.ppermute(value, ('sp', 'core'), pairs)  39.7 us
    ppermute x6, starting transfers between devices, swap(): return lax.ppermute(value, 'core', [(0, 1), (1, 0)])  37.7 us
    ppermute x8, starting transfers between devices, passed(): return lax.ppermute(value, ('sp', 'core'), pairs)  24.8 us
    all_to_all x5, starting transfers between devices, exchange(): return lax.all_to_all(value, axis, split_axis=0, concat_axis=0, tiled=True)  21.7 us
    all_to_all x5, waiting for transfers between devices, exchange(): return lax.all_to_all(value, axis, split_axis=0, concat_axis=0, tiled=True)  15.4 us
    pallas_call x2, Pallas kernels, attend(): pl.pallas_call(functools.partial(attend_kernel, groups, len(mine)), in_sp...  8.55 us
  transfers between devices with their start and end apart: 19, of which 8 were waited for; matrix products, arithmetic and copies ran while one was open for 0% of the time, Pallas kernels for 5%

profile of v6, /device:TPU:65, one launch (start us, length us, event | category | flops | bytes accessed | tf_op | source)
XLA Modules:
  0.0 258.4 jit_solution(17810123558847393895)
XLA Ops:
  0.0 4.5 %source_columns.1 = bf16[4,2,64,128]{3,2,1,0:T(8,128)(2,1)} custom-call(bf16[512,2048]{1,0:T(8,128)(2,1)} %source_ref.1, f32[1,2048]{1,0:T(1,128)} %bitcast.9, bf16[2,32,2048]{2,1,0:T(8,128)(2,1)} %bitcast.7, bf16[2,32,2048]{2,1,0:T(8,128)(2,1)} %bitcast.8), custom_call_target="tpu_custom_call" | custom-call | tf_op jit(solution)/shard_map/source_columns/pallas_call | solution.py:66
  4.5 50.7 %all_to_all.45.held_ref = bf16[8,64,128]{2,1,0:T(8,128)(2,1)S(1)} all-to-all(bf16[8,64,128]{2,1,0:T(8,128)(2,1)} %bitcast.6), channel_id=1, replica_groups=mesh['grp'=2,'sp'=16,'kv'=2,'quarter'=4,'core'=2] {'quarter','core'}, dimensions={0} | all-to-all | bytes 262144 | tf_op jit(solution)/shard_map/all_to_all | solution.py:318
  60.7 9.2 %collective-permute-done.1.came_ref = bf16[1,256,128]{2,1,0:T(8,128)(2,1)S(1)} collective-permute-done((bf16[1,256,128]{2,1,0:T(8,128)(2,1)S(1)}, bf16[1,256,128]{2,1,0:T(8,128)(2,1)S(1)}, u32[]{:S(2)}, u32[]{:S(2)}) %collective-permute-start.1) | collective-permute-done | bytes 65568 | tf_op jit(solution)/shard_map/ppermute | solution.py:327
  72.9 3.7 %all-to-all-start.1 = ((bf16[8,16,2048]{2,1,0:T(8,128)(2,1)}), bf16[8,16,2048]{2,1,0:T(8,128)(2,1)S(1)}, u32[]{:S(2)}, u32[]{:S(2)}) async-start(bf16[8,16,2048]{2,1,0:T(8,128)(2,1)} %first_norm.1), calls=%async_computation.1 | async-start | bytes 1048576 | tf_op jit(solution)/shard_map/all_to_all | solution.py:318
  76.6 3.7 %collective-permute-done.2.came_ref = bf16[2,256,128]{2,1,0:T(8,128)(2,1)S(1)} collective-permute-done((bf16[2,256,128]{2,1,0:T(8,128)(2,1)S(1)}, bf16[2,256,128]{2,1,0:T(8,128)(2,1)S(1)}, u32[]{:S(2)}, u32[]{:S(2)}) %collective-permute-start.2) | collective-permute-done | bytes 131104 | tf_op jit(solution)/shard_map/ppermute | solution.py:327
  83.4 5.9 %collective-permute-done.3.came_ref = bf16[4,256,128]{2,1,0:T(8,128)(2,1)S(1)} collective-permute-done((bf16[4,256,128]{2,1,0:T(8,128)(2,1)S(1)}, bf16[4,256,128]{2,1,0:T(8,128)(2,1)S(1)}, u32[]{:S(2)}, u32[]{:S(2)}) %collective-permute-start.3) | collective-permute-done | bytes 262176 | tf_op jit(solution)/shard_map/ppermute | solution.py:327
  89.3 6.9 %collective-permute-start.4 = (bf16[8,256,128]{2,1,0:T(8,128)(2,1)S(1)}, bf16[8,256,128]{2,1,0:T(8,128)(2,1)}, u32[]{:S(2)}, u32[]{:S(2)}) collective-permute-start(bf16[8,256,128]{2,1,0:T(8,128)(2,1)S(1)} %join.8.refs_1_), channel_id=1, source_target_pairs={{0,16},{1,241},{16,32},{17,1},{32,48},{33,17},{48,64},{49,33},{64,... | collective-permute-start | bytes 1572872 | tf_op jit(solution)/shard_map/ppermute | solution.py:327
  96.3 7.1 %collective-permute-start.7 = (bf16[2,128,2048]{2,1,0:T(8,128)(2,1)S(1)}, bf16[2,128,2048]{2,1,0:T(8,128)(2,1)S(1)}, u32[]{:S(2)}, u32[]{:S(2)}) collective-permute-start(bf16[2,128,2048]{2,1,0:T(8,128)(2,1)S(1)} %copy-done), channel_id=1, source_target_pairs={{0,1},{1,0},{2,3},{3,2},{4,5},{5,4},{6,7},{7,6},{8,9},{9,8},{10,11... | collective-permute-start | bytes 3145736 | tf_op jit(solution)/shard_map/ppermute | solution.py:331
  105.4 8.5 %collective-permute-start.6 = (bf16[8,256,128]{2,1,0:T(8,128)(2,1)}, bf16[8,256,128]{2,1,0:T(8,128)(2,1)}, u32[]{:S(2)}, u32[]{:S(2)}) collective-permute-start(bf16[8,256,128]{2,1,0:T(8,128)(2,1)} %collective-permute-done.4.refs_2_), channel_id=1, source_target_pairs={{0,1},{1,0},{2,3},{3,2},{4,5},{5,4},{6,7},{7,6},{8,9},{9,8},{10,11... | collective-permute-start | bytes 1572872 | tf_op jit(solution)/shard_map/ppermute | solution.py:331
  119.8 7.9 %all-to-all-done.2.refs_0_ = bf16[4,128,256]{2,1,0:T(8,128)(2,1)S(1)} async-done(((bf16[4,128,256]{2,1,0:T(8,128)(2,1)}), bf16[4,128,256]{2,1,0:T(8,128)(2,1)S(1)}, u32[]{:S(2)}, u32[]{:S(2)}) %all-to-all-start.2) | async-done | bytes 262176 | tf_op jit(solution)/shard_map/all_to_all | solution.py:318
  127.7 4.5 %attend.2 = bf16[4,144,256]{2,1,0:T(8,128)(2,1)} custom-call(s32[1]{0:T(128)} %bitcast.core_ref, bf16[4,128,256]{2,1,0:T(8,128)(2,1)S(1)} %all-to-all-done.2.refs_0_, bf16[8,256,128]{2,1,0:T(8,128)(2,1)} %copy-done.1, bf16[8,256,128]{2,1,0:T(8,128)(2,1)} %collective-permute-done.4.refs_2_, bf16[8,256,128]{2,1,0:T(8,128)(2,1)} %collective-permute-done.5.refs_3_, ...), custom_call_target="tpu_custom_call" | custom-call | tf_op jit(solution)/shard_map/attend/pallas_call | solution.py:189
  132.3 10.9 %all_to_all.46.refs_0_ = bf16[4,144,256]{2,1,0:T(8,128)(2,1)S(1)} all-to-all(bf16[4,144,256]{2,1,0:T(8,128)(2,1)} %attend.2), channel_id=1, replica_groups=mesh['grp'=2,'sp'=16,'kv'=2,'quarter'=4,'core'=2] {'quarter'}, dimensions={0} | all-to-all | bytes 589824 | tf_op jit(solution)/shard_map/all_to_all | solution.py:318
  144.5 4.2 %all-to-all-start.4 = ((bf16[8,16,2048]{2,1,0:T(8,128)(2,1)}), bf16[8,16,2048]{2,1,0:T(8,128)(2,1)S(1)}, u32[]{:S(2)}, u32[]{:S(2)}) async-start(bf16[8,16,2048]{2,1,0:T(8,128)(2,1)} %merge_and_project.2), calls=%async_computation.4 | async-start | bytes 1048576 | tf_op jit(solution)/shard_map/all_to_all | solution.py:318
  151.9 10.6 %collective-permute-done.8.came_ref = bf16[1,256,128]{2,1,0:T(8,128)(2,1)S(1)} collective-permute-done((bf16[1,256,128]{2,1,0:T(8,128)(2,1)S(1)}, bf16[1,256,128]{2,1,0:T(8,128)(2,1)S(1)}, u32[]{:S(2)}, u32[]{:S(2)}) %collective-permute-start.8) | collective-permute-done | bytes 65568 | tf_op jit(solution)/shard_map/ppermute | solution.py:327
  163.2 3.8 %collective-permute-start.9 = (bf16[2,256,128]{2,1,0:T(8,128)(2,1)}, bf16[2,256,128]{2,1,0:T(8,128)(2,1)S(1)}, u32[]{:S(2)}, u32[]{:S(2)}) collective-permute-start(bf16[2,256,128]{2,1,0:T(8,128)(2,1)} %join.9.mine_ref), channel_id=1, source_target_pairs={{0,64},{1,193},{16,80},{17,209},{32,96},{33,225},{48,112},{49,241}... | collective-permute-start | bytes 393224 | tf_op jit(solution)/shard_map/ppermute | solution.py:327
  168.1 6.6 %all-to-all-start.5 = ((bf16[8,16,2048]{2,1,0:T(8,128)(2,1)}), bf16[8,16,2048]{2,1,0:T(8,128)(2,1)S(1)}, u32[]{:S(2)}, u32[]{:S(2)}) async-start(bf16[8,16,2048]{2,1,0:T(8,128)(2,1)} %get-tuple-element.21), calls=%async_computation.5 | async-start | bytes 1048576 | tf_op jit(solution)/shard_map/all_to_all | solution.py:318
  180.4 8.3 %collective-permute-done.10.came_ref = bf16[4,256,128]{2,1,0:T(8,128)(2,1)S(1)} collective-permute-done((bf16[4,256,128]{2,1,0:T(8,128)(2,1)}, bf16[4,256,128]{2,1,0:T(8,128)(2,1)S(1)}, u32[]{:S(2)}, u32[]{:S(2)}) %collective-permute-start.10) | collective-permute-done | bytes 262176 | tf_op jit(solution)/shard_map/ppermute | solution.py:327
  192.4 9.1 %collective-permute-start.12 = (bf16[8,256,128]{2,1,0:T(8,128)(2,1)}, bf16[8,256,128]{2,1,0:T(8,128)(2,1)}, u32[]{:S(2)}, u32[]{:S(2)}) collective-permute-start(bf16[8,256,128]{2,1,0:T(8,128)(2,1)} %join.11.refs_1_), channel_id=1, source_target_pairs={{0,1},{1,0},{2,3},{3,2},{4,5},{5,4},{6,7},{7,6},{8,9},{9,8},{10,11... | collective-permute-start | bytes 1572872 | tf_op jit(solution)/shard_map/ppermute | solution.py:331
  203.9 8.2 %collective-permute-start.13 = (bf16[8,256,128]{2,1,0:T(8,128)(2,1)S(1)}, bf16[8,256,128]{2,1,0:T(8,128)(2,1)}, u32[]{:S(2)}, u32[]{:S(2)}) collective-permute-start(bf16[8,256,128]{2,1,0:T(8,128)(2,1)S(1)} %collective-permute-done.11.refs_2_), channel_id=1, source_target_pairs={{0,1},{1,0},{2,3},{3,2},{4,5},{5,4},{6,7},{7,6},{8,9},{9,8},{10,11... | collective-permute-start | bytes 1572872 | tf_op jit(solution)/shard_map/ppermute | solution.py:331
  212.1 3.7 %all-to-all-start.6 = ((bf16[4,128,256]{2,1,0:T(8,128)(2,1)}), bf16[4,128,256]{2,1,0:T(8,128)(2,1)S(1)}, u32[]{:S(2)}, u32[]{:S(2)}) async-start(bf16[4,128,256]{2,1,0:T(8,128)(2,1)} %project_queries.3), calls=%async_computation.6 | async-start | bytes 524288 | tf_op jit(solution)/shard_map/all_to_all | solution.py:318
  215.7 7.5 %all-to-all-done.6.refs_0_ = bf16[4,128,256]{2,1,0:T(8,128)(2,1)S(1)} async-done(((bf16[4,128,256]{2,1,0:T(8,128)(2,1)}), bf16[4,128,256]{2,1,0:T(8,128)(2,1)S(1)}, u32[]{:S(2)}, u32[]{:S(2)}) %all-to-all-start.6) | async-done | bytes 262176 | tf_op jit(solution)/shard_map/all_to_all | solution.py:318
  223.2 4.0 %attend.3 = bf16[4,144,256]{2,1,0:T(8,128)(2,1)S(1)} custom-call(s32[1]{0:T(128)} %bitcast.core_ref, bf16[4,128,256]{2,1,0:T(8,128)(2,1)S(1)} %all-to-all-done.6.refs_0_, bf16[8,256,128]{2,1,0:T(8,128)(2,1)} %join.11.refs_1_, bf16[8,256,128]{2,1,0:T(8,128)(2,1)} %copy-done.8, bf16[8,256,128]{2,1,0:T(8,128)(2,1)} %collective-permute-done.12.refs_3_, ...), custom_call_target="tpu_custom_call" | custom-call | tf_op jit(solution)/shard_map/attend/pallas_call | solution.py:189
  227.2 10.7 %all_to_all.47.refs_0_ = bf16[4,144,256]{2,1,0:T(8,128)(2,1)S(1)} all-to-all(bf16[4,144,256]{2,1,0:T(8,128)(2,1)S(1)} %attend.3), channel_id=1, replica_groups=mesh['grp'=2,'sp'=16,'kv'=2,'quarter'=4,'core'=2] {'quarter'}, dimensions={0} | all-to-all | bytes 589824 | tf_op jit(solution)/shard_map/all_to_all | solution.py:318
  238.5 19.1 %all_to_all.48.part_ref = bf16[8,16,2048]{2,1,0:T(8,128)(2,1)S(1)} all-to-all(bf16[8,16,2048]{2,1,0:T(8,128)(2,1)S(1)} %merge_and_project.3), channel_id=1, replica_groups=mesh['grp'=2,'sp'=16,'kv'=2,'quarter'=4,'core'=2] {'kv','quarter'}, dimensions={0} | all-to-all | bytes 1048576 | tf_op jit(solution)/shard_map/all_to_all | solution.py:318
  (53 shorter events, 38.7 us)
Async XLA Ops:
  0.0 71.9 %copy-start.5 = (f32[2,2048]{1,0:T(2,128)S(1)}, f32[2,2048]{1,0:T(2,128)}, u32[]{:S(2)}) copy-start(f32[2,2048]{1,0:T(2,128)} %query_gain_ref.3) | copy-start | bytes 49156
  0.0 71.9 %copy-start.4 = (bf16[16,2048]{1,0:T(8,128)(2,1)S(1)}, bf16[16,2048]{1,0:T(8,128)(2,1)}, u32[]{:S(2)}) copy-start(bf16[16,2048]{1,0:T(8,128)(2,1)} %residual_ref.1) | copy-start | bytes 196612
  4.5 91.8 %copy-start = (bf16[2,128,2048]{2,1,0:T(8,128)(2,1)S(1)}, bf16[2,128,2048]{2,1,0:T(8,128)(2,1)}, u32[]{:S(2)}) copy-start(bf16[2,128,2048]{2,1,0:T(8,128)(2,1)} %refs_1_.3) | copy-start | bytes 3145732
  55.9 14.0 %collective-permute-start.1 = (bf16[1,256,128]{2,1,0:T(8,128)(2,1)S(1)}, bf16[1,256,128]{2,1,0:T(8,128)(2,1)S(1)}, u32[]{:S(2)}, u32[]{:S(2)}) collective-permute-start(bf16[1,256,128]{2,1,0:T(8,128)(2,1)S(1)} %get-tuple-element.18.mine_ref), channel_id=1, source_target_pairs={{0,128},{1,129},{16,144},{17,145},{32,160},{33,161},{48,176},{49,1... | collective-permute-start | bytes 196616 | tf_op jit(solution)/shard_map/ppermute | solution.py:327
  57.8 56.1 %collective-permute-start = (bf16[2,2048,128]{2,1,0:T(8,128)(2,1)}, bf16[2,2048,128]{2,1,0:T(8,128)(2,1)}, u32[]{:S(2)}, u32[]{:S(2)}) collective-permute-start(bf16[2,2048,128]{2,1,0:T(8,128)(2,1)} %mine_ref.3), channel_id=1, source_target_pairs={{0,1},{1,0},{2,3},{3,2},{4,5},{5,4},{6,7},{7,6},{8,9},{9,8},{10,11... | collective-permute-start | bytes 3145736 | tf_op jit(solution)/shard_map/ppermute | solution.py:331
  69.9 10.3 %collective-permute-start.2 = (bf16[2,256,128]{2,1,0:T(8,128)(2,1)S(1)}, bf16[2,256,128]{2,1,0:T(8,128)(2,1)S(1)}, u32[]{:S(2)}, u32[]{:S(2)}) collective-permute-start(bf16[2,256,128]{2,1,0:T(8,128)(2,1)S(1)} %join.6.mine_ref), channel_id=1, source_target_pairs={{0,64},{1,193},{16,80},{17,209},{32,96},{33,225},{48,112},{49,241}... | collective-permute-start | bytes 393224 | tf_op jit(solution)/shard_map/ppermute | solution.py:327
  72.9 41.1 %all-to-all-start.1 = ((bf16[8,16,2048]{2,1,0:T(8,128)(2,1)}), bf16[8,16,2048]{2,1,0:T(8,128)(2,1)S(1)}, u32[]{:S(2)}, u32[]{:S(2)}) async-start(bf16[8,16,2048]{2,1,0:T(8,128)(2,1)} %first_norm.1), calls=%async_computation.1 | async-start | bytes 1048576 | tf_op jit(solution)/shard_map/all_to_all | solution.py:318
  80.3 9.0 %collective-permute-start.3 = (bf16[4,256,128]{2,1,0:T(8,128)(2,1)S(1)}, bf16[4,256,128]{2,1,0:T(8,128)(2,1)S(1)}, u32[]{:S(2)}, u32[]{:S(2)}) collective-permute-start(bf16[4,256,128]{2,1,0:T(8,128)(2,1)S(1)} %join.7.mine_ref), channel_id=1, source_target_pairs={{0,32},{1,225},{16,48},{17,241},{32,64},{33,1},{48,80},{49,17},{64... | collective-permute-start | bytes 786440 | tf_op jit(solution)/shard_map/ppermute | solution.py:327
  89.3 38.4 %copy-start.1 = (bf16[8,256,128]{2,1,0:T(8,128)(2,1)}, bf16[8,256,128]{2,1,0:T(8,128)(2,1)S(1)}, u32[]{:S(2)}) copy-start(bf16[8,256,128]{2,1,0:T(8,128)(2,1)S(1)} %join.8.refs_1_) | copy-start | bytes 1572868
  89.3 16.1 %collective-permute-start.4 = (bf16[8,256,128]{2,1,0:T(8,128)(2,1)S(1)}, bf16[8,256,128]{2,1,0:T(8,128)(2,1)}, u32[]{:S(2)}, u32[]{:S(2)}) collective-permute-start(bf16[8,256,128]{2,1,0:T(8,128)(2,1)S(1)} %join.8.refs_1_), channel_id=1, source_target_pairs={{0,16},{1,241},{16,32},{17,1},{32,48},{33,17},{48,64},{49,33},{64,... | collective-permute-start | bytes 1572872 | tf_op jit(solution)/shard_map/ppermute | solution.py:327
  96.3 35.9 %collective-permute-start.7 = (bf16[2,128,2048]{2,1,0:T(8,128)(2,1)S(1)}, bf16[2,128,2048]{2,1,0:T(8,128)(2,1)S(1)}, u32[]{:S(2)}, u32[]{:S(2)}) collective-permute-start(bf16[2,128,2048]{2,1,0:T(8,128)(2,1)S(1)} %copy-done), channel_id=1, source_target_pairs={{0,1},{1,0},{2,3},{3,2},{4,5},{5,4},{6,7},{7,6},{8,9},{9,8},{10,11... | collective-permute-start | bytes 3145736 | tf_op jit(solution)/shard_map/ppermute | solution.py:331
  103.5 16.3 %collective-permute-start.5 = (bf16[8,256,128]{2,1,0:T(8,128)(2,1)S(1)}, bf16[8,256,128]{2,1,0:T(8,128)(2,1)}, u32[]{:S(2)}, u32[]{:S(2)}) collective-permute-start(bf16[8,256,128]{2,1,0:T(8,128)(2,1)S(1)} %join.8.refs_1_), channel_id=1, source_target_pairs={{0,1},{1,0},{2,3},{3,2},{4,5},{5,4},{6,7},{7,6},{8,9},{9,8},{10,11... | collective-permute-start | bytes 1572872 | tf_op jit(solution)/shard_map/ppermute | solution.py:331
  105.4 22.3 %collective-permute-start.6 = (bf16[8,256,128]{2,1,0:T(8,128)(2,1)}, bf16[8,256,128]{2,1,0:T(8,128)(2,1)}, u32[]{:S(2)}, u32[]{:S(2)}) collective-permute-start(bf16[8,256,128]{2,1,0:T(8,128)(2,1)} %collective-permute-done.4.refs_2_), channel_id=1, source_target_pairs={{0,1},{1,0},{2,3},{3,2},{4,5},{5,4},{6,7},{7,6},{8,9},{9,8},{10,11... | collective-permute-start | bytes 1572872 | tf_op jit(solution)/shard_map/ppermute | solution.py:331
  116.3 11.4 %all-to-all-start.2 = ((bf16[4,128,256]{2,1,0:T(8,128)(2,1)}), bf16[4,128,256]{2,1,0:T(8,128)(2,1)S(1)}, u32[]{:S(2)}, u32[]{:S(2)}) async-start(bf16[4,128,256]{2,1,0:T(8,128)(2,1)} %project_queries.2), calls=%async_computation.2 | async-start | bytes 524288 | tf_op jit(solution)/shard_map/all_to_all | solution.py:318
  143.2 23.9 %copy-start.6 = (f32[2,2048]{1,0:T(2,128)S(1)}, f32[2,2048]{1,0:T(2,128)}, u32[]{:S(2)}) copy-start(f32[2,2048]{1,0:T(2,128)} %out_gain_ref.3) | copy-start | bytes 49156
  144.5 22.5 %all-to-all-start.4 = ((bf16[8,16,2048]{2,1,0:T(8,128)(2,1)}), bf16[8,16,2048]{2,1,0:T(8,128)(2,1)S(1)}, u32[]{:S(2)}, u32[]{:S(2)}) async-start(bf16[8,16,2048]{2,1,0:T(8,128)(2,1)} %merge_and_project.2), calls=%async_computation.4 | async-start | bytes 1048576 | tf_op jit(solution)/shard_map/all_to_all | solution.py:318
  148.7 13.8 %collective-permute-start.8 = (bf16[1,256,128]{2,1,0:T(8,128)(2,1)S(1)}, bf16[1,256,128]{2,1,0:T(8,128)(2,1)S(1)}, u32[]{:S(2)}, u32[]{:S(2)}) collective-permute-start(bf16[1,256,128]{2,1,0:T(8,128)(2,1)S(1)} %copy-done.7), channel_id=1, source_target_pairs={{0,128},{1,129},{16,144},{17,145},{32,160},{33,161},{48,176},{49,1... | collective-permute-start | bytes 196616 | tf_op jit(solution)/shard_map/ppermute | solution.py:327
  163.2 13.6 %collective-permute-start.9 = (bf16[2,256,128]{2,1,0:T(8,128)(2,1)}, bf16[2,256,128]{2,1,0:T(8,128)(2,1)S(1)}, u32[]{:S(2)}, u32[]{:S(2)}) collective-permute-start(bf16[2,256,128]{2,1,0:T(8,128)(2,1)} %join.9.mine_ref), channel_id=1, source_target_pairs={{0,64},{1,193},{16,80},{17,209},{32,96},{33,225},{48,112},{49,241}... | collective-permute-start | bytes 393224 | tf_op jit(solution)/shard_map/ppermute | solution.py:327
  168.1 33.4 %all-to-all-start.5 = ((bf16[8,16,2048]{2,1,0:T(8,128)(2,1)}), bf16[8,16,2048]{2,1,0:T(8,128)(2,1)S(1)}, u32[]{:S(2)}, u32[]{:S(2)}) async-start(bf16[8,16,2048]{2,1,0:T(8,128)(2,1)} %get-tuple-element.21), calls=%async_computation.5 | async-start | bytes 1048576 | tf_op jit(solution)/shard_map/all_to_all | solution.py:318
  178.4 10.3 %collective-permute-start.10 = (bf16[4,256,128]{2,1,0:T(8,128)(2,1)}, bf16[4,256,128]{2,1,0:T(8,128)(2,1)S(1)}, u32[]{:S(2)}, u32[]{:S(2)}) collective-permute-start(bf16[4,256,128]{2,1,0:T(8,128)(2,1)} %join.10.mine_ref), channel_id=1, source_target_pairs={{0,32},{1,225},{16,48},{17,241},{32,64},{33,1},{48,80},{49,17},{64... | collective-permute-start | bytes 786440 | tf_op jit(solution)/shard_map/ppermute | solution.py:327
  190.4 13.4 %collective-permute-start.11 = (bf16[8,256,128]{2,1,0:T(8,128)(2,1)}, bf16[8,256,128]{2,1,0:T(8,128)(2,1)S(1)}, u32[]{:S(2)}, u32[]{:S(2)}) collective-permute-start(bf16[8,256,128]{2,1,0:T(8,128)(2,1)} %join.11.refs_1_), channel_id=1, source_target_pairs={{0,16},{1,241},{16,32},{17,1},{32,48},{33,17},{48,64},{49,33},{64,... | collective-permute-start | bytes 1572872 | tf_op jit(solution)/shard_map/ppermute | solution.py:327
  192.4 23.3 %collective-permute-start.12 = (bf16[8,256,128]{2,1,0:T(8,128)(2,1)}, bf16[8,256,128]{2,1,0:T(8,128)(2,1)}, u32[]{:S(2)}, u32[]{:S(2)}) collective-permute-start(bf16[8,256,128]{2,1,0:T(8,128)(2,1)} %join.11.refs_1_), channel_id=1, source_target_pairs={{0,1},{1,0},{2,3},{3,2},{4,5},{5,4},{6,7},{7,6},{8,9},{9,8},{10,11... | collective-permute-start | bytes 1572872 | tf_op jit(solution)/shard_map/ppermute | solution.py:331
  203.9 19.4 %collective-permute-start.13 = (bf16[8,256,128]{2,1,0:T(8,128)(2,1)S(1)}, bf16[8,256,128]{2,1,0:T(8,128)(2,1)}, u32[]{:S(2)}, u32[]{:S(2)}) collective-permute-start(bf16[8,256,128]{2,1,0:T(8,128)(2,1)S(1)} %collective-permute-done.11.refs_2_), channel_id=1, source_target_pairs={{0,1},{1,0},{2,3},{3,2},{4,5},{5,4},{6,7},{7,6},{8,9},{9,8},{10,11... | collective-permute-start | bytes 1572872 | tf_op jit(solution)/shard_map/ppermute | solution.py:331
  212.1 11.2 %all-to-all-start.6 = ((bf16[4,128,256]{2,1,0:T(8,128)(2,1)}), bf16[4,128,256]{2,1,0:T(8,128)(2,1)S(1)}, u32[]{:S(2)}, u32[]{:S(2)}) async-start(bf16[4,128,256]{2,1,0:T(8,128)(2,1)} %project_queries.3), calls=%async_computation.6 | async-start | bytes 524288 | tf_op jit(solution)/shard_map/all_to_all | solution.py:318
  (4 other events, 26.8 us)

commit v7 on v5

--- a/solution.py
+++ b/solution.py
@@ -110,11 +110,11 @@
     )(*held_in_vmem(rows, gain))
 
 
-def query_kernel(layer, core_ref, rows_ref, mine_ref, other_ref, out_ref):
+def query_kernel(core_ref, rows_ref, mine_ref, other_ref, out_ref):
     chips, block, features = rows_ref.shape
     rows = rows_ref[...].reshape(chips * block, features)
-    mine = dot(rows, mine_ref[layer]).astype(BF16)
-    other = dot(rows, other_ref[layer]).astype(BF16)
+    mine = dot(rows, mine_ref[0]).astype(BF16)
+    other = dot(rows, other_ref[0]).astype(BF16)
     first = core_ref[0] == 0
     width = mine.shape[1]
     low = jnp.where(first, mine, other)
@@ -124,16 +124,25 @@
         out_ref[peer, :, width:] = high
 
 
-def project_queries(layer, core, rows, mine, other, copies, held):
-    chips, block, _ = rows.shape
-    return pl.pallas_call(
-        functools.partial(query_kernel, layer),
-        in_specs=[pl.BlockSpec(memory_space=pltpu.SMEM)] + in_vmem(3),
-        out_specs=in_vmem(1)[0],
-        out_shape=held((copies, chips * block, 2 * mine.shape[2]), BF16),
+def project_queries(layer, core, rows, mine, other, copies, placed):
+    chips, block, features = rows.shape
+    width = mine.shape[2]
+    weight = pl.BlockSpec((1, features, width), lambda i: (layer, 0, 0))
+    shape = (copies, chips * block, 2 * width)
+    return pl.pallas_call(
+        query_kernel,
+        grid=(1,),
+        in_specs=[
+            pl.BlockSpec(memory_space=pltpu.SMEM),
+            pl.BlockSpec(memory_space=pltpu.VMEM),
+            weight,
+            weight,
+        ],
+        out_specs=pl.BlockSpec(shape, lambda i: (0, 0, 0)),
+        out_shape=placed(shape, BF16),
         compiler_params=pltpu.CompilerParams(vmem_limit_bytes=8192 * 1024),
         name="project_queries",
-    )(core, pltpu.with_memory_space_constraint(rows, pltpu.HBM), *held_in_vmem(mine, other))
+    )(core, *held_in_vmem(rows), *[pltpu.with_memory_space_constraint(a, pltpu.HBM) for a in (mine, other)])
 
 
 def attend_kernel(groups, pieces, core_ref, *refs):
@@ -226,41 +235,31 @@
     )(*held_in_vmem(held))
 
 
-def halves_kernel(own_ref, low_ref, high_ref):
-    count = low_ref.shape[0]
-    low_ref[...] = own_ref[:count]
-    high_ref[...] = own_ref[count:]
-
-
-def halves(own):
-    shape = (own.shape[0] // 2, *own.shape[1:])
-    return pl.pallas_call(
-        halves_kernel,
-        in_specs=in_vmem(1),
-        out_specs=in_vmem(2),
-        out_shape=[vmem_out(shape)] * 2,
+def join_kernel(distance, stage_ref, mine_ref, came_ref, out_ref):
+    count = mine_ref.shape[0]
+    bit = stage_ref[0] & distance
+
+    @pl.when(bit == 0)
+    def _():
+        out_ref[:count] = mine_ref[...]
+        out_ref[count:] = came_ref[...]
+
+    @pl.when(bit != 0)
+    def _():
+        out_ref[:count] = came_ref[...]
+        out_ref[count:] = mine_ref[...]
+
+
+def join(distance, stage, mine, came, placed):
+    count, *rest = mine.shape
+    return pl.pallas_call(
+        functools.partial(join_kernel, distance),
+        in_specs=[pl.BlockSpec(memory_space=pltpu.SMEM)] + in_vmem(2),
+        out_specs=in_vmem(1)[0],
+        out_shape=placed((2 * count, *rest), BF16),
         compiler_params=pltpu.CompilerParams(vmem_limit_bytes=2048 * 1024),
-        name="halves",
-    )(*held_in_vmem(own))
-
-
-def join_kernel(*refs):
-    at = 0
-    for ref in refs[:-1]:
-        refs[-1][at : at + ref.shape[0]] = ref[...]
-        at += ref.shape[0]
-
-
-def join(*pieces):
-    count = sum(piece.shape[0] for piece in pieces)
-    return pl.pallas_call(
-        join_kernel,
-        in_specs=in_vmem(len(pieces)),
-        out_specs=in_vmem(1)[0],
-        out_shape=pltpu.HBM((count, *pieces[0].shape[1:]), BF16),
-        compiler_params=pltpu.CompilerParams(vmem_limit_bytes=4096 * 1024),
         name="join",
-    )(*held_in_vmem(*pieces))
+    )(stage, mine, came)
 
 
 def merge_kernel(layer, core_ref, *refs):
@@ -335,8 +334,13 @@
     return lax.all_to_all(value, axis, split_axis=0, concat_axis=0, tiled=True)
 
 
-def shifted(value, distance, size):
-    return lax.ppermute(value, STAGES, [(z, (z + distance) % size) for z in range(size)])
+def passed(value, distance, stages):
+    pairs = [
+        (2 * stage + core, 2 * ((stage + (distance, -distance)[core]) % stages) + core)
+        for stage in range(stages)
+        for core in range(2)
+    ]
+    return lax.ppermute(value, ("far", "near", "core"), pairs)
 
 
 def swap(value):
@@ -349,11 +353,6 @@
 
 def after(value, *others):
     return lax.optimization_barrier((value, *others))[0]
-
-
-def near_step(own, size):
-    low, high = halves(own)
-    return shifted(own, 1, size), shifted(own, -1, size), shifted(low, -2, size), shifted(high, 2, size)
 
 
 def layers(
@@ -371,6 +370,7 @@
     chips = quarters * lax.axis_size("kv")
     stages = lax.axis_size("far") * lax.axis_size("near")
     core = lax.axis_index("core").astype(jnp.int32).reshape(1)
+    stage = lax.axis_index(STAGES).astype(jnp.int32).reshape(1)
     width = key_weight.shape[2]
 
     columns = source_columns(source, source_gain[None], key_weight, value_weight, quarters)
@@ -379,16 +379,19 @@
     first, later = split(held, lax.axis_size("far"))
     own = exchange(first, "far")
     normed = after(first_norm(target, query_gain, chips), own)
-    pieces = near_step(own, stages)
+    came = passed(own, 2, stages)
+    near = join(2, stage, own, came, pltpu.VMEM)
+    came = passed(near, 1, stages)
+    far = [swap(near)]
+    far.append(swap(came))
+    near_later = lax.all_gather(after(later, near), STAGES, axis=0, tiled=True)
+    near = [near, came]
     query_other = swap(query_weight)
     out_other = swap(out_weight)
     rows = exchange(normed, CHIPS)
     mine = project_queries(0, core, rows, query_weight, query_other, quarters, pltpu.HBM)
-    near_later = lax.all_gather(after(later, mine), STAGES, axis=0, tiled=True)
-    near = join(own, *after(pieces, mine))
-    far = swap(near)
     queries = exchange(mine, "quarter")
-    (parts,) = attend(core, [queries], [near], [far])
+    (parts,) = attend(core, [queries], near, far)
     parts, out_other = lax.optimization_barrier((parts, out_other))
     parts = exchange(parts, "quarter")
     projected = merge_and_project(0, core, [parts], out_weight, out_other, chips)

time: 273 us -> 259 us (0.949)
  waiting for transfers between devices: 42.6 us -> 33.3 us
  blocking collectives: 122 us -> 130 us
  starting transfers between devices: 64.1 us -> 56.5 us
  local copies, waits for them, and re-layouts: 4.77 us -> 0.02 us
    all_to_all x3, waiting for transfers between devices: 20.3 us -> 7.87 us  [exchange(): return lax.all_to_all(value, axis, split_axis=0, concat_axis=0, tiled=True)]
    ppermute x4 -> x2, starting transfers between devices: 27.1 us -> 14.9 us  [passed(): return lax.ppermute(value, ('far', 'near', 'core'), pairs)]
    all_to_all x5, blocking collectives: 122 us -> 130 us  [exchange(): return lax.all_to_all(value, axis, split_axis=0, concat_axis=0, tiled=True)]
    unnamed x24 -> x10, local copies, waits for them, and re-layouts: 4.77 us -> 0.02 us
    ppermute x4 -> x5, starting transfers between devices: 20.4 us -> 23.8 us  [swap(): return lax.ppermute(value, 'core', [(0, 1), (1, 0)])]
    ppermute x4 -> x2, waiting for transfers between devices: 9.53 us -> 10.2 us  [passed(): return lax.ppermute(value, ('far', 'near', 'core'), pairs)]
  transfers between devices with their start and end apart: 14 -> 13, of which waited for: 7 -> 6; matrix products, arithmetic and copies ran while one was open for 0% -> 0% of each run, Pallas kernels for 3% -> 4%
where the time goes in v7:
time: 259 us; the launch traced here: 256 us
  blocking collectives  130 us (50%)
  starting transfers between devices  56.5 us (22%)
  waiting for transfers between devices  33.3 us (13%)
  Pallas kernels  22.5 us (9%)
  between operations  13.6 us (5%)
    all_to_all x5, blocking collectives, exchange(): return lax.all_to_all(value, axis, split_axis=0, concat_axis=0, tiled=True)  130 us
    ppermute x5, starting transfers between devices, swap(): return lax.ppermute(value, 'core', [(0, 1), (1, 0)])  23.8 us
    ppermute x2, starting transfers between devices, passed(): return lax.ppermute(value, ('far', 'near', 'core'), pairs)  14.9 us
    all_to_all x3, starting transfers between devices, exchange(): return lax.all_to_all(value, axis, split_axis=0, concat_axis=0, tiled=True)  13.8 us
    ppermute x2, waiting for transfers between devices, passed(): return lax.ppermute(value, ('far', 'near', 'core'), pairs)  10.2 us
    pallas_call x2, Pallas kernels, attend(): pl.pallas_call(functools.partial(attend_kernel, groups, len(mine)), in_sp...  9.25 us
    all_gather x1, waiting for transfers between devices, layers(): near_later = lax.all_gather(after(later, near), STAGES, axis=0, tiled=True)  8.88 us
    all_to_all x3, waiting for transfers between devices, exchange(): return lax.all_to_all(value, axis, split_axis=0, concat_axis=0, tiled=True)  7.87 us
  transfers between devices with their start and end apart: 13, of which 6 were waited for; matrix products, arithmetic and copies ran while one was open for 0% of the time, Pallas kernels for 4%

profile of v7, /device:TPU:65, one launch (start us, length us, event | category | flops | bytes accessed | tf_op | source)
XLA Modules:
  0.0 255.5 jit_solution(8454359395480203943)
XLA Ops:
  6.6 4.5 %source_columns.1 = bf16[4,2,96,128]{3,2,1,0:T(8,128)(2,1)} custom-call(bf16[512,2048]{1,0:T(8,128)(2,1)} %source_ref.1, f32[1,2048]{1,0:T(1,128)} %bitcast.9, bf16[2,32,2048]{2,1,0:T(8,128)(2,1)} %bitcast.7, bf16[2,32,2048]{2,1,0:T(8,128)(2,1)} %bitcast.8), custom_call_target="tpu_custom_call" | custom-call | tf_op jit(solution)/shard_map/source_columns/pallas_call | solution.py:79
  11.1 51.4 %all_to_all.40.held_ref = bf16[8,96,128]{2,1,0:T(8,128)(2,1)S(1)} all-to-all(bf16[8,96,128]{2,1,0:T(8,128)(2,1)} %bitcast.6), channel_id=1, replica_groups=mesh['grp'=2,'far'=4,'near'=4,'kv'=2,'quarter'=4,'core'=2] {'quarter','c..., dimensions={0} | all-to-all | bytes 393216 | tf_op jit(solution)/shard_map/all_to_all | solution.py:334
  63.3 17.5 %all_to_all.41.mine_ref = bf16[4,256,128]{2,1,0:T(8,128)(2,1)S(1)} all-to-all(bf16[4,256,128]{2,1,0:T(8,128)(2,1)} %get-tuple-element.15), channel_id=1, replica_groups=mesh['grp'=2,'far'=4,'near'=4,'kv'=2,'quarter'=4,'core'=2] {'far'}, dimensions={0} | all-to-all | bytes 524288 | tf_op jit(solution)/shard_map/all_to_all | solution.py:334
  80.8 9.7 %collective-permute-start.1 = (bf16[4,256,128]{2,1,0:T(8,128)(2,1)S(1)}, bf16[4,256,128]{2,1,0:T(8,128)(2,1)S(1)}, u32[]{:S(2)}, u32[]{:S(2)}) collective-permute-start(bf16[4,256,128]{2,1,0:T(8,128)(2,1)S(1)} %all_to_all.41.mine_ref), channel_id=1, source_target_pairs={{0,32},{1,225},{16,48},{17,241},{32,64},{33,1},{48,80},{49,17},{64... | collective-permute-start | bytes 786440 | tf_op jit(solution)/shard_map/ppermute | solution.py:343
  90.5 6.3 %collective-permute-done.1.came_ref = bf16[4,256,128]{2,1,0:T(8,128)(2,1)S(1)} collective-permute-done((bf16[4,256,128]{2,1,0:T(8,128)(2,1)S(1)}, bf16[4,256,128]{2,1,0:T(8,128)(2,1)S(1)}, u32[]{:S(2)}, u32[]{:S(2)}) %collective-permute-start.1) | collective-permute-done | bytes 262176 | tf_op jit(solution)/shard_map/ppermute | solution.py:343
  97.0 3.0 %collective-permute-start = (bf16[2,2048,128]{2,1,0:T(8,128)(2,1)}, bf16[2,2048,128]{2,1,0:T(8,128)(2,1)}, u32[]{:S(2)}, u32[]{:S(2)}) collective-permute-start(bf16[2,2048,128]{2,1,0:T(8,128)(2,1)} %mine_ref.3), channel_id=1, source_target_pairs={{0,1},{1,0},{2,3},{3,2},{4,5},{5,4},{6,7},{7,6},{8,9},{9,8},{10,11... | collective-permute-start | bytes 3145736 | tf_op jit(solution)/shard_map/ppermute | solution.py:347
  100.9 5.0 %all-to-all-start.2 = ((bf16[8,16,2048]{2,1,0:T(8,128)(2,1)}), bf16[8,16,2048]{2,1,0:T(8,128)(2,1)S(1)}, u32[]{:S(2)}, u32[]{:S(2)}) async-start(bf16[8,16,2048]{2,1,0:T(8,128)(2,1)} %first_norm.1), calls=%async_computation.2 | async-start | bytes 1048576 | tf_op jit(solution)/shard_map/all_to_all | solution.py:334
  106.0 5.3 %collective-permute-start.2 = (bf16[8,256,128]{2,1,0:T(8,128)(2,1)S(1)}, bf16[8,256,128]{2,1,0:T(8,128)(2,1)}, u32[]{:S(2)}, u32[]{:S(2)}) collective-permute-start(bf16[8,256,128]{2,1,0:T(8,128)(2,1)S(1)} %join.1.refs_1_), channel_id=1, source_target_pairs={{0,16},{1,241},{16,32},{17,1},{32,48},{33,17},{48,64},{49,33},{64,... | collective-permute-start | bytes 1572872 | tf_op jit(solution)/shard_map/ppermute | solution.py:343
  111.3 2.4 collective-permute-start.5
  115.7 3.9 %collective-permute-done.2.refs_2_ = bf16[8,256,128]{2,1,0:T(8,128)(2,1)} collective-permute-done((bf16[8,256,128]{2,1,0:T(8,128)(2,1)S(1)}, bf16[8,256,128]{2,1,0:T(8,128)(2,1)}, u32[]{:S(2)}, u32[]{:S(2)}) %collective-permute-start.2) | collective-permute-done | bytes 524320 | tf_op jit(solution)/shard_map/ppermute | solution.py:343
  119.6 4.8 %collective-permute-start.4 = (bf16[8,256,128]{2,1,0:T(8,128)(2,1)}, bf16[8,256,128]{2,1,0:T(8,128)(2,1)}, u32[]{:S(2)}, u32[]{:S(2)}) collective-permute-start(bf16[8,256,128]{2,1,0:T(8,128)(2,1)} %collective-permute-done.2.refs_2_), channel_id=1, source_target_pairs={{0,1},{1,0},{2,3},{3,2},{4,5},{5,4},{6,7},{7,6},{8,9},{9,8},{10,11... | collective-permute-start | bytes 1572872 | tf_op jit(solution)/shard_map/ppermute | solution.py:347
  124.4 2.4 project_queries.2
  126.7 5.2 %all-to-all-start.3 = ((bf16[4,128,256]{2,1,0:T(8,128)(2,1)}), bf16[4,128,256]{2,1,0:T(8,128)(2,1)S(1)}, u32[]{:S(2)}, u32[]{:S(2)}) async-start(bf16[4,128,256]{2,1,0:T(8,128)(2,1)} %project_queries.2), calls=%async_computation.3 | async-start | bytes 524288 | tf_op jit(solution)/shard_map/all_to_all | solution.py:334
  131.9 7.9 %all-to-all-done.3.refs_0_ = bf16[4,128,256]{2,1,0:T(8,128)(2,1)S(1)} async-done(((bf16[4,128,256]{2,1,0:T(8,128)(2,1)}), bf16[4,128,256]{2,1,0:T(8,128)(2,1)S(1)}, u32[]{:S(2)}, u32[]{:S(2)}) %all-to-all-start.3) | async-done | bytes 262176 | tf_op jit(solution)/shard_map/all_to_all | solution.py:334
  139.8 4.6 %attend.2 = bf16[4,144,256]{2,1,0:T(8,128)(2,1)} custom-call(s32[1]{0:T(128)} %bitcast.core_ref, bf16[4,128,256]{2,1,0:T(8,128)(2,1)S(1)} %all-to-all-done.3.refs_0_, bf16[8,256,128]{2,1,0:T(8,128)(2,1)} %copy-done.1, bf16[8,256,128]{2,1,0:T(8,128)(2,1)} %collective-permute-done.2.refs_2_, bf16[8,256,128]{2,1,0:T(8,128)(2,1)} %collective-permute-done.3.refs_3_, ...), custom_call_target="tpu_custom_call" | custom-call | tf_op jit(solution)/shard_map/attend/pallas_call | solution.py:202
  144.4 3.5 %all-to-all-start.4 = ((bf16[4,144,256]{2,1,0:T(8,128)(2,1)}), bf16[4,144,256]{2,1,0:T(8,128)(2,1)S(1)}, u32[]{:S(2)}, u32[]{:S(2)}) async-start(bf16[4,144,256]{2,1,0:T(8,128)(2,1)} %attend.2), calls=%async_computation.4 | async-start | bytes 589824 | tf_op jit(solution)/shard_map/all_to_all | solution.py:334
  147.9 8.9 %all-gather.2.cloned.1.call-done.refs_2_ = bf16[32,256,128]{2,1,0:T(8,128)(2,1)} async-done(((bf16[2,256,128]{2,1,0:T(8,128)(2,1)}), bf16[32,256,128]{2,1,0:T(8,128)(2,1)}) %all-gather.2.cloned.1.call-update) | async-done | bytes 2097168 | tf_op jit(solution)/shard_map/all_gather | solution.py:387
  156.8 11.7 %collective-permute-start.7 = (bf16[32,256,128]{2,1,0:T(8,128)(2,1)}, bf16[32,256,128]{2,1,0:T(8,128)(2,1)}, u32[]{:S(2)}, u32[]{:S(2)}) collective-permute-start(bf16[32,256,128]{2,1,0:T(8,128)(2,1)} %all-gather.2.cloned.1.call-done.refs_2_), channel_id=1, source_target_pairs={{0,1},{1,0},{2,3},{3,2},{4,5},{5,4},{6,7},{7,6},{8,9},{9,8},{10,11... | collective-permute-start | bytes 6291464 | tf_op jit(solution)/shard_map/ppermute | solution.py:347
  169.1 24.0 %all_to_all.42.part_ref = bf16[8,16,2048]{2,1,0:T(8,128)(2,1)S(1)} all-to-all(bf16[8,16,2048]{2,1,0:T(8,128)(2,1)S(1)} %merge_and_project.2), channel_id=1, replica_groups=mesh['grp'=2,'far'=4,'near'=4,'kv'=2,'quarter'=4,'core'=2] {'kv','quarter'}, dimensions={0} | all-to-all | bytes 1048576 | tf_op jit(solution)/shard_map/all_to_all | solution.py:334
  194.2 20.9 %all_to_all.43.rows_ref = bf16[8,16,2048]{2,1,0:T(8,128)(2,1)S(1)} all-to-all(bf16[8,16,2048]{2,1,0:T(8,128)(2,1)} %get-tuple-element.19), channel_id=1, replica_groups=mesh['grp'=2,'far'=4,'near'=4,'kv'=2,'quarter'=4,'core'=2] {'kv','quarter'}, dimensions={0} | all-to-all | bytes 1048576 | tf_op jit(solution)/shard_map/all_to_all | solution.py:334
  218.8 3.1 %collective-permute-done.6.refs_1_ = bf16[1,128,256]{2,1,0:T(8,128)(2,1)S(1)} collective-permute-done((bf16[1,128,256]{2,1,0:T(8,128)(2,1)S(1)}, bf16[1,128,256]{2,1,0:T(8,128)(2,1)S(1)}, u32[]{:S(2)}, u32[]{:S(2)}) %collective-permute-start.6) | collective-permute-done | bytes 65568 | tf_op jit(solution)/shard_map/ppermute | solution.py:351
  221.9 4.7 %attend.3 = (bf16[1,144,256]{2,1,0:T(8,128)(2,1)S(1)}, bf16[1,144,256]{2,1,0:T(8,128)(2,1)S(1)}) custom-call(s32[1]{0:T(128)} %bitcast.core_ref, bf16[1,128,256]{2,1,0:T(8,128)(2,1)S(1)} %project_queries.3.refs_0_, bf16[1,128,256]{2,1,0:T(8,128)(2,1)S(1)} %collective-permute-done.6.refs_1_, bf16[32,256,128]{2,1,0:T(8,128)(2,1)} %all-gather.2.cloned.1.call-done.refs_2_, ...), custom_call_target="tpu_custom_call" | custom-call | tf_op jit(solution)/shard_map/attend/pallas_call | solution.py:202
  228.5 3.2 %collective-permute-done.8.refs_1_ = bf16[1,144,256]{2,1,0:T(8,128)(2,1)S(1)} collective-permute-done((bf16[1,144,256]{2,1,0:T(8,128)(2,1)S(1)}, bf16[1,144,256]{2,1,0:T(8,128)(2,1)S(1)}, u32[]{:S(2)}, u32[]{:S(2)}) %collective-permute-start.8) | collective-permute-done | bytes 73760 | tf_op jit(solution)/shard_map/ppermute | solution.py:351
  232.2 15.7 %all_to_all.44.part_ref = bf16[8,16,2048]{2,1,0:T(8,128)(2,1)S(1)} all-to-all(bf16[8,16,2048]{2,1,0:T(8,128)(2,1)S(1)} %merge_and_project.3), channel_id=1, replica_groups=mesh['grp'=2,'far'=4,'near'=4,'kv'=2,'quarter'=4,'core'=2] {'kv','quarter'}, dimensions={0} | all-to-all | bytes 1048576 | tf_op jit(solution)/shard_map/all_to_all | solution.py:334
  (30 shorter events, 12.3 us)
Async XLA Ops:
  6.5 150.3 %all-gather.2.cloned.1.call-start = ((), (), s32[]{:S(2)}) async-start(), calls=%async_computation.8 | async-start | bytes 2228224 | tf_op jit(solution)/shard_map/all_gather | solution.py:387
  6.6 93.4 %copy-start.2 = (bf16[16,2048]{1,0:T(8,128)(2,1)S(1)}, bf16[16,2048]{1,0:T(8,128)(2,1)}, u32[]{:S(2)}) copy-start(bf16[16,2048]{1,0:T(8,128)(2,1)} %residual_ref.1) | copy-start | bytes 196612
  6.6 93.4 %copy-start.3 = (f32[2,2048]{1,0:T(2,128)S(1)}, f32[2,2048]{1,0:T(2,128)}, u32[]{:S(2)}) copy-start(f32[2,2048]{1,0:T(2,128)} %query_gain_ref.3) | copy-start | bytes 49156
  11.1 100.2 %copy-start = (bf16[2,128,2048]{2,1,0:T(8,128)(2,1)S(1)}, bf16[2,128,2048]{2,1,0:T(8,128)(2,1)}, u32[]{:S(2)}) copy-start(bf16[2,128,2048]{2,1,0:T(8,128)(2,1)} %refs_2_.1) | copy-start | bytes 3145732
  80.8 16.0 %collective-permute-start.1 = (bf16[4,256,128]{2,1,0:T(8,128)(2,1)S(1)}, bf16[4,256,128]{2,1,0:T(8,128)(2,1)S(1)}, u32[]{:S(2)}, u32[]{:S(2)}) collective-permute-start(bf16[4,256,128]{2,1,0:T(8,128)(2,1)S(1)} %all_to_all.41.mine_ref), channel_id=1, source_target_pairs={{0,32},{1,225},{16,48},{17,241},{32,64},{33,1},{48,80},{49,17},{64... | collective-permute-start | bytes 786440 | tf_op jit(solution)/shard_map/ppermute | solution.py:343
  96.9 29.8 %copy-start.1 = (bf16[8,256,128]{2,1,0:T(8,128)(2,1)}, bf16[8,256,128]{2,1,0:T(8,128)(2,1)S(1)}, u32[]{:S(2)}) copy-start(bf16[8,256,128]{2,1,0:T(8,128)(2,1)S(1)} %join.1.refs_1_) | copy-start | bytes 1572868
  97.0 27.4 %collective-permute-start = (bf16[2,2048,128]{2,1,0:T(8,128)(2,1)}, bf16[2,2048,128]{2,1,0:T(8,128)(2,1)}, u32[]{:S(2)}, u32[]{:S(2)}) collective-permute-start(bf16[2,2048,128]{2,1,0:T(8,128)(2,1)} %mine_ref.3), channel_id=1, source_target_pairs={{0,1},{1,0},{2,3},{3,2},{4,5},{5,4},{6,7},{7,6},{8,9},{9,8},{10,11... | collective-permute-start | bytes 3145736 | tf_op jit(solution)/shard_map/ppermute | solution.py:347
  100.9 23.4 %all-to-all-start.2 = ((bf16[8,16,2048]{2,1,0:T(8,128)(2,1)}), bf16[8,16,2048]{2,1,0:T(8,128)(2,1)S(1)}, u32[]{:S(2)}, u32[]{:S(2)}) async-start(bf16[8,16,2048]{2,1,0:T(8,128)(2,1)} %first_norm.1), calls=%async_computation.2 | async-start | bytes 1048576 | tf_op jit(solution)/shard_map/all_to_all | solution.py:334
  106.0 13.6 %collective-permute-start.2 = (bf16[8,256,128]{2,1,0:T(8,128)(2,1)S(1)}, bf16[8,256,128]{2,1,0:T(8,128)(2,1)}, u32[]{:S(2)}, u32[]{:S(2)}) collective-permute-start(bf16[8,256,128]{2,1,0:T(8,128)(2,1)S(1)} %join.1.refs_1_), channel_id=1, source_target_pairs={{0,16},{1,241},{16,32},{17,1},{32,48},{33,17},{48,64},{49,33},{64,... | collective-permute-start | bytes 1572872 | tf_op jit(solution)/shard_map/ppermute | solution.py:343
  111.3 33.1 %collective-permute-start.5 = (bf16[2,128,2048]{2,1,0:T(8,128)(2,1)S(1)}, bf16[2,128,2048]{2,1,0:T(8,128)(2,1)S(1)}, u32[]{:S(2)}, u32[]{:S(2)}) collective-permute-start(bf16[2,128,2048]{2,1,0:T(8,128)(2,1)S(1)} %copy-done), channel_id=1, source_target_pairs={{0,1},{1,0},{2,3},{3,2},{4,5},{5,4},{6,7},{7,6},{8,9},{9,8},{10,11... | collective-permute-start | bytes 3145736 | tf_op jit(solution)/shard_map/ppermute | solution.py:347
  113.7 18.2 %collective-permute-start.3 = (bf16[8,256,128]{2,1,0:T(8,128)(2,1)S(1)}, bf16[8,256,128]{2,1,0:T(8,128)(2,1)}, u32[]{:S(2)}, u32[]{:S(2)}) collective-permute-start(bf16[8,256,128]{2,1,0:T(8,128)(2,1)S(1)} %join.1.refs_1_), channel_id=1, source_target_pairs={{0,1},{1,0},{2,3},{3,2},{4,5},{5,4},{6,7},{7,6},{8,9},{9,8},{10,11... | collective-permute-start | bytes 1572872 | tf_op jit(solution)/shard_map/ppermute | solution.py:347
  119.6 20.2 %collective-permute-start.4 = (bf16[8,256,128]{2,1,0:T(8,128)(2,1)}, bf16[8,256,128]{2,1,0:T(8,128)(2,1)}, u32[]{:S(2)}, u32[]{:S(2)}) collective-permute-start(bf16[8,256,128]{2,1,0:T(8,128)(2,1)} %collective-permute-done.2.refs_2_), channel_id=1, source_target_pairs={{0,1},{1,0},{2,3},{3,2},{4,5},{5,4},{6,7},{7,6},{8,9},{9,8},{10,11... | collective-permute-start | bytes 1572872 | tf_op jit(solution)/shard_map/ppermute | solution.py:347
  126.7 13.1 %all-to-all-start.3 = ((bf16[4,128,256]{2,1,0:T(8,128)(2,1)}), bf16[4,128,256]{2,1,0:T(8,128)(2,1)S(1)}, u32[]{:S(2)}, u32[]{:S(2)}) async-start(bf16[4,128,256]{2,1,0:T(8,128)(2,1)} %project_queries.2), calls=%async_computation.3 | async-start | bytes 524288 | tf_op jit(solution)/shard_map/all_to_all | solution.py:334
  144.4 24.1 %all-to-all-start.4 = ((bf16[4,144,256]{2,1,0:T(8,128)(2,1)}), bf16[4,144,256]{2,1,0:T(8,128)(2,1)S(1)}, u32[]{:S(2)}, u32[]{:S(2)}) async-start(bf16[4,144,256]{2,1,0:T(8,128)(2,1)} %attend.2), calls=%async_computation.4 | async-start | bytes 589824 | tf_op jit(solution)/shard_map/all_to_all | solution.py:334
  147.9 45.2 %copy-start.4 = (f32[2,2048]{1,0:T(2,128)S(1)}, f32[2,2048]{1,0:T(2,128)}, u32[]{:S(2)}) copy-start(f32[2,2048]{1,0:T(2,128)} %out_gain_ref.3) | copy-start | bytes 49156
  156.8 65.0 %collective-permute-start.7 = (bf16[32,256,128]{2,1,0:T(8,128)(2,1)}, bf16[32,256,128]{2,1,0:T(8,128)(2,1)}, u32[]{:S(2)}, u32[]{:S(2)}) collective-permute-start(bf16[32,256,128]{2,1,0:T(8,128)(2,1)} %all-gather.2.cloned.1.call-done.refs_2_), channel_id=1, source_target_pairs={{0,1},{1,0},{2,3},{3,2},{4,5},{5,4},{6,7},{7,6},{8,9},{9,8},{10,11... | collective-permute-start | bytes 6291464 | tf_op jit(solution)/shard_map/ppermute | solution.py:347
  216.8 5.0 %collective-permute-start.6 = (bf16[1,128,256]{2,1,0:T(8,128)(2,1)S(1)}, bf16[1,128,256]{2,1,0:T(8,128)(2,1)S(1)}, u32[]{:S(2)}, u32[]{:S(2)}) collective-permute-start(bf16[1,128,256]{2,1,0:T(8,128)(2,1)S(1)} %project_queries.3.refs_0_), channel_id=1, source_target_pairs={{0,2},{2,0},{4,6},{6,4},{1,3},{3,1},{5,7},{7,5},{8,10},{10,8},{12,... | collective-permute-start | bytes 196616 | tf_op jit(solution)/shard_map/ppermute | solution.py:351
  226.5 5.1 %collective-permute-start.8 = (bf16[1,144,256]{2,1,0:T(8,128)(2,1)S(1)}, bf16[1,144,256]{2,1,0:T(8,128)(2,1)S(1)}, u32[]{:S(2)}, u32[]{:S(2)}) collective-permute-start(bf16[1,144,256]{2,1,0:T(8,128)(2,1)S(1)} %get-tuple-element.23), channel_id=1, source_target_pairs={{0,2},{2,0},{4,6},{6,4},{1,3},{3,1},{5,7},{7,5},{8,10},{10,8},{12,... | collective-permute-start | bytes 221192 | tf_op jit(solution)/shard_map/ppermute | solution.py:351
Sparse Core Ops, SparseCore 0:
  97.1 59.6 all-gather.1

commit v8 on v7

--- a/solution.py
+++ b/solution.py
@@ -94,25 +94,22 @@
 
 
 def norm_kernel(rows_ref, gain_ref, out_ref):
-    normed = scaled(rows_ref[...].astype(F32), gain_ref[:1, :]).astype(BF16)
-    for peer in range(out_ref.shape[0]):
-        out_ref[peer] = normed
-
-
-def first_norm(rows, gain, chips):
+    out_ref[0] = scaled(rows_ref[...].astype(F32), gain_ref[:1, :]).astype(BF16)
+
+
+def first_norm(rows, gain):
     return pl.pallas_call(
         norm_kernel,
         in_specs=in_vmem(2),
         out_specs=in_vmem(1)[0],
-        out_shape=pltpu.HBM((chips, *rows.shape), BF16),
+        out_shape=vmem_out((1, *rows.shape)),
         compiler_params=pltpu.CompilerParams(vmem_limit_bytes=4096 * 1024),
         name="first_norm",
     )(*held_in_vmem(rows, gain))
 
 
-def query_kernel(core_ref, rows_ref, mine_ref, other_ref, out_ref):
-    chips, block, features = rows_ref.shape
-    rows = rows_ref[...].reshape(chips * block, features)
+def query_kernel(order, core_ref, rows_ref, mine_ref, other_ref, out_ref):
+    rows = jnp.concatenate([rows_ref[chip] for chip in order], axis=0)
     mine = dot(rows, mine_ref[0]).astype(BF16)
     other = dot(rows, other_ref[0]).astype(BF16)
     first = core_ref[0] == 0
@@ -124,13 +121,13 @@
         out_ref[peer, :, width:] = high
 
 
-def project_queries(layer, core, rows, mine, other, copies, placed):
+def project_queries(layer, core, rows, order, mine, other, copies, placed):
     chips, block, features = rows.shape
     width = mine.shape[2]
     weight = pl.BlockSpec((1, features, width), lambda i: (layer, 0, 0))
     shape = (copies, chips * block, 2 * width)
     return pl.pallas_call(
-        query_kernel,
+        functools.partial(query_kernel, tuple(order)),
         grid=(1,),
         in_specs=[
             pl.BlockSpec(memory_space=pltpu.SMEM),
@@ -334,13 +331,13 @@
     return lax.all_to_all(value, axis, split_axis=0, concat_axis=0, tiled=True)
 
 
-def passed(value, distance, stages):
+def passed(value, distance, axes, size):
     pairs = [
-        (2 * stage + core, 2 * ((stage + (distance, -distance)[core]) % stages) + core)
-        for stage in range(stages)
+        (2 * at + core, 2 * ((at + (distance, -distance)[core]) % size) + core)
+        for at in range(size)
         for core in range(2)
     ]
-    return lax.ppermute(value, ("far", "near", "core"), pairs)
+    return lax.ppermute(value, (*axes, "core"), pairs)
 
 
 def swap(value):
@@ -370,6 +367,7 @@
     chips = quarters * lax.axis_size("kv")
     stages = lax.axis_size("far") * lax.axis_size("near")
     core = lax.axis_index("core").astype(jnp.int32).reshape(1)
+    chip = lax.axis_index(CHIPS).astype(jnp.int32).reshape(1)
     stage = lax.axis_index(STAGES).astype(jnp.int32).reshape(1)
     width = key_weight.shape[2]
 
@@ -378,18 +376,22 @@
     held = exchange(columns, GROUP)
     first, later = split(held, lax.axis_size("far"))
     own = exchange(first, "far")
-    normed = after(first_norm(target, query_gain, chips), own)
-    came = passed(own, 2, stages)
+    rows = first_norm(target, query_gain)
+    for distance in [chips >> bit for bit in range(1, chips.bit_length())]:
+        came = passed(rows, distance, CHIPS, chips)
+        rows = join(distance, chip, rows, came, pltpu.VMEM)
+    width_of_chip = chips.bit_length() - 1
+    order = [int(f"{at:0{width_of_chip}b}"[::-1], 2) for at in range(chips)]
+    came = passed(own, 2, STAGES, stages)
     near = join(2, stage, own, came, pltpu.VMEM)
-    came = passed(near, 1, stages)
+    came = passed(near, 1, STAGES, stages)
     far = [swap(near)]
     far.append(swap(came))
-    near_later = lax.all_gather(after(later, near), STAGES, axis=0, tiled=True)
+    near_later = lax.all_gather(after(later, own), STAGES, axis=0, tiled=True)
     near = [near, came]
     query_other = swap(query_weight)
     out_other = swap(out_weight)
-    rows = exchange(normed, CHIPS)
-    mine = project_queries(0, core, rows, query_weight, query_other, quarters, pltpu.HBM)
+    mine = project_queries(0, core, rows, order, query_weight, query_other, quarters, pltpu.HBM)
     queries = exchange(mine, "quarter")
     (parts,) = attend(core, [queries], near, far)
     parts, out_other = lax.optimization_barrier((parts, out_other))
@@ -400,7 +402,7 @@
 
     rows = exchange(normed, CHIPS)
     far_later = swap(near_later)
-    mine = project_queries(1, core, rows, query_weight, query_other, 1, pltpu.VMEM)
+    mine = project_queries(1, core, rows, range(chips), query_weight, query_other, 1, pltpu.VMEM)
     theirs = beside(mine, quarters)
     kept, sent = attend(core, [mine, theirs], [near_later], [far_later])
     came = beside(sent, quarters)

time: 259 us -> 251 us (0.969)
  the two profiles are of different devices: /device:TPU:65 before, /device:TPU:80 now
where the time goes in v8:
time: 251 us; the launch traced here: 249 us
  blocking collectives  135 us (54%)
  starting transfers between devices  39.8 us (16%)
  waiting for transfers between devices  39.6 us (16%)
  Pallas kernels  21.8 us (9%)
  between operations  13.7 us (5%)
    all_to_all x6, blocking collectives, exchange(): return lax.all_to_all(value, axis, split_axis=0, concat_axis=0, tiled=True)  135 us
    ppermute x5, waiting for transfers between devices, passed(): return lax.ppermute(value, (*axes, 'core'), pairs)  24 us
    ppermute x5, starting transfers between devices, passed(): return lax.ppermute(value, (*axes, 'core'), pairs)  19.1 us
    ppermute x5, starting transfers between devices, swap(): return lax.ppermute(value, 'core', [(0, 1), (1, 0)])  12.9 us
    ppermute x2, waiting for transfers between devices, beside(): return lax.ppermute(value, 'quarter', [(q, q ^ 1) for q in range(quarters)])  10.5 us
    pallas_call x2, Pallas kernels, attend(): pl.pallas_call(functools.partial(attend_kernel, groups, len(mine)), in_sp...  9.25 us
  transfers between devices with their start and end apart: 14, of which 7 were waited for; matrix products, arithmetic and copies ran while one was open for 0% of the time, Pallas kernels for 4%

profile of v8, /device:TPU:80, one launch (start us, length us, event | category | flops | bytes accessed | tf_op | source)
XLA Modules:
  0.0 249.4 jit_solution(6933888396195606717)
XLA Ops:
  6.6 4.6 %source_columns.1 = bf16[4,2,96,128]{3,2,1,0:T(8,128)(2,1)} custom-call(bf16[512,2048]{1,0:T(8,128)(2,1)} %source_ref.1, f32[1,2048]{1,0:T(1,128)} %bitcast.10, bf16[2,32,2048]{2,1,0:T(8,128)(2,1)} %bitcast.8, bf16[2,32,2048]{2,1,0:T(8,128)(2,1)} %bitcast.9), custom_call_target="tpu_custom_call" | custom-call | tf_op jit(solution)/shard_map/source_columns/pallas_call | solution.py:79
  11.1 13.3 %all_to_all.35.held_ref = bf16[8,96,128]{2,1,0:T(8,128)(2,1)S(1)} all-to-all(bf16[8,96,128]{2,1,0:T(8,128)(2,1)} %bitcast.7), channel_id=1, replica_groups=mesh['grp'=2,'far'=4,'near'=4,'kv'=2,'quarter'=4,'core'=2] {'quarter','c..., dimensions={0} | all-to-all | bytes 393216 | tf_op jit(solution)/shard_map/all_to_all | solution.py:331
  25.3 59.8 %all_to_all.36.mine_ref = bf16[4,256,128]{2,1,0:T(8,128)(2,1)S(1)} all-to-all(bf16[4,256,128]{2,1,0:T(8,128)(2,1)} %get-tuple-element.14), channel_id=1, replica_groups=mesh['grp'=2,'far'=4,'near'=4,'kv'=2,'quarter'=4,'core'=2] {'far'}, dimensions={0} | all-to-all | bytes 524288 | tf_op jit(solution)/shard_map/all_to_all | solution.py:331
  87.0 3.6 %collective-permute-start.4 = (bf16[4,256,128]{2,1,0:T(8,128)(2,1)S(1)}, bf16[4,256,128]{2,1,0:T(8,128)(2,1)S(1)}, u32[]{:S(2)}, u32[]{:S(2)}) collective-permute-start(bf16[4,256,128]{2,1,0:T(8,128)(2,1)S(1)} %all_to_all.36.mine_ref), channel_id=1, source_target_pairs={{0,32},{1,225},{16,48},{17,241},{32,64},{33,1},{48,80},{49,17},{64... | collective-permute-start | bytes 786440 | tf_op jit(solution)/shard_map/ppermute | solution.py:340
  90.6 7.6 %collective-permute-done.4.came_ref = bf16[4,256,128]{2,1,0:T(8,128)(2,1)S(1)} collective-permute-done((bf16[4,256,128]{2,1,0:T(8,128)(2,1)S(1)}, bf16[4,256,128]{2,1,0:T(8,128)(2,1)S(1)}, u32[]{:S(2)}, u32[]{:S(2)}) %collective-permute-start.4) | collective-permute-done | bytes 262176 | tf_op jit(solution)/shard_map/ppermute | solution.py:340
  98.3 5.5 %collective-permute-start.5 = (bf16[8,256,128]{2,1,0:T(8,128)(2,1)S(1)}, bf16[8,256,128]{2,1,0:T(8,128)(2,1)}, u32[]{:S(2)}, u32[]{:S(2)}) collective-permute-start(bf16[8,256,128]{2,1,0:T(8,128)(2,1)S(1)} %join.7.refs_1_), channel_id=1, source_target_pairs={{0,16},{1,241},{16,32},{17,1},{32,48},{33,17},{48,64},{49,33},{64,... | collective-permute-start | bytes 1572872 | tf_op jit(solution)/shard_map/ppermute | solution.py:340
  103.7 4.6 %collective-permute-start.8 = (bf16[2,128,2048]{2,1,0:T(8,128)(2,1)S(1)}, bf16[2,128,2048]{2,1,0:T(8,128)(2,1)S(1)}, u32[]{:S(2)}, u32[]{:S(2)}) collective-permute-start(bf16[2,128,2048]{2,1,0:T(8,128)(2,1)S(1)} %copy-done), channel_id=1, source_target_pairs={{0,1},{1,0},{2,3},{3,2},{4,5},{5,4},{6,7},{7,6},{8,9},{9,8},{10,11... | collective-permute-start | bytes 3145736 | tf_op jit(solution)/shard_map/ppermute | solution.py:344
  108.5 5.9 %collective-permute-start = (bf16[1,16,2048]{2,1,0:T(8,128)(2,1)S(1)}, bf16[1,16,2048]{2,1,0:T(8,128)(2,1)S(1)}, u32[]{:S(2)}, u32[]{:S(2)}) collective-permute-start(bf16[1,16,2048]{2,1,0:T(8,128)(2,1)S(1)} %first_norm.1.mine_ref), channel_id=1, source_target_pairs={{0,8},{1,9},{2,10},{3,11},{4,12},{5,13},{6,14},{7,15},{8,0},{9,1},... | collective-permute-start | bytes 196616 | tf_op jit(solution)/shard_map/ppermute | solution.py:340
  114.4 5.0 %collective-permute-done.came_ref = bf16[1,16,2048]{2,1,0:T(8,128)(2,1)S(1)} collective-permute-done((bf16[1,16,2048]{2,1,0:T(8,128)(2,1)S(1)}, bf16[1,16,2048]{2,1,0:T(8,128)(2,1)S(1)}, u32[]{:S(2)}, u32[]{:S(2)}) %collective-permute-start) | collective-permute-done | bytes 65568 | tf_op jit(solution)/shard_map/ppermute | solution.py:340
  121.4 8.5 %collective-permute-done.1.came_ref = bf16[2,16,2048]{2,1,0:T(8,128)(2,1)S(1)} collective-permute-done((bf16[2,16,2048]{2,1,0:T(8,128)(2,1)S(1)}, bf16[2,16,2048]{2,1,0:T(8,128)(2,1)S(1)}, u32[]{:S(2)}, u32[]{:S(2)}) %collective-permute-start.1) | collective-permute-done | bytes 131104 | tf_op jit(solution)/shard_map/ppermute | solution.py:340
  129.9 2.2 collective-permute-start.2
  134.1 2.4 collective-permute-start.7
  136.6 2.9 %collective-permute-done.2.came_ref = bf16[4,16,2048]{2,1,0:T(8,128)(2,1)S(1)} collective-permute-done((bf16[4,16,2048]{2,1,0:T(8,128)(2,1)S(1)}, bf16[4,16,2048]{2,1,0:T(8,128)(2,1)S(1)}, u32[]{:S(2)}, u32[]{:S(2)}) %collective-permute-start.2) | collective-permute-done | bytes 262176 | tf_op jit(solution)/shard_map/ppermute | solution.py:340
  139.5 2.3 project_queries.2
  141.9 10.6 %all_to_all.37.refs_0_ = bf16[4,128,256]{2,1,0:T(8,128)(2,1)S(1)} all-to-all(bf16[4,128,256]{2,1,0:T(8,128)(2,1)} %project_queries.2), channel_id=1, replica_groups=mesh['grp'=2,'far'=4,'near'=4,'kv'=2,'quarter'=4,'core'=2] {'quarter'}, dimensions={0} | all-to-all | bytes 524288 | tf_op jit(solution)/shard_map/all_to_all | solution.py:331
  152.5 4.6 %attend.2 = bf16[4,144,256]{2,1,0:T(8,128)(2,1)} custom-call(s32[1]{0:T(128)} %bitcast.core_ref, bf16[4,128,256]{2,1,0:T(8,128)(2,1)S(1)} %all_to_all.37.refs_0_, bf16[8,256,128]{2,1,0:T(8,128)(2,1)} %copy-done.1, bf16[8,256,128]{2,1,0:T(8,128)(2,1)} %collective-permute-done.5.refs_2_, bf16[8,256,128]{2,1,0:T(8,128)(2,1)} %collective-permute-done.6.refs_3_, ...), custom_call_target="tpu_custom_call" | custom-call | tf_op jit(solution)/shard_map/attend/pallas_call | solution.py:199
  157.1 3.5 %all-to-all-start.3 = ((bf16[4,144,256]{2,1,0:T(8,128)(2,1)}), bf16[4,144,256]{2,1,0:T(8,128)(2,1)S(1)}, u32[]{:S(2)}, u32[]{:S(2)}) async-start(bf16[4,144,256]{2,1,0:T(8,128)(2,1)} %attend.2), calls=%async_computation.3 | async-start | bytes 589824 | tf_op jit(solution)/shard_map/all_to_all | solution.py:331
  162.6 4.9 %all-to-all-done.3.refs_0_ = bf16[4,144,256]{2,1,0:T(8,128)(2,1)S(1)} async-done(((bf16[4,144,256]{2,1,0:T(8,128)(2,1)}), bf16[4,144,256]{2,1,0:T(8,128)(2,1)S(1)}, u32[]{:S(2)}, u32[]{:S(2)}) %all-to-all-start.3) | async-done | bytes 294944 | tf_op jit(solution)/shard_map/all_to_all | solution.py:331
  168.1 18.1 %all_to_all.38.part_ref = bf16[8,16,2048]{2,1,0:T(8,128)(2,1)S(1)} all-to-all(bf16[8,16,2048]{2,1,0:T(8,128)(2,1)S(1)} %merge_and_project.2), channel_id=1, replica_groups=mesh['grp'=2,'far'=4,'near'=4,'kv'=2,'quarter'=4,'core'=2] {'kv','quarter'}, dimensions={0} | all-to-all | bytes 1048576 | tf_op jit(solution)/shard_map/all_to_all | solution.py:331
  187.4 16.7 %all_to_all.39.rows_ref = bf16[8,16,2048]{2,1,0:T(8,128)(2,1)S(1)} all-to-all(bf16[8,16,2048]{2,1,0:T(8,128)(2,1)} %get-tuple-element.17), channel_id=1, replica_groups=mesh['grp'=2,'far'=4,'near'=4,'kv'=2,'quarter'=4,'core'=2] {'kv','quarter'}, dimensions={0} | all-to-all | bytes 1048576 | tf_op jit(solution)/shard_map/all_to_all | solution.py:331
  207.9 4.0 %collective-permute-done.9.refs_1_ = bf16[1,128,256]{2,1,0:T(8,128)(2,1)S(1)} collective-permute-done((bf16[1,128,256]{2,1,0:T(8,128)(2,1)S(1)}, bf16[1,128,256]{2,1,0:T(8,128)(2,1)S(1)}, u32[]{:S(2)}, u32[]{:S(2)}) %collective-permute-start.9) | collective-permute-done | bytes 65568 | tf_op jit(solution)/shard_map/ppermute | solution.py:348
  211.9 4.7 %attend.3 = (bf16[1,144,256]{2,1,0:T(8,128)(2,1)S(1)}, bf16[1,144,256]{2,1,0:T(8,128)(2,1)S(1)}) custom-call(s32[1]{0:T(128)} %bitcast.core_ref, bf16[1,128,256]{2,1,0:T(8,128)(2,1)S(1)} %project_queries.3.refs_0_, bf16[1,128,256]{2,1,0:T(8,128)(2,1)S(1)} %collective-permute-done.9.refs_1_, bf16[32,256,128]{2,1,0:T(8,128)(2,1)} %all-gather.2.cloned.1.call-done.refs_2_, ...), custom_call_target="tpu_custom_call" | custom-call | tf_op jit(solution)/shard_map/attend/pallas_call | solution.py:199
  218.8 6.5 %collective-permute-done.11.refs_1_ = bf16[1,144,256]{2,1,0:T(8,128)(2,1)S(1)} collective-permute-done((bf16[1,144,256]{2,1,0:T(8,128)(2,1)S(1)}, bf16[1,144,256]{2,1,0:T(8,128)(2,1)S(1)}, u32[]{:S(2)}, u32[]{:S(2)}) %collective-permute-start.11) | collective-permute-done | bytes 73760 | tf_op jit(solution)/shard_map/ppermute | solution.py:348
  225.8 15.9 %all_to_all.40.part_ref = bf16[8,16,2048]{2,1,0:T(8,128)(2,1)S(1)} all-to-all(bf16[8,16,2048]{2,1,0:T(8,128)(2,1)S(1)} %merge_and_project.3), channel_id=1, replica_groups=mesh['grp'=2,'far'=4,'near'=4,'kv'=2,'quarter'=4,'core'=2] {'kv','quarter'}, dimensions={0} | all-to-all | bytes 1048576 | tf_op jit(solution)/shard_map/all_to_all | solution.py:331
  (36 shorter events, 17.9 us)
Async XLA Ops:
  6.5 154.1 %all-gather.2.cloned.1.call-start = ((), (), s32[]{:S(2)}) async-start(), calls=%async_computation.7 | async-start | bytes 2228224 | tf_op jit(solution)/shard_map/all_gather | solution.py:390
  6.6 97.2 %copy-start = (bf16[2,128,2048]{2,1,0:T(8,128)(2,1)S(1)}, bf16[2,128,2048]{2,1,0:T(8,128)(2,1)}, u32[]{:S(2)}) copy-start(bf16[2,128,2048]{2,1,0:T(8,128)(2,1)} %refs_2_.1) | copy-start | bytes 3145732
  6.6 101.8 %copy-start.2 = (bf16[16,2048]{1,0:T(8,128)(2,1)S(1)}, bf16[16,2048]{1,0:T(8,128)(2,1)}, u32[]{:S(2)}) copy-start(bf16[16,2048]{1,0:T(8,128)(2,1)} %residual_ref.1) | copy-start | bytes 196612
  6.6 101.8 %copy-start.3 = (f32[2,2048]{1,0:T(2,128)S(1)}, f32[2,2048]{1,0:T(2,128)}, u32[]{:S(2)}) copy-start(f32[2,2048]{1,0:T(2,128)} %query_gain_ref.3) | copy-start | bytes 49156
  85.1 54.4 %collective-permute-start.3 = (bf16[2,2048,128]{2,1,0:T(8,128)(2,1)}, bf16[2,2048,128]{2,1,0:T(8,128)(2,1)}, u32[]{:S(2)}, u32[]{:S(2)}) collective-permute-start(bf16[2,2048,128]{2,1,0:T(8,128)(2,1)} %mine_ref.3), channel_id=1, source_target_pairs={{0,1},{1,0},{2,3},{3,2},{4,5},{5,4},{6,7},{7,6},{8,9},{9,8},{10,11... | collective-permute-start | bytes 3145736 | tf_op jit(solution)/shard_map/ppermute | solution.py:344
  87.0 11.2 %collective-permute-start.4 = (bf16[4,256,128]{2,1,0:T(8,128)(2,1)S(1)}, bf16[4,256,128]{2,1,0:T(8,128)(2,1)S(1)}, u32[]{:S(2)}, u32[]{:S(2)}) collective-permute-start(bf16[4,256,128]{2,1,0:T(8,128)(2,1)S(1)} %all_to_all.36.mine_ref), channel_id=1, source_target_pairs={{0,32},{1,225},{16,48},{17,241},{32,64},{33,1},{48,80},{49,17},{64... | collective-permute-start | bytes 786440 | tf_op jit(solution)/shard_map/ppermute | solution.py:340
  98.3 43.6 %copy-start.1 = (bf16[8,256,128]{2,1,0:T(8,128)(2,1)}, bf16[8,256,128]{2,1,0:T(8,128)(2,1)S(1)}, u32[]{:S(2)}) copy-start(bf16[8,256,128]{2,1,0:T(8,128)(2,1)S(1)} %join.7.refs_1_) | copy-start | bytes 1572868
  98.3 35.8 %collective-permute-start.5 = (bf16[8,256,128]{2,1,0:T(8,128)(2,1)S(1)}, bf16[8,256,128]{2,1,0:T(8,128)(2,1)}, u32[]{:S(2)}, u32[]{:S(2)}) collective-permute-start(bf16[8,256,128]{2,1,0:T(8,128)(2,1)S(1)} %join.7.refs_1_), channel_id=1, source_target_pairs={{0,16},{1,241},{16,32},{17,1},{32,48},{33,17},{48,64},{49,33},{64,... | collective-permute-start | bytes 1572872 | tf_op jit(solution)/shard_map/ppermute | solution.py:340
  103.7 53.3 %collective-permute-start.8 = (bf16[2,128,2048]{2,1,0:T(8,128)(2,1)S(1)}, bf16[2,128,2048]{2,1,0:T(8,128)(2,1)S(1)}, u32[]{:S(2)}, u32[]{:S(2)}) collective-permute-start(bf16[2,128,2048]{2,1,0:T(8,128)(2,1)S(1)} %copy-done), channel_id=1, source_target_pairs={{0,1},{1,0},{2,3},{3,2},{4,5},{5,4},{6,7},{7,6},{8,9},{9,8},{10,11... | collective-permute-start | bytes 3145736 | tf_op jit(solution)/shard_map/ppermute | solution.py:344
  108.5 10.9 %collective-permute-start = (bf16[1,16,2048]{2,1,0:T(8,128)(2,1)S(1)}, bf16[1,16,2048]{2,1,0:T(8,128)(2,1)S(1)}, u32[]{:S(2)}, u32[]{:S(2)}) collective-permute-start(bf16[1,16,2048]{2,1,0:T(8,128)(2,1)S(1)} %first_norm.1.mine_ref), channel_id=1, source_target_pairs={{0,8},{1,9},{2,10},{3,11},{4,12},{5,13},{6,14},{7,15},{8,0},{9,1},... | collective-permute-start | bytes 196616 | tf_op jit(solution)/shard_map/ppermute | solution.py:340
  119.5 10.5 %collective-permute-start.1 = (bf16[2,16,2048]{2,1,0:T(8,128)(2,1)S(1)}, bf16[2,16,2048]{2,1,0:T(8,128)(2,1)S(1)}, u32[]{:S(2)}, u32[]{:S(2)}) collective-permute-start(bf16[2,16,2048]{2,1,0:T(8,128)(2,1)S(1)} %join.4.mine_ref), channel_id=1, source_target_pairs={{0,4},{1,13},{2,6},{3,15},{4,8},{5,1},{6,10},{7,3},{8,12},{9,5},{1... | collective-permute-start | bytes 393224 | tf_op jit(solution)/shard_map/ppermute | solution.py:340
  129.9 9.5 %collective-permute-start.2 = (bf16[4,16,2048]{2,1,0:T(8,128)(2,1)S(1)}, bf16[4,16,2048]{2,1,0:T(8,128)(2,1)S(1)}, u32[]{:S(2)}, u32[]{:S(2)}) collective-permute-start(bf16[4,16,2048]{2,1,0:T(8,128)(2,1)S(1)} %join.5.mine_ref), channel_id=1, source_target_pairs={{0,2},{1,15},{2,4},{3,1},{4,6},{5,3},{6,8},{7,5},{8,10},{9,7},{10,... | collective-permute-start | bytes 786440 | tf_op jit(solution)/shard_map/ppermute | solution.py:340
  132.1 20.3 %collective-permute-start.6 = (bf16[8,256,128]{2,1,0:T(8,128)(2,1)S(1)}, bf16[8,256,128]{2,1,0:T(8,128)(2,1)}, u32[]{:S(2)}, u32[]{:S(2)}) collective-permute-start(bf16[8,256,128]{2,1,0:T(8,128)(2,1)S(1)} %join.7.refs_1_), channel_id=1, source_target_pairs={{0,1},{1,0},{2,3},{3,2},{4,5},{5,4},{6,7},{7,6},{8,9},{9,8},{10,11... | collective-permute-start | bytes 1572872 | tf_op jit(solution)/shard_map/ppermute | solution.py:344
  134.1 18.4 %collective-permute-start.7 = (bf16[8,256,128]{2,1,0:T(8,128)(2,1)}, bf16[8,256,128]{2,1,0:T(8,128)(2,1)}, u32[]{:S(2)}, u32[]{:S(2)}) collective-permute-start(bf16[8,256,128]{2,1,0:T(8,128)(2,1)} %collective-permute-done.5.refs_2_), channel_id=1, source_target_pairs={{0,1},{1,0},{2,3},{3,2},{4,5},{5,4},{6,7},{7,6},{8,9},{9,8},{10,11... | collective-permute-start | bytes 1572872 | tf_op jit(solution)/shard_map/ppermute | solution.py:344
  157.1 10.5 %all-to-all-start.3 = ((bf16[4,144,256]{2,1,0:T(8,128)(2,1)}), bf16[4,144,256]{2,1,0:T(8,128)(2,1)S(1)}, u32[]{:S(2)}, u32[]{:S(2)}) async-start(bf16[4,144,256]{2,1,0:T(8,128)(2,1)} %attend.2), calls=%async_computation.3 | async-start | bytes 589824 | tf_op jit(solution)/shard_map/all_to_all | solution.py:331
  160.6 25.7 %copy-start.4 = (f32[2,2048]{1,0:T(2,128)S(1)}, f32[2,2048]{1,0:T(2,128)}, u32[]{:S(2)}) copy-start(f32[2,2048]{1,0:T(2,128)} %out_gain_ref.3) | copy-start | bytes 49156
  160.6 51.3 %collective-permute-start.10 = (bf16[32,256,128]{2,1,0:T(8,128)(2,1)}, bf16[32,256,128]{2,1,0:T(8,128)(2,1)}, u32[]{:S(2)}, u32[]{:S(2)}) collective-permute-start(bf16[32,256,128]{2,1,0:T(8,128)(2,1)} %all-gather.2.cloned.1.call-done.refs_2_), channel_id=1, source_target_pairs={{0,1},{1,0},{2,3},{3,2},{4,5},{5,4},{6,7},{7,6},{8,9},{9,8},{10,11... | collective-permute-start | bytes 6291464 | tf_op jit(solution)/shard_map/ppermute | solution.py:344
  205.8 6.2 %collective-permute-start.9 = (bf16[1,128,256]{2,1,0:T(8,128)(2,1)S(1)}, bf16[1,128,256]{2,1,0:T(8,128)(2,1)S(1)}, u32[]{:S(2)}, u32[]{:S(2)}) collective-permute-start(bf16[1,128,256]{2,1,0:T(8,128)(2,1)S(1)} %project_queries.3.refs_0_), channel_id=1, source_target_pairs={{0,2},{2,0},{4,6},{6,4},{1,3},{3,1},{5,7},{7,5},{8,10},{10,8},{12,... | collective-permute-start | bytes 196616 | tf_op jit(solution)/shard_map/ppermute | solution.py:348
  216.6 8.7 %collective-permute-start.11 = (bf16[1,144,256]{2,1,0:T(8,128)(2,1)S(1)}, bf16[1,144,256]{2,1,0:T(8,128)(2,1)S(1)}, u32[]{:S(2)}, u32[]{:S(2)}) collective-permute-start(bf16[1,144,256]{2,1,0:T(8,128)(2,1)S(1)} %get-tuple-element.21), channel_id=1, source_target_pairs={{0,2},{2,0},{4,6},{6,4},{1,3},{3,1},{5,7},{7,5},{8,10},{10,8},{12,... | collective-permute-start | bytes 221192 | tf_op jit(solution)/shard_map/ppermute | solution.py:348
Sparse Core Ops, SparseCore 0:
  85.2 68.6 all-gather.1
